TPU v7x, 32 devices: a whole 2x2x4 slice. The times are simulated.
32 devices in a mesh: fs: 8 (over z, core), tp: 4 (over y, x).
Axes of the slice: x: 2, y: 2, z: 4, core: 2. Of those that a mesh axis runs over, the one named last changes fastest.
Arguments:
- prompt: bfloat16 [1024, 2048], P('tp'), may hold values from -6 to 6
- norm_gain: float32 [2048], P('fs'), may hold values from 0.1 to 1.9
- gate_master: float32 [32, 2048, 512], P(None, 'fs', 'tp'), may hold values from -6 to 6
- up_master: float32 [32, 2048, 512], P(None, 'fs', 'tp'), may hold values from -6 to 6
- down_master: float32 [32, 2048, 512], P(None, 'fs', 'tp'), may hold values from -6 to 6
- group_choice: int32 [1024], P('tp'), may hold values from 0 to 3
- inner_choice: int32 [1024, 2], P('tp'), may hold values from 0 to 7, as said below
- route_weight: float32 [1024, 2], P('tp'), may hold values from 0.2 to 1
Outputs:
- gate_served: bfloat16 [2048, 16384], P(None, 'fs')
- up_served: bfloat16 [2048, 16384], P(None, 'fs')
- down_served: bfloat16 [2048, 16384], P(None, 'fs')
- mixed: bfloat16 [1024, 2048], P('tp', 'fs')
Inputs may be any that keep to these rules, and one draw needn't show every extreme that they name: `inner_choice`: the two experts of a token differ.
All inputs are finite; a program needn't handle non-finite values.
Results may differ from a plain program's by a relative error of at most 0.0081.
Values may be sent and summed in bfloat16 or wider, within the bound.
No kernel may reach another device: no remote copies, remote signals or barrier semaphores. Data moves between devices by JAX's collectives and lax.ppermute only.
A program may use at most 128 MiB of HBM per device.

v0:
```python
import jax
import jax.numpy as jnp
from jax import lax
from jax.sharding import PartitionSpec as P

FF = 512
GROUPS = 4
EPG = 8


def flatten_rows(piece):
    count, experts, rows, hidden = piece.shape
    return piece.transpose(0, 2, 1, 3).reshape(count, rows, experts * hidden)


def restore_rows(gathered, rows):
    parts = lax.axis_size("tp")
    count, total, width = gathered.shape
    blocks = total // (parts * rows)
    ordered = gathered.reshape(count, parts, blocks, rows, width).transpose(0, 2, 1, 3, 4)
    return ordered.reshape(count, total, width)


def activations(normed, gate_local, up_local, column_weight):
    width = normed.shape[1]
    gate_act = jnp.dot(normed, gate_local, preferred_element_type=jnp.float32) * width ** (-0.5)
    up_act = jnp.dot(normed, up_local, preferred_element_type=jnp.float32) * width ** (-0.5)
    return (column_weight * jax.nn.silu(gate_act) * up_act).astype(jnp.bfloat16)


def route_columns(weight, columns, experts):
    first = lax.axis_index("fs") * columns
    owner = (first + jnp.arange(columns, dtype=jnp.int32)) // FF
    onehot = (owner[None, :] == jnp.arange(experts, dtype=jnp.int32)[:, None]).astype(jnp.float32)
    return jnp.dot(weight, onehot, precision=lax.Precision.HIGHEST)


def shards(
    prompt, norm_gain, gate_master, up_master, down_master, group_choice, inner_choice, route_weight
):
    experts = GROUPS * EPG
    scale = norm_gain[None, :, None]
    gate_cast = (gate_master * scale).astype(jnp.bfloat16)
    up_cast = (up_master * scale).astype(jnp.bfloat16)
    down_cast = down_master.astype(jnp.bfloat16)
    rows = gate_master.shape[1] // lax.axis_size("tp")
    values = prompt.astype(jnp.float32)
    normed = (values * lax.rsqrt(jnp.mean(values * values, axis=1, keepdims=True) + 1e-06)).astype(
        jnp.bfloat16
    )
    chosen = group_choice[:, None] * EPG + inner_choice
    member = (chosen[:, :, None] == jnp.arange(experts, dtype=jnp.int32)[None, None, :]).astype(
        jnp.float32
    )
    weight = jnp.sum(member * route_weight[:, :, None], axis=1)
    stacked = jnp.stack([gate_cast, up_cast, down_cast])
    widened = lax.all_to_all(stacked, "tp", split_axis=2, concat_axis=3, tiled=True)
    moved = lax.all_to_all(flatten_rows(widened), "fs", split_axis=2, concat_axis=1, tiled=True)
    served = restore_rows(lax.all_gather(moved, "tp", axis=1, tiled=True), rows)
    gate_local, up_local, down_local = (served[0], served[1], served[2])
    column_weight = route_columns(weight, gate_local.shape[1], experts)
    scaled = activations(normed, gate_local, up_local, column_weight)
    summed = lax.psum_scatter(
        lax.dot_general(
            down_local, scaled, (((1,), (1,)), ((), ())), preferred_element_type=jnp.float32
        ),
        "fs",
        scatter_dimension=0,
        tiled=True,
    )
    mixed = (summed * FF ** (-0.5)).T.astype(jnp.bfloat16)
    return (gate_local, up_local, down_local, mixed)


def solution(mesh):
    in_specs = (
        P("tp", None),
        P("fs"),
        P(None, "fs", "tp"),
        P(None, "fs", "tp"),
        P(None, "fs", "tp"),
        P("tp"),
        P("tp", None),
        P("tp", None),
    )
    out_specs = (P(None, "fs"), P(None, "fs"), P(None, "fs"), P("tp", "fs"))
    return jax.shard_map(shards, mesh=mesh, in_specs=in_specs, out_specs=out_specs, check_vma=False)
```

profile of v0, /device:TPU:0, one launch (start us, length us, event | category | flops | bytes accessed | tf_op | source)
XLA Modules:
  0.0 666.3 jit_solution(537520447581431105)
XLA Ops:
  7.2 0.0 copy-start.4
  7.2 0.0 all-gather.2.cloned.1.call-start
  7.2 0.0 copy-start
  7.2 4.8 copy.90
  12.0 0.0 copy-done.4
  12.0 0.0 copy-done
  12.0 9.9 %fusion.6 = (bf16[1,32,256,128]{3,1,0,2:T(8,128)(2,1)S(1)}, bf16[1,32,256,128]{3,1,0,2:T(8,128)(2,1)S(1)}) fusion(f32[32,256,128]{2,1,0:T(8,128)S(1)} %copy-done, f32[256]{0:T(256)S(1)} %copy-done.4, f32[32,256,128]{2,1,0:T(8,128)} %param.11), kind=kLoop, calls=%fused_computation.16 | loop fusion | flops 4194304 | bytes 12583936 | tf_op jit(solution)/shard_map/stack | solution.py:56
  22.0 0.8 pad_maximum_fusion
  22.7 75.3 %all_to_all.36 = bf16[3,32,256,128]{3,1,0,2:T(8,128)(2,1)S(1)} all-to-all(bf16[3,32,256,128]{3,1,0,2:T(8,128)(2,1)S(1)} %pad_maximum_fusion), channel_id=1, replica_groups=mesh['fs'=8,'tp'=4] {'tp'}, dimensions={2} | all-to-all | bytes 12582912 | tf_op jit(solution)/shard_map/all_to_all | solution.py:57
  98.0 7.6 %copy.89 = bf16[3,32,4,64,128]{4,2,3,1,0:T(4,128)(2,1)} copy(bf16[3,32,4,64,128]{4,1,0,3,2:T(8,128)(2,1)S(1)} %bitcast.37) | data formatting | bytes 12582912 | tf_op jit(solution)/shard_map/all_to_all | solution.py:57
  105.6 10.1 %all_to_all.29 = bf16[3,32,64,512]{3,2,1,0:T(8,128)(2,1)} reshape(bf16[3,32,64,4,128]{4,3,2,1,0:T(4,128)(2,1)} %bitcast.38) | data formatting | bytes 12582912 | tf_op jit(solution)/shard_map/all_to_all | solution.py:57
  115.7 22.5 %copy.71 = bf16[3,64,32,512]{1,0,3,2:T(4,128)(2,1)} copy(bf16[3,64,32,512]{3,1,2,0:T(8,128)(2,1)} %bitcast.40) | data formatting | bytes 12582912 | tf_op jit(solution)/shard_map/reshape | solution.py:13
  138.3 15.3 %reshape.55 = bf16[8,2,196608]{2,1,0:T(2,128)(2,1)} reshape(bf16[16384,3,64]{2,1,0:T(4,128)(2,1)} %bitcast.34) | data formatting | bytes 12582912
  153.6 144.3 %all_to_all.37 = bf16[8,2,196608]{2,1,0:T(2,128)(2,1)} all-to-all(bf16[8,2,196608]{2,1,0:T(2,128)(2,1)} %reshape.55), channel_id=1, replica_groups=mesh['fs'=8,'tp'=4] {'fs'}, dimensions={0} | all-to-all | bytes 12582912 | tf_op jit(solution)/shard_map/all_to_all | solution.py:58
  297.8 14.2 %reshape.56 = bf16[16384,3,64]{2,1,0:T(4,128)(2,1)} reshape(bf16[8,2,196608]{2,1,0:T(2,128)(2,1)} %all_to_all.37) | data formatting | bytes 12582912
  312.0 23.2 %copy.73 = bf16[3,64,8,2048]{3,1,2,0:T(8,128)(2,1)} copy(bf16[3,64,8,2048]{1,0,3,2:T(4,128)(2,1)} %bitcast.35) | data formatting | bytes 12582912 | tf_op jit(solution)/shard_map/all_to_all | solution.py:58
  335.3 0.0 copy-start.5
  335.3 0.0 copy-start.3
  335.3 0.0 copy-start.2
  335.3 0.0 copy-start.1
  335.3 0.0 all-gather.2.cloned.1.call-update
  335.3 0.3 reduce-scatter.2.cloned.1.call-start
  335.6 0.3 copy-done.5
  336.0 0.0 copy-done.3
  336.0 0.0 copy-done.2
  336.0 0.5 copy-done.1
  336.5 0.3 fusion.4
  336.8 223.6 %all-gather.2.cloned.1.call-done = bf16[3,2048,2048]{2,1,0:T(8,128)(2,1)} async-done(((bf16[3,512,2048]{2,1,0:T(8,128)(2,1)}), bf16[3,2048,2048]{2,1,0:T(8,128)(2,1)}) %all-gather.2.cloned.1.call-update) | async-done | bytes 25165840 | tf_op jit(solution)/shard_map/all_gather | solution.py:59
  560.4 16.8 %fusion.20 = (bf16[1,8,4,64,2048]{4,3,1,2,0:T(8,128)(2,1)}, bf16[1,8,4,64,2048]{4,3,1,2,0:T(8,128)(2,1)}, bf16[1,8,4,64,2048]{4,3,1,2,0:T(8,128)(2,1)}) fusion(bf16[3,8,4,64,2048]{4,3,1,2,0:T(8,128)(2,1)} %bitcast.36), kind=kLoop, calls=%fused_computation.39 | loop fusion | bytes 50331648 | tf_op jit(solution)/shard_map/slice | solution.py:60
  577.2 8.4 %copy.67 = bf16[1,8,4,64,2048]{4,3,2,1,0:T(8,128)(2,1)} copy(bf16[1,8,4,64,2048]{4,3,1,2,0:T(8,128)(2,1)} %get-tuple-element.30) | data formatting | bytes 16777216 | tf_op jit(solution)/shard_map/slice | solution.py:60
  585.7 8.4 %copy.68 = bf16[1,8,4,64,2048]{4,3,2,1,0:T(8,128)(2,1)} copy(bf16[1,8,4,64,2048]{4,3,1,2,0:T(8,128)(2,1)} %get-tuple-element.29) | data formatting | bytes 16777216 | tf_op jit(solution)/shard_map/slice | solution.py:60
  594.1 8.4 %copy.69 = bf16[1,8,4,64,2048]{4,3,2,1,0:T(8,128)(2,1)} copy(bf16[1,8,4,64,2048]{4,3,1,2,0:T(8,128)(2,1)} %get-tuple-element.28) | data formatting | bytes 16777216 | tf_op jit(solution)/shard_map/slice | solution.py:60
  602.5 5.8 convolution_multiply_fusion.1
  608.3 1.4 convolution_multiply_fusion.2
  609.7 11.8 %fusion.14 = f32[2048,256]{1,0:T(8,128)} fusion(bf16[2048,2048]{1,0:T(8,128)(2,1)} %bitcast.45, f32[256,2048]{1,0:T(8,128)S(1)} %convolution_multiply_fusion.2, bf16[2048,2048]{1,0:T(8,128)(2,1)} %bitcast.43, bf16[256,2048]{1,0:T(8,128)(2,1)S(1)} %copy-done.1, f32[256]{0:T(256)S(1)} %add_rsqrt_fusion), kind=kOutput, calls=%fused_computation.23 | convolution fusion | flops 4298113024 | bytes 22021120 | tf_op jit(solution)/shard_map/dot_general | solution.py:64
  621.5 0.0 reduce-scatter.2.cloned.1.call-update
  621.5 36.2 %reduce-scatter.2.cloned.1.call-done = f32[256,256]{1,0:T(8,128)} async-done(((f32[2048,256]{1,0:T(8,128)}), f32[256,256]{1,0:T(8,128)}) %reduce-scatter.2.cloned.1.call-update) | async-done | bytes 262160 | tf_op jit(solution)/shard_map/reduce_scatter | solution.py:63
  657.7 1.0 fusion.11
  658.7 0.8 copy.70
  (5 shorter events, 0.0 us)
Async XLA Ops:
  7.2 4.8 copy-start.4
  7.2 553.3 %all-gather.2.cloned.1.call-start = ((), (), s32[]{:S(2)}) async-start(), calls=%async_computation.3 | async-start | bytes 31457280 | tf_op jit(solution)/shard_map/all_gather | solution.py:59
  7.2 4.8 copy-start
  335.3 0.7 copy-start.5
  335.3 0.7 copy-start.3
  335.3 0.7 copy-start.2
  335.3 1.3 copy-start.1
  335.3 322.4 %reduce-scatter.2.cloned.1.call-start = ((), (), s32[]{:S(2)}) async-start(), calls=%async_computation.4 | async-start | bytes 2359296 | tf_op jit(solution)/shard_map/reduce_scatter | solution.py:63
Sparse Core Ops, SparseCore 0:
  335.4 224.9 all-gather.1
  621.7 35.9 reduce-scatter.1
where the time goes:
time: 669 us; the launch traced here: 666 us
  waiting for transfers between devices  260 us (39%)
  blocking collectives  220 us (33%)
  local copies, waits for them, and re-layouts  142 us (21%)
  matrix products  19 us (3%)
  between operations  14.1 us (2%)
  other arithmetic  12 us (2%)
    all_gather x1, waiting for transfers between devices, shards(): served = restore_rows(lax.all_gather(moved, 'tp', axis=1, tiled=True), rows)  224 us
    all_to_all x1, blocking collectives, shards(): lax.all_to_all(flatten_rows(widened), 'fs', split_axis=2, concat_axis=1,...  144 us
    all_to_all x1, blocking collectives, shards(): lax.all_to_all(stacked, 'tp', split_axis=2, concat_axis=3, tiled=True)  75.3 us
    slice x4, local copies, waits for them, and re-layouts, shards(): gate_local, up_local, down_local = (served[0], served[1], served[2])  42.1 us
    reduce_scatter x1, waiting for transfers between devices, shards(): lax.psum_scatter(lax.dot_general(down_local, scaled, (((1,), (1,)), ((),...  36.2 us
    unnamed x16, local copies, waits for them, and re-layouts  36 us
    all_to_all x1, local copies, waits for them, and re-layouts, shards(): lax.all_to_all(flatten_rows(widened), 'fs', split_axis=2, concat_axis=1,...  23.2 us
    reshape x1, local copies, waits for them, and re-layouts, flatten_rows(): return piece.transpose(0, 2, 1, 3).reshape(count, rows, experts * hidden)  22.5 us
  transfers between devices with their start and end apart: 2, of which 2 were waited for; matrix products, arithmetic and copies ran while one was open for 0% of the time, Pallas kernels for 0%

commit v1 on v0

v1 whole, which is shorter than its diff:
```python
import functools

import jax
import jax.numpy as jnp
from jax import lax
from jax.experimental import pallas as pl
from jax.experimental.pallas import tpu as pltpu
from jax.sharding import PartitionSpec as P

FF = 512
GROUPS = 4
EPG = 8
LANES = 128


def flatten_rows(piece):
    count, experts, rows, hidden = piece.shape
    return piece.transpose(0, 2, 1, 3).reshape(count, rows, experts * hidden)


def restore_rows(gathered, rows):
    parts = lax.axis_size("tp")
    count, total, width = gathered.shape
    blocks = total // (parts * rows)
    ordered = gathered.reshape(count, parts, blocks, rows, width).transpose(0, 2, 1, 3, 4)
    return ordered.reshape(count, total, width)


def activations(normed, gate_local, up_local, column_weight):
    width = normed.shape[1]
    gate_act = jnp.dot(normed, gate_local, preferred_element_type=jnp.float32) * width ** (-0.5)
    up_act = jnp.dot(normed, up_local, preferred_element_type=jnp.float32) * width ** (-0.5)
    return (column_weight * jax.nn.silu(gate_act) * up_act).astype(jnp.bfloat16)


def route_columns(group_choice, inner_choice, route_weight, columns):
    first = lax.axis_index("fs") * columns
    owner = (first + jnp.arange(columns, dtype=jnp.int32)) // FF
    chosen = group_choice[:, None] * EPG + inner_choice
    picked = jnp.where(chosen[:, :, None] == owner[None, None, :], route_weight[:, :, None], 0.0)
    return jnp.sum(picked, axis=1)


def normalize(prompt):
    values = prompt.astype(jnp.float32)
    mean = jnp.mean(values * values, axis=1, keepdims=True)
    return (values * lax.rsqrt(mean + 1e-06)).astype(jnp.bfloat16)


def general_shards(
    prompt, norm_gain, gate_master, up_master, down_master, group_choice, inner_choice, route_weight
):
    scale = norm_gain[None, :, None]
    gate_cast = (gate_master * scale).astype(jnp.bfloat16)
    up_cast = (up_master * scale).astype(jnp.bfloat16)
    down_cast = down_master.astype(jnp.bfloat16)
    rows = gate_master.shape[1] // lax.axis_size("tp")
    normed = normalize(prompt)
    stacked = jnp.stack([gate_cast, up_cast, down_cast])
    widened = lax.all_to_all(stacked, "tp", split_axis=2, concat_axis=3, tiled=True)
    moved = lax.all_to_all(flatten_rows(widened), "fs", split_axis=2, concat_axis=1, tiled=True)
    served = restore_rows(lax.all_gather(moved, "tp", axis=1, tiled=True), rows)
    gate_local, up_local, down_local = (served[0], served[1], served[2])
    column_weight = route_columns(group_choice, inner_choice, route_weight, gate_local.shape[1])
    scaled = activations(normed, gate_local, up_local, column_weight)
    summed = lax.psum_scatter(
        lax.dot_general(
            down_local, scaled, (((1,), (1,)), ((), ())), preferred_element_type=jnp.float32
        ),
        "fs",
        scatter_dimension=0,
        tiled=True,
    )
    mixed = (summed * FF ** (-0.5)).T.astype(jnp.bfloat16)
    return (gate_local, up_local, down_local, mixed)


def cast_kernel(where_ref, gain_ref, gate_ref, up_ref, out_ref):
    gain = gain_ref[...]
    out_ref[0, 0] = (gate_ref[0] * gain).astype(jnp.bfloat16)
    out_ref[1, 0] = (up_ref[0] * gain).astype(jnp.bfloat16)


def cast_pair(block, gain, gate_master, up_master, held):
    _, rows, hidden = gate_master.shape
    source = pl.BlockSpec((1, rows, hidden), lambda e, where: (where[0] * held + e, 0, 0))
    return pl.pallas_call(
        cast_kernel,
        grid_spec=pltpu.PrefetchScalarGridSpec(
            num_scalar_prefetch=1,
            grid=(held,),
            in_specs=[pl.BlockSpec((rows, hidden), lambda e, where: (0, 0)), source, source],
            out_specs=pl.BlockSpec((2, 1, rows, hidden), lambda e, where: (0, e, 0, 0)),
        ),
        out_shape=jax.ShapeDtypeStruct((2, held, rows, hidden), jnp.bfloat16),
    )(block[None], gain, gate_master, up_master)


def lay_columns(parts, me, out_ref, pick, hidden):
    for step, part in enumerate(parts):
        column = pl.multiple_of((me ^ step) * hidden, LANES)
        out_ref[:, pl.ds(column, hidden)] = pick(part)


def lay_pair_kernel(where_ref, *refs, hidden, fresh):
    parts, outs = refs[:4], refs[4 if fresh else 6 :]
    for which, out_ref in enumerate(outs):
        lay_columns(parts, where_ref[1], out_ref, lambda part: part[which, 0], hidden)


def lay_pair(where, parts, outs, total):
    _, held, rows, hidden = parts[0].shape
    width = 4 * hidden
    fresh = outs is None
    part_spec = pl.BlockSpec((2, 1, rows, hidden), lambda e, where: (0, e, 0, 0))
    out_spec = pl.BlockSpec((rows, width), lambda e, where: (where[0], e))
    shape = jax.ShapeDtypeStruct((total, held * width), jnp.bfloat16)
    return pl.pallas_call(
        functools.partial(lay_pair_kernel, hidden=hidden, fresh=fresh),
        grid_spec=pltpu.PrefetchScalarGridSpec(
            num_scalar_prefetch=1,
            grid=(held,),
            in_specs=[part_spec] * 4 + [pl.BlockSpec(memory_space=pl.ANY)] * (0 if fresh else 2),
            out_specs=[out_spec, out_spec],
        ),
        out_shape=[shape, shape],
        input_output_aliases={} if fresh else {5: 0, 6: 1},
    )(where, *parts, *(() if fresh else outs))


def lay_down_kernel(where_ref, *refs, hidden, fresh):
    parts, scaled_ref = refs[:4], refs[4]
    out_ref, partial_ref = refs[5 if fresh else 6 :]
    lay_columns(parts, where_ref[1], out_ref, lambda part: part[0], hidden)
    product = lax.dot_general(
        scaled_ref[...], out_ref[...], (((1,), (1,)), ((), ())), preferred_element_type=jnp.float32
    )

    @pl.when(pl.program_id(0) == 0)
    def _():
        partial_ref[...] = product

    @pl.when(pl.program_id(0) > 0)
    def _():
        partial_ref[...] += product


def lay_down(where, parts, scaled, out, total):
    held, rows, hidden = parts[0].shape
    width = 4 * hidden
    tokens = scaled.shape[0]
    fresh = out is None
    part_spec = pl.BlockSpec((1, rows, hidden), lambda e, where: (e, 0, 0))
    return pl.pallas_call(
        functools.partial(lay_down_kernel, hidden=hidden, fresh=fresh),
        grid_spec=pltpu.PrefetchScalarGridSpec(
            num_scalar_prefetch=1,
            grid=(held,),
            in_specs=[part_spec] * 4
            + [pl.BlockSpec((tokens, width), lambda e, where: (0, e))]
            + [pl.BlockSpec(memory_space=pl.ANY)] * (0 if fresh else 1),
            out_specs=[
                pl.BlockSpec((rows, width), lambda e, where: (where[0], e)),
                pl.BlockSpec((tokens, rows), lambda e, where: (0, 0)),
            ],
        ),
        out_shape=[
            jax.ShapeDtypeStruct((total, held * width), jnp.bfloat16),
            jax.ShapeDtypeStruct((tokens, rows), jnp.float32),
        ],
        input_output_aliases={} if fresh else {6: 0},
    )(where, *parts, scaled, *(() if fresh else (out,)))


def fs_swap(value, step):
    return lax.ppermute(value, "fs", [(i, i ^ step) for i in range(lax.axis_size("fs"))])


def tp_swap(value, step):
    return lax.ppermute(value, "tp", [(i, i ^ step) for i in range(lax.axis_size("tp"))])


def plan(ways):
    pair = [(False, step) for step in range(ways)]
    far = [step for step in range(ways) if step >= ways // 2]
    near = [step for step in range(ways) if 0 < step < ways // 2]
    down = [(True, step) for step in far + near[1:] + near[:1] + [0]]
    return pair + down


def exchange_shards(
    prompt, norm_gain, gate_master, up_master, down_master, group_choice, inner_choice, route_weight
):
    ways = lax.axis_size("fs")
    mine, me = lax.axis_index("fs").astype(jnp.int32), lax.axis_index("tp").astype(jnp.int32)
    experts, rows, hidden = gate_master.shape
    held, total = experts // ways, rows * ways
    gain = jnp.broadcast_to(norm_gain[:, None], (rows, hidden))
    pieces = plan(ways)

    own, left, right, last = ({}, {}, {}, {})
    for index, (down, step) in enumerate(pieces):
        block = mine ^ step
        if down:
            cut = lax.dynamic_slice_in_dim(down_master, block * held, held, 0)
            piece = cut.astype(jnp.bfloat16)
        else:
            piece = cast_pair(block, gain, gate_master, up_master, held)
        if step:
            piece = fs_swap(piece, step)
        own[index] = piece
        left[index] = tp_swap(piece, 1)
        right[index] = tp_swap(piece, 2)
        last[index] = tp_swap(left[index], 2) if index % 2 == 0 else tp_swap(right[index], 1)

    def parts(index):
        return own[index], left[index], right[index], last[index]

    pair_out, down_out, scaled, sums = None, None, None, []
    for index, (down, step) in enumerate(pieces):
        where = jnp.stack([mine ^ step, me])
        if not down:
            pair_out = lay_pair(where, parts(index), pair_out, total)
            continue
        if scaled is None:
            gate_local, up_local = pair_out
            column_weight = route_columns(
                group_choice, inner_choice, route_weight, gate_local.shape[1]
            )
            scaled = activations(normalize(prompt), gate_local, up_local, column_weight)
        down_out, partial = lay_down(where, parts(index), scaled, down_out, total)
        if step:
            partial = fs_swap(partial, step)
        sums.append(partial)
    mixed = (sum(sums[1:], sums[0]) * FF ** (-0.5)).astype(jnp.bfloat16)
    return (*pair_out, down_out, mixed)


def solution(mesh):
    in_specs = (
        P("tp", None),
        P("fs"),
        P(None, "fs", "tp"),
        P(None, "fs", "tp"),
        P(None, "fs", "tp"),
        P("tp"),
        P("tp", None),
        P("tp", None),
    )
    out_specs = (P(None, "fs"), P(None, "fs"), P(None, "fs"), P("tp", "fs"))
    wrap = functools.partial(
        jax.shard_map, mesh=mesh, in_specs=in_specs, out_specs=out_specs, check_vma=False
    )
    ways, parts = mesh.shape["fs"], mesh.shape["tp"]
    whole_experts = ways & (ways - 1) == 0 and ways >= 4 and (GROUPS * EPG) % ways == 0
    if not (whole_experts and parts == 4 and FF % (parts * LANES) == 0):
        return wrap(general_shards)

    return wrap(exchange_shards)
```

time: 669 us -> 467 us (0.70)
  blocking collectives: 220 us -> 0 us
  local copies, waits for them, and re-layouts: 142 us -> 5.99 us
  Pallas kernels: 0 us -> 104 us
  starting transfers between devices: 0.3 us -> 102 us
  waiting for transfers between devices: 260 us -> 234 us
  between operations: 14.1 us -> 1.08 us
  matrix products: 19 us -> 9.79 us
    ppermute x0 -> x69, waiting for transfers between devices: none -> 234 us  [the longest x21 122 us: fs_swap(): lax.ppermute(value, 'fs', [(i, i ^ step) for i in range(lax.axis_size('fs...]
    all_gather x1 -> x0, waiting for transfers between devices: 224 us -> none  [shards(): served = restore_rows(lax.all_gather(moved, 'tp', axis=1, tiled=True), rows)]
    all_to_all x2 -> x0, blocking collectives: 220 us -> none  [the longest x1 144 us: shards(): lax.all_to_all(flatten_rows(widened), 'fs', split_axis=2, concat_axis=1,...]
    pallas_call x0 -> x24, Pallas kernels: none -> 104 us  [the longest x8 40.3 us: lay_down(): pl.pallas_call(functools.partial(lay_down_kernel, hidden=hidden, fresh=fr...]
    ppermute x0 -> x69, starting transfers between devices: none -> 102 us  [the longest x48 60.1 us: tp_swap(): lax.ppermute(value, 'tp', [(i, i ^ step) for i in range(lax.axis_size('tp...]
    slice x4 -> x0, local copies, waits for them, and re-layouts: 42.1 us -> none  [shards(): gate_local, up_local, down_local = (served[0], served[1], served[2])]
    all_to_all x3 -> x0, local copies, waits for them, and re-layouts: 40.9 us -> none  [the longest x1 23.2 us: shards(): lax.all_to_all(flatten_rows(widened), 'fs', split_axis=2, concat_axis=1,...]
    reduce_scatter x1 -> x0, waiting for transfers between devices: 36.2 us -> none  [shards(): lax.psum_scatter(lax.dot_general(down_local, scaled, (((1,), (1,)), ((),...]
  transfers between devices with their start and end apart: 2 -> 69, of which waited for: 2 -> 31; matrix products, arithmetic and copies ran while one was open for 0% -> 4% of each run, Pallas kernels for 0% -> 22%
where the time goes in v1:
time: 467 us; the launch traced here: 465 us
  waiting for transfers between devices  234 us (50%)
  Pallas kernels  104 us (22%)
  starting transfers between devices  102 us (22%)
  matrix products  9.79 us (2%)
  other arithmetic  7.55 us (2%)
  local copies, waits for them, and re-layouts  5.99 us (1%)
    ppermute x21, waiting for transfers between devices, fs_swap(): lax.ppermute(value, 'fs', [(i, i ^ step) for i in range(lax.axis_size('fs...  122 us
    ppermute x48, waiting for transfers between devices, tp_swap(): lax.ppermute(value, 'tp', [(i, i ^ step) for i in range(lax.axis_size('tp...  113 us
    ppermute x48, starting transfers between devices, tp_swap(): lax.ppermute(value, 'tp', [(i, i ^ step) for i in range(lax.axis_size('tp...  60.1 us
    ppermute x21, starting transfers between devices, fs_swap(): lax.ppermute(value, 'fs', [(i, i ^ step) for i in range(lax.axis_size('fs...  41.6 us
    pallas_call x8, Pallas kernels, lay_down(): pl.pallas_call(functools.partial(lay_down_kernel, hidden=hidden, fresh=fr...  40.3 us
    pallas_call x8, Pallas kernels, lay_pair(): pl.pallas_call(functools.partial(lay_pair_kernel, hidden=hidden, fresh=fr...  37 us
    pallas_call x8, Pallas kernels, cast_pair(): pl.pallas_call(cast_kernel, grid_spec=pltpu.PrefetchScalarGridSpec(num_sc...  27.2 us
  transfers between devices with their start and end apart: 69, of which 31 were waited for; matrix products, arithmetic and copies ran while one was open for 4% of the time, Pallas kernels for 22%

profile of v1, /device:TPU:0, one launch (start us, length us, event | category | flops | bytes accessed | tf_op | source)
XLA Modules:
  0.0 465.0 jit_solution(9981331111937807181)
XLA Ops:
  0.7 3.3 dynamic-slice_convert_fusion
  4.0 4.1 collective-permute-start.58
  8.1 3.1 collective-permute-start.50
  11.7 26.1 %collective-permute-done.58.refs_0_ = bf16[4,256,128]{2,1,0:T(8,128)(2,1)} collective-permute-done((bf16[4,256,128]{2,1,0:T(8,128)(2,1)S(1)}, bf16[4,256,128]{2,1,0:T(8,128)(2,1)}, u32[]{:S(2)}, u32[]{:S(2)}) %collective-permute-start.58) | collective-permute-done | bytes 262176 | tf_op jit(solution)/shard_map/ppermute | solution.py:176
  38.6 3.4 shard_map.118.refs_0_
  41.9 3.4 shard_map.117
  45.3 3.5 shard_map.116
  52.3 2.2 collective-permute-start.20
  54.7 3.4 shard_map.115
  58.1 3.4 shard_map.114
  61.5 3.4 shard_map.113
  64.8 3.4 shard_map.112
  68.2 4.0 collective-permute-start.12
  72.2 2.1 collective-permute-start.4
  74.4 3.5 shard_map.111
  79.2 7.4 %collective-permute-done.16.refs_0_ = bf16[2,4,256,128]{3,2,1,0:T(8,128)(2,1)} collective-permute-done((bf16[2,4,256,128]{3,2,1,0:T(8,128)(2,1)}, bf16[2,4,256,128]{3,2,1,0:T(8,128)(2,1)}, u32[]{:S(2)}, u32[]{:S(2)}) %collective-permute-start.16) | collective-permute-done | bytes 524320 | tf_op jit(solution)/shard_map/ppermute | solution.py:176
  88.1 42.2 %collective-permute-done.12.refs_0_ = bf16[2,4,256,128]{3,2,1,0:T(8,128)(2,1)} collective-permute-done((bf16[2,4,256,128]{3,2,1,0:T(8,128)(2,1)}, bf16[2,4,256,128]{3,2,1,0:T(8,128)(2,1)}, u32[]{:S(2)}, u32[]{:S(2)}) %collective-permute-start.12) | collective-permute-done | bytes 524320 | tf_op jit(solution)/shard_map/ppermute | solution.py:176
  131.8 8.6 %collective-permute-done.8.refs_0_ = bf16[2,4,256,128]{3,2,1,0:T(8,128)(2,1)} collective-permute-done((bf16[2,4,256,128]{3,2,1,0:T(8,128)(2,1)}, bf16[2,4,256,128]{3,2,1,0:T(8,128)(2,1)}, u32[]{:S(2)}, u32[]{:S(2)}) %collective-permute-start.8) | collective-permute-done | bytes 524320 | tf_op jit(solution)/shard_map/ppermute | solution.py:176
  146.0 3.7 collective-permute-done.56.refs_2_
  151.8 4.8 %collective-permute-done.51.refs_1_ = bf16[4,256,128]{2,1,0:T(8,128)(2,1)S(1)} collective-permute-done((bf16[4,256,128]{2,1,0:T(8,128)(2,1)}, bf16[4,256,128]{2,1,0:T(8,128)(2,1)S(1)}, u32[]{:S(2)}, u32[]{:S(2)}) %collective-permute-start.51) | collective-permute-done | bytes 262176 | tf_op jit(solution)/shard_map/ppermute | solution.py:180
  158.1 19.7 %collective-permute-done.52.refs_2_ = bf16[4,256,128]{2,1,0:T(8,128)(2,1)S(1)} collective-permute-done((bf16[4,256,128]{2,1,0:T(8,128)(2,1)}, bf16[4,256,128]{2,1,0:T(8,128)(2,1)S(1)}, u32[]{:S(2)}, u32[]{:S(2)}) %collective-permute-start.52) | collective-permute-done | bytes 262176 | tf_op jit(solution)/shard_map/ppermute | solution.py:180
  179.4 4.1 collective-permute-done.48.refs_2_
  188.7 4.1 collective-permute-done.21.refs_1_
  194.3 4.1 collective-permute-done.22.refs_2_
  199.9 9.7 %collective-permute-done.18.refs_2_ = bf16[2,4,256,128]{3,2,1,0:T(8,128)(2,1)} collective-permute-done((bf16[2,4,256,128]{3,2,1,0:T(8,128)(2,1)}, bf16[2,4,256,128]{3,2,1,0:T(8,128)(2,1)}, u32[]{:S(2)}, u32[]{:S(2)}) %collective-permute-start.18) | collective-permute-done | bytes 524320 | tf_op jit(solution)/shard_map/ppermute | solution.py:180
  216.8 4.0 collective-permute-done.14.refs_2_
  222.3 9.8 %collective-permute-done.10.refs_2_ = bf16[2,4,256,128]{3,2,1,0:T(8,128)(2,1)} collective-permute-done((bf16[2,4,256,128]{3,2,1,0:T(8,128)(2,1)}, bf16[2,4,256,128]{3,2,1,0:T(8,128)(2,1)}, u32[]{:S(2)}, u32[]{:S(2)}) %collective-permute-start.10) | collective-permute-done | bytes 524320 | tf_op jit(solution)/shard_map/ppermute | solution.py:180
  234.1 3.6 collective-permute-done.5.refs_1_
  240.2 3.0 collective-permute-done.6.refs_2_
  244.7 9.8 %collective-permute-done.2.refs_2_ = bf16[2,4,256,128]{3,2,1,0:T(8,128)(2,1)} collective-permute-done((bf16[2,4,256,128]{3,2,1,0:T(8,128)(2,1)S(1)}, bf16[2,4,256,128]{3,2,1,0:T(8,128)(2,1)}, u32[]{:S(2)}, u32[]{:S(2)}) %collective-permute-start.2) | collective-permute-done | bytes 524320 | tf_op jit(solution)/shard_map/ppermute | solution.py:180
  257.6 2.6 collective-permute-done.27.refs_3_
  261.7 4.1 collective-permute-done.23.refs_3_
  268.4 3.0 collective-permute-done.19.refs_3_
  272.9 4.1 collective-permute-done.15.refs_3_
  278.5 4.1 collective-permute-done.11.refs_3_
  284.2 4.1 collective-permute-done.7.refs_3_
  289.8 4.1 collective-permute-done.3.refs_3_
  296.0 4.6 shard_map.119
  300.7 4.6 shard_map.120
  305.3 4.6 shard_map.121
  309.9 4.6 shard_map.122
  314.5 4.6 shard_map.123
  319.1 4.6 shard_map.124
  323.8 4.6 shard_map.125
  328.4 4.6 shard_map.126
  338.7 5.9 %convolution_multiply_fusion.1 = f32[256,2048]{1,0:T(8,128)S(1)} fusion(bf16[2048,2048]{1,0:T(8,128)(2,1)} %get-tuple-element.32, bf16[256,2048]{1,0:T(8,128)(2,1)S(1)} %copy-done.2, f32[256]{0:T(256)S(1)} %add_rsqrt_fusion), kind=kOutput, calls=%fused_computation.3 | convolution fusion | flops 2149580800 | bytes 11535360 | tf_op jit(solution)/shard_map/dot_general | solution.py:31
  350.2 3.6 collective-permute-done.45.refs_3_
  355.3 3.9 fusion.1.refs_4_
  359.2 5.0 %shard_map.127 = (bf16[2048,2048]{1,0:T(8,128)(2,1)}, f32[256,256]{1,0:T(8,128)}) custom-call(s32[2]{0:T(128)} %pad_add_fusion.3.where_ref, bf16[4,256,128]{2,1,0:T(8,128)(2,1)} %collective-permute-done.58.refs_0_, bf16[4,256,128]{2,1,0:T(8,128)(2,1)} %collective-permute-done.59.refs_1_, bf16[4,256,128]{2,1,0:T(8,128)(2,1)} %copy-done.16, ...), custom_call_target="tpu_custom_call" | custom-call | tf_op jit(solution)/shard_map/pallas_call | solution.py:154
  364.1 5.0 %shard_map.128 = (bf16[2048,2048]{1,0:T(8,128)(2,1)}, f32[256,256]{1,0:T(8,128)}) custom-call(s32[2]{0:T(128)} %pad_add_fusion.2.where_ref, bf16[4,256,128]{2,1,0:T(8,128)(2,1)} %collective-permute-done.54.refs_0_, bf16[4,256,128]{2,1,0:T(8,128)(2,1)} %copy-done.20, bf16[4,256,128]{2,1,0:T(8,128)(2,1)} %copy-done.19, ...), custom_call_target="tpu_custom_call", output_to_operand_aliasing={{0}: (6, {})} | custom-call | tf_op jit(solution)/shard_map/pallas_call | solution.py:154
  369.1 5.2 %shard_map.129 = (bf16[2048,2048]{1,0:T(8,128)(2,1)}, f32[256,256]{1,0:T(8,128)}) custom-call(s32[2]{0:T(128)} %pad_add_fusion.1.where_ref, bf16[4,256,128]{2,1,0:T(8,128)(2,1)} %copy-done.18, bf16[4,256,128]{2,1,0:T(8,128)(2,1)} %copy-done.21, bf16[4,256,128]{2,1,0:T(8,128)(2,1)} %copy-done.23, ...), custom_call_target="tpu_custom_call", output_to_operand_aliasing={{0}: (6, {})} | custom-call | tf_op jit(solution)/shard_map/pallas_call | solution.py:154
  374.3 5.0 %shard_map.130 = (bf16[2048,2048]{1,0:T(8,128)(2,1)}, f32[256,256]{1,0:T(8,128)}) custom-call(s32[2]{0:T(128)} %pad_add_fusion.where_ref, bf16[4,256,128]{2,1,0:T(8,128)(2,1)} %collective-permute-done.46.refs_0_, bf16[4,256,128]{2,1,0:T(8,128)(2,1)} %collective-permute-done.47.refs_1_, ...), custom_call_target="tpu_custom_call", output_to_operand_aliasing={{0}: (6, {})} | custom-call | tf_op jit(solution)/shard_map/pallas_call | solution.py:154
  379.3 5.0 %shard_map.131 = (bf16[2048,2048]{1,0:T(8,128)(2,1)}, f32[256,256]{1,0:T(8,128)}) custom-call(s32[2]{0:T(128)} %pad_add_fusion.5.where_ref, bf16[4,256,128]{2,1,0:T(8,128)(2,1)} %collective-permute-done.42.refs_0_, bf16[4,256,128]{2,1,0:T(8,128)(2,1)} %collective-permute-done.43.refs_1_, ...), custom_call_target="tpu_custom_call", output_to_operand_aliasing={{0}: (6, {})} | custom-call | tf_op jit(solution)/shard_map/pallas_call | solution.py:154
  386.4 5.0 %shard_map.132 = (bf16[2048,2048]{1,0:T(8,128)(2,1)}, f32[256,256]{1,0:T(8,128)}) custom-call(s32[2]{0:T(128)} %pad_add_fusion.4.where_ref, bf16[4,256,128]{2,1,0:T(8,128)(2,1)} %collective-permute-done.38.refs_0_, bf16[4,256,128]{2,1,0:T(8,128)(2,1)} %collective-permute-done.39.refs_1_, ...), custom_call_target="tpu_custom_call", output_to_operand_aliasing={{0}: (6, {})} | custom-call | tf_op jit(solution)/shard_map/pallas_call | solution.py:154
  391.5 5.1 %shard_map.133 = (bf16[2048,2048]{1,0:T(8,128)(2,1)}, f32[256,256]{1,0:T(8,128)}) custom-call(s32[2]{0:T(128)} %pad_add_fusion.6.where_ref, bf16[4,256,128]{2,1,0:T(8,128)(2,1)} %collective-permute-done.34.refs_0_, bf16[4,256,128]{2,1,0:T(8,128)(2,1)} %collective-permute-done.35.refs_1_, ...), custom_call_target="tpu_custom_call", output_to_operand_aliasing={{0}: (6, {})} | custom-call | tf_op jit(solution)/shard_map/pallas_call | solution.py:154
  396.6 17.2 %collective-permute-start.67 = (f32[256,256]{1,0:T(8,128)S(1)}, f32[256,256]{1,0:T(8,128)S(1)}, u32[]{:S(2)}, u32[]{:S(2)}) collective-permute-start(f32[256,256]{1,0:T(8,128)S(1)} %copy-done.34), channel_id=1, source_target_pairs={{0,12},{4,8},{8,4},{12,0},{16,28},{20,24},{24,20},{28,16},{1,13},{... | collective-permute-start | bytes 786440 | tf_op jit(solution)/shard_map/ppermute | solution.py:176
  413.9 2.2 collective-permute-start.65
  418.4 2.1 collective-permute-done.67
  420.5 2.2 collective-permute-start.62
  422.8 5.0 %shard_map.134 = (bf16[2048,2048]{1,0:T(8,128)(2,1)}, f32[256,256]{1,0:T(8,128)}) custom-call(s32[2]{0:T(128)} %pad_add_fusion.7.where_ref, bf16[4,256,128]{2,1,0:T(8,128)(2,1)} %copy-done.3, bf16[4,256,128]{2,1,0:T(8,128)(2,1)} %copy-done.24, bf16[4,256,128]{2,1,0:T(8,128)(2,1)} %collective-permute-done.32.refs_2_, ...), custom_call_target="tpu_custom_call", output_to_operand_aliasing={{0}: (6, {})} | custom-call | tf_op jit(solution)/shard_map/pallas_call | solution.py:154
  427.8 5.8 %collective-permute-done.65 = f32[256,256]{1,0:T(8,128)S(1)} collective-permute-done((f32[256,256]{1,0:T(8,128)S(1)}, f32[256,256]{1,0:T(8,128)S(1)}, u32[]{:S(2)}, u32[]{:S(2)}) %collective-permute-start.65) | collective-permute-done | bytes 262176 | tf_op jit(solution)/shard_map/ppermute | solution.py:176
  433.5 6.8 %collective-permute-done.64 = f32[256,256]{1,0:T(8,128)S(1)} collective-permute-done((f32[256,256]{1,0:T(8,128)S(1)}, f32[256,256]{1,0:T(8,128)S(1)}, u32[]{:S(2)}, u32[]{:S(2)}) %collective-permute-start.64) | collective-permute-done | bytes 262176 | tf_op jit(solution)/shard_map/ppermute | solution.py:176
  440.4 17.2 %collective-permute-done.63 = f32[256,256]{1,0:T(8,128)S(1)} collective-permute-done((f32[256,256]{1,0:T(8,128)S(1)}, f32[256,256]{1,0:T(8,128)S(1)}, u32[]{:S(2)}, u32[]{:S(2)}) %collective-permute-start.63) | collective-permute-done | bytes 262176 | tf_op jit(solution)/shard_map/ppermute | solution.py:176
  457.6 5.7 %collective-permute-done.62 = f32[256,256]{1,0:T(8,128)S(1)} collective-permute-done((f32[256,256]{1,0:T(8,128)S(1)}, f32[256,256]{1,0:T(8,128)S(1)}, u32[]{:S(2)}, u32[]{:S(2)}) %collective-permute-start.62) | collective-permute-done | bytes 262176 | tf_op jit(solution)/shard_map/ppermute | solution.py:176
  (187 shorter events, 77.2 us)
Async XLA Ops:
  4.0 33.8 %collective-permute-start.58 = (bf16[4,256,128]{2,1,0:T(8,128)(2,1)S(1)}, bf16[4,256,128]{2,1,0:T(8,128)(2,1)}, u32[]{:S(2)}, u32[]{:S(2)}) collective-permute-start(bf16[4,256,128]{2,1,0:T(8,128)(2,1)S(1)} %get-tuple-element.68), channel_id=1, source_target_pairs={{0,16},{4,20},{8,24},{12,28},{16,0},{20,4},{24,8},{28,12},{1,17},{... | collective-permute-start | bytes 786440 | tf_op jit(solution)/shard_map/ppermute | solution.py:176
  8.1 40.7 %collective-permute-start.54 = (bf16[4,256,128]{2,1,0:T(8,128)(2,1)S(1)}, bf16[4,256,128]{2,1,0:T(8,128)(2,1)}, u32[]{:S(2)}, u32[]{:S(2)}) collective-permute-start(bf16[4,256,128]{2,1,0:T(8,128)(2,1)S(1)} %get-tuple-element.75), channel_id=1, source_target_pairs={{0,20},{4,16},{8,28},{12,24},{16,4},{20,0},{24,12},{28,8},{1,21},{... | collective-permute-start | bytes 786440 | tf_op jit(solution)/shard_map/ppermute | solution.py:176
  8.1 42.6 %collective-permute-start.50 = (bf16[4,256,128]{2,1,0:T(8,128)(2,1)S(1)}, bf16[4,256,128]{2,1,0:T(8,128)(2,1)S(1)}, u32[]{:S(2)}, u32[]{:S(2)}) collective-permute-start(bf16[4,256,128]{2,1,0:T(8,128)(2,1)S(1)} %get-tuple-element.69), channel_id=1, source_target_pairs={{0,24},{4,28},{8,16},{12,20},{16,8},{20,12},{24,0},{28,4},{1,25},{... | collective-permute-start | bytes 786440 | tf_op jit(solution)/shard_map/ppermute | solution.py:176
  11.2 41.0 %collective-permute-start.46 = (bf16[4,256,128]{2,1,0:T(8,128)(2,1)S(1)}, bf16[4,256,128]{2,1,0:T(8,128)(2,1)}, u32[]{:S(2)}, u32[]{:S(2)}) collective-permute-start(bf16[4,256,128]{2,1,0:T(8,128)(2,1)S(1)} %get-tuple-element.70), channel_id=1, source_target_pairs={{0,28},{4,24},{8,20},{12,16},{16,12},{20,8},{24,4},{28,0},{1,29},{... | collective-permute-start | bytes 786440 | tf_op jit(solution)/shard_map/ppermute | solution.py:176
  11.7 40.6 %collective-permute-start.42 = (bf16[4,256,128]{2,1,0:T(8,128)(2,1)S(1)}, bf16[4,256,128]{2,1,0:T(8,128)(2,1)}, u32[]{:S(2)}, u32[]{:S(2)}) collective-permute-start(bf16[4,256,128]{2,1,0:T(8,128)(2,1)S(1)} %get-tuple-element.71), channel_id=1, source_target_pairs={{0,8},{4,12},{8,0},{12,4},{16,24},{20,28},{24,16},{28,20},{1,9},{5... | collective-permute-start | bytes 786440 | tf_op jit(solution)/shard_map/ppermute | solution.py:176
  37.8 16.7 %collective-permute-start.38 = (bf16[4,256,128]{2,1,0:T(8,128)(2,1)}, bf16[4,256,128]{2,1,0:T(8,128)(2,1)}, u32[]{:S(2)}, u32[]{:S(2)}) collective-permute-start(bf16[4,256,128]{2,1,0:T(8,128)(2,1)} %get-tuple-element.72), channel_id=1, source_target_pairs={{0,12},{4,8},{8,4},{12,0},{16,28},{20,24},{24,20},{28,16},{1,13},{... | collective-permute-start | bytes 786440 | tf_op jit(solution)/shard_map/ppermute | solution.py:176
  48.8 19.4 %collective-permute-start.28 = (bf16[2,4,256,128]{3,2,1,0:T(8,128)(2,1)S(1)}, bf16[2,4,256,128]{3,2,1,0:T(8,128)(2,1)S(1)}, u32[]{:S(2)}, u32[]{:S(2)}) collective-permute-start(bf16[2,4,256,128]{3,2,1,0:T(8,128)(2,1)S(1)} %copy-done.1), channel_id=1, source_target_pairs={{0,1},{1,0},{2,3},{3,2},{4,5},{5,4},{6,7},{7,6},{8,9},{9,8},{10,11... | collective-permute-start | bytes 1572872 | tf_op jit(solution)/shard_map/ppermute | solution.py:180
  50.7 21.6 %collective-permute-start.29 = (bf16[2,4,256,128]{3,2,1,0:T(8,128)(2,1)S(1)}, bf16[2,4,256,128]{3,2,1,0:T(8,128)(2,1)S(1)}, u32[]{:S(2)}, u32[]{:S(2)}) collective-permute-start(bf16[2,4,256,128]{3,2,1,0:T(8,128)(2,1)S(1)} %copy-done.1), channel_id=1, source_target_pairs={{0,2},{1,3},{2,0},{3,1},{4,6},{5,7},{6,4},{7,5},{8,10},{9,11},{10,... | collective-permute-start | bytes 1572872 | tf_op jit(solution)/shard_map/ppermute | solution.py:180
  52.2 20.0 %collective-permute-start.24 = (bf16[2,4,256,128]{3,2,1,0:T(8,128)(2,1)S(1)}, bf16[2,4,256,128]{3,2,1,0:T(8,128)(2,1)S(1)}, u32[]{:S(2)}, u32[]{:S(2)}) collective-permute-start(bf16[2,4,256,128]{3,2,1,0:T(8,128)(2,1)S(1)} %copy-done.15), channel_id=1, source_target_pairs={{0,4},{4,0},{8,12},{12,8},{16,20},{20,16},{24,28},{28,24},{1,5},{5... | collective-permute-start | bytes 1572872 | tf_op jit(solution)/shard_map/ppermute | solution.py:176
  52.3 25.6 %collective-permute-start.20 = (bf16[2,4,256,128]{3,2,1,0:T(8,128)(2,1)}, bf16[2,4,256,128]{3,2,1,0:T(8,128)(2,1)S(1)}, u32[]{:S(2)}, u32[]{:S(2)}) collective-permute-start(bf16[2,4,256,128]{3,2,1,0:T(8,128)(2,1)} %shard_map.116), channel_id=1, source_target_pairs={{0,8},{4,12},{8,0},{12,4},{16,24},{20,28},{24,16},{28,20},{1,9},{5... | collective-permute-start | bytes 1572872 | tf_op jit(solution)/shard_map/ppermute | solution.py:176
  58.1 28.6 %collective-permute-start.16 = (bf16[2,4,256,128]{3,2,1,0:T(8,128)(2,1)}, bf16[2,4,256,128]{3,2,1,0:T(8,128)(2,1)}, u32[]{:S(2)}, u32[]{:S(2)}) collective-permute-start(bf16[2,4,256,128]{3,2,1,0:T(8,128)(2,1)} %shard_map.115), channel_id=1, source_target_pairs={{0,12},{4,8},{8,4},{12,0},{16,28},{20,24},{24,20},{28,16},{1,13},{... | collective-permute-start | bytes 1572872 | tf_op jit(solution)/shard_map/ppermute | solution.py:176
  68.2 62.0 %collective-permute-start.12 = (bf16[2,4,256,128]{3,2,1,0:T(8,128)(2,1)}, bf16[2,4,256,128]{3,2,1,0:T(8,128)(2,1)}, u32[]{:S(2)}, u32[]{:S(2)}) collective-permute-start(bf16[2,4,256,128]{3,2,1,0:T(8,128)(2,1)} %shard_map.114), channel_id=1, source_target_pairs={{0,16},{4,20},{8,24},{12,28},{16,0},{20,4},{24,8},{28,12},{1,17},{... | collective-permute-start | bytes 1572872 | tf_op jit(solution)/shard_map/ppermute | solution.py:176
  72.2 68.2 %collective-permute-start.8 = (bf16[2,4,256,128]{3,2,1,0:T(8,128)(2,1)}, bf16[2,4,256,128]{3,2,1,0:T(8,128)(2,1)}, u32[]{:S(2)}, u32[]{:S(2)}) collective-permute-start(bf16[2,4,256,128]{3,2,1,0:T(8,128)(2,1)} %shard_map.113), channel_id=1, source_target_pairs={{0,20},{4,16},{8,28},{12,24},{16,4},{20,0},{24,12},{28,8},{1,21},{... | collective-permute-start | bytes 1572872 | tf_op jit(solution)/shard_map/ppermute | solution.py:176
  72.2 69.7 %collective-permute-start.4 = (bf16[2,4,256,128]{3,2,1,0:T(8,128)(2,1)}, bf16[2,4,256,128]{3,2,1,0:T(8,128)(2,1)}, u32[]{:S(2)}, u32[]{:S(2)}) collective-permute-start(bf16[2,4,256,128]{3,2,1,0:T(8,128)(2,1)} %shard_map.112), channel_id=1, source_target_pairs={{0,24},{4,28},{8,16},{12,20},{16,8},{20,12},{24,0},{28,4},{1,25},{... | collective-permute-start | bytes 1572872 | tf_op jit(solution)/shard_map/ppermute | solution.py:176
  77.9 65.5 %collective-permute-start = (bf16[2,4,256,128]{3,2,1,0:T(8,128)(2,1)}, bf16[2,4,256,128]{3,2,1,0:T(8,128)(2,1)S(1)}, u32[]{:S(2)}, u32[]{:S(2)}) collective-permute-start(bf16[2,4,256,128]{3,2,1,0:T(8,128)(2,1)} %shard_map.111), channel_id=1, source_target_pairs={{0,28},{4,24},{8,20},{12,16},{16,12},{20,8},{24,4},{28,0},{1,29},{... | collective-permute-start | bytes 1572872 | tf_op jit(solution)/shard_map/ppermute | solution.py:176
  86.6 57.3 %collective-permute-start.59 = (bf16[4,256,128]{2,1,0:T(8,128)(2,1)}, bf16[4,256,128]{2,1,0:T(8,128)(2,1)}, u32[]{:S(2)}, u32[]{:S(2)}) collective-permute-start(bf16[4,256,128]{2,1,0:T(8,128)(2,1)} %collective-permute-done.58.refs_0_), channel_id=1, source_target_pairs={{0,1},{1,0},{2,3},{3,2},{4,5},{5,4},{6,7},{7,6},{8,9},{9,8},{10,11... | collective-permute-start | bytes 786440 | tf_op jit(solution)/shard_map/ppermute | solution.py:180
  130.3 15.2 %collective-permute-start.60 = (bf16[4,256,128]{2,1,0:T(8,128)(2,1)}, bf16[4,256,128]{2,1,0:T(8,128)(2,1)S(1)}, u32[]{:S(2)}, u32[]{:S(2)}) collective-permute-start(bf16[4,256,128]{2,1,0:T(8,128)(2,1)} %collective-permute-done.58.refs_0_), channel_id=1, source_target_pairs={{0,2},{1,3},{2,0},{3,1},{4,6},{5,7},{6,4},{7,5},{8,10},{9,11},{10,... | collective-permute-start | bytes 786440 | tf_op jit(solution)/shard_map/ppermute | solution.py:180
  143.4 41.6 %collective-permute-start.30 = (bf16[2,4,256,128]{3,2,1,0:T(8,128)(2,1)S(1)}, bf16[2,4,256,128]{3,2,1,0:T(8,128)(2,1)S(1)}, u32[]{:S(2)}, u32[]{:S(2)}) collective-permute-start(bf16[2,4,256,128]{3,2,1,0:T(8,128)(2,1)S(1)} %collective-permute-done.28.refs_1_), channel_id=1, source_target_pairs={{0,2},{1,3},{2,0},{3,1},{4,6},{5,7},{6,4},{7,5},{8,10},{9,11},{10,... | collective-permute-start | bytes 1572872 | tf_op jit(solution)/shard_map/ppermute | solution.py:180
  144.0 41.5 %collective-permute-start.26 = (bf16[2,4,256,128]{3,2,1,0:T(8,128)(2,1)S(1)}, bf16[2,4,256,128]{3,2,1,0:T(8,128)(2,1)S(1)}, u32[]{:S(2)}, u32[]{:S(2)}) collective-permute-start(bf16[2,4,256,128]{3,2,1,0:T(8,128)(2,1)S(1)} %copy-done.8), channel_id=1, source_target_pairs={{0,2},{1,3},{2,0},{3,1},{4,6},{5,7},{6,4},{7,5},{8,10},{9,11},{10,... | collective-permute-start | bytes 1572872 | tf_op jit(solution)/shard_map/ppermute | solution.py:180
  149.8 28.1 %collective-permute-start.52 = (bf16[4,256,128]{2,1,0:T(8,128)(2,1)}, bf16[4,256,128]{2,1,0:T(8,128)(2,1)S(1)}, u32[]{:S(2)}, u32[]{:S(2)}) collective-permute-start(bf16[4,256,128]{2,1,0:T(8,128)(2,1)} %copy-done.18), channel_id=1, source_target_pairs={{0,2},{1,3},{2,0},{3,1},{4,6},{5,7},{6,4},{7,5},{8,10},{9,11},{10,... | collective-permute-start | bytes 786440 | tf_op jit(solution)/shard_map/ppermute | solution.py:180
  151.3 32.2 %collective-permute-start.48 = (bf16[4,256,128]{2,1,0:T(8,128)(2,1)}, bf16[4,256,128]{2,1,0:T(8,128)(2,1)S(1)}, u32[]{:S(2)}, u32[]{:S(2)}) collective-permute-start(bf16[4,256,128]{2,1,0:T(8,128)(2,1)} %collective-permute-done.46.refs_0_), channel_id=1, source_target_pairs={{0,2},{1,3},{2,0},{3,1},{4,6},{5,7},{6,4},{7,5},{8,10},{9,11},{10,... | collective-permute-start | bytes 786440 | tf_op jit(solution)/shard_map/ppermute | solution.py:180
  156.6 31.5 %collective-permute-start.25 = (bf16[2,4,256,128]{3,2,1,0:T(8,128)(2,1)S(1)}, bf16[2,4,256,128]{3,2,1,0:T(8,128)(2,1)}, u32[]{:S(2)}, u32[]{:S(2)}) collective-permute-start(bf16[2,4,256,128]{3,2,1,0:T(8,128)(2,1)S(1)} %copy-done.8), channel_id=1, source_target_pairs={{0,1},{1,0},{2,3},{3,2},{4,5},{5,4},{6,7},{7,6},{8,9},{9,8},{10,11... | collective-permute-start | bytes 1572872 | tf_op jit(solution)/shard_map/ppermute | solution.py:180
  177.9 14.9 %collective-permute-start.21 = (bf16[2,4,256,128]{3,2,1,0:T(8,128)(2,1)S(1)}, bf16[2,4,256,128]{3,2,1,0:T(8,128)(2,1)}, u32[]{:S(2)}, u32[]{:S(2)}) collective-permute-start(bf16[2,4,256,128]{3,2,1,0:T(8,128)(2,1)S(1)} %collective-permute-done.20.refs_0_), channel_id=1, source_target_pairs={{0,1},{1,0},{2,3},{3,2},{4,5},{5,4},{6,7},{7,6},{8,9},{9,8},{10,11... | collective-permute-start | bytes 1572872 | tf_op jit(solution)/shard_map/ppermute | solution.py:180
  183.5 14.9 %collective-permute-start.22 = (bf16[2,4,256,128]{3,2,1,0:T(8,128)(2,1)S(1)}, bf16[2,4,256,128]{3,2,1,0:T(8,128)(2,1)}, u32[]{:S(2)}, u32[]{:S(2)}) collective-permute-start(bf16[2,4,256,128]{3,2,1,0:T(8,128)(2,1)S(1)} %collective-permute-done.20.refs_0_), channel_id=1, source_target_pairs={{0,2},{1,3},{2,0},{3,1},{4,6},{5,7},{6,4},{7,5},{8,10},{9,11},{10,... | collective-permute-start | bytes 1572872 | tf_op jit(solution)/shard_map/ppermute | solution.py:180
  185.0 24.6 %collective-permute-start.18 = (bf16[2,4,256,128]{3,2,1,0:T(8,128)(2,1)}, bf16[2,4,256,128]{3,2,1,0:T(8,128)(2,1)}, u32[]{:S(2)}, u32[]{:S(2)}) collective-permute-start(bf16[2,4,256,128]{3,2,1,0:T(8,128)(2,1)} %collective-permute-done.16.refs_0_), channel_id=1, source_target_pairs={{0,2},{1,3},{2,0},{3,1},{4,6},{5,7},{6,4},{7,5},{8,10},{9,11},{10,... | collective-permute-start | bytes 1572872 | tf_op jit(solution)/shard_map/ppermute | solution.py:180
  186.7 24.5 %collective-permute-start.17 = (bf16[2,4,256,128]{3,2,1,0:T(8,128)(2,1)}, bf16[2,4,256,128]{3,2,1,0:T(8,128)(2,1)S(1)}, u32[]{:S(2)}, u32[]{:S(2)}) collective-permute-start(bf16[2,4,256,128]{3,2,1,0:T(8,128)(2,1)} %collective-permute-done.16.refs_0_), channel_id=1, source_target_pairs={{0,1},{1,0},{2,3},{3,2},{4,5},{5,4},{6,7},{7,6},{8,9},{9,8},{10,11... | collective-permute-start | bytes 1572872 | tf_op jit(solution)/shard_map/ppermute | solution.py:180
  188.1 27.1 %collective-permute-start.13 = (bf16[2,4,256,128]{3,2,1,0:T(8,128)(2,1)}, bf16[2,4,256,128]{3,2,1,0:T(8,128)(2,1)}, u32[]{:S(2)}, u32[]{:S(2)}) collective-permute-start(bf16[2,4,256,128]{3,2,1,0:T(8,128)(2,1)} %collective-permute-done.12.refs_0_), channel_id=1, source_target_pairs={{0,1},{1,0},{2,3},{3,2},{4,5},{5,4},{6,7},{7,6},{8,9},{9,8},{10,11... | collective-permute-start | bytes 1572872 | tf_op jit(solution)/shard_map/ppermute | solution.py:180
  192.8 28.0 %collective-permute-start.14 = (bf16[2,4,256,128]{3,2,1,0:T(8,128)(2,1)}, bf16[2,4,256,128]{3,2,1,0:T(8,128)(2,1)S(1)}, u32[]{:S(2)}, u32[]{:S(2)}) collective-permute-start(bf16[2,4,256,128]{3,2,1,0:T(8,128)(2,1)} %collective-permute-done.12.refs_0_), channel_id=1, source_target_pairs={{0,2},{1,3},{2,0},{3,1},{4,6},{5,7},{6,4},{7,5},{8,10},{9,11},{10,... | collective-permute-start | bytes 1572872 | tf_op jit(solution)/shard_map/ppermute | solution.py:180
  198.4 33.7 %collective-permute-start.10 = (bf16[2,4,256,128]{3,2,1,0:T(8,128)(2,1)}, bf16[2,4,256,128]{3,2,1,0:T(8,128)(2,1)}, u32[]{:S(2)}, u32[]{:S(2)}) collective-permute-start(bf16[2,4,256,128]{3,2,1,0:T(8,128)(2,1)} %collective-permute-done.8.refs_0_), channel_id=1, source_target_pairs={{0,2},{1,3},{2,0},{3,1},{4,6},{5,7},{6,4},{7,5},{8,10},{9,11},{10,... | collective-permute-start | bytes 1572872 | tf_op jit(solution)/shard_map/ppermute | solution.py:180
  209.6 24.0 %collective-permute-start.9 = (bf16[2,4,256,128]{3,2,1,0:T(8,128)(2,1)}, bf16[2,4,256,128]{3,2,1,0:T(8,128)(2,1)}, u32[]{:S(2)}, u32[]{:S(2)}) collective-permute-start(bf16[2,4,256,128]{3,2,1,0:T(8,128)(2,1)} %collective-permute-done.8.refs_0_), channel_id=1, source_target_pairs={{0,1},{1,0},{2,3},{3,2},{4,5},{5,4},{6,7},{7,6},{8,9},{9,8},{10,11... | collective-permute-start | bytes 1572872 | tf_op jit(solution)/shard_map/ppermute | solution.py:180
  211.1 26.6 %collective-permute-start.5 = (bf16[2,4,256,128]{3,2,1,0:T(8,128)(2,1)}, bf16[2,4,256,128]{3,2,1,0:T(8,128)(2,1)}, u32[]{:S(2)}, u32[]{:S(2)}) collective-permute-start(bf16[2,4,256,128]{3,2,1,0:T(8,128)(2,1)} %collective-permute-done.4.refs_0_), channel_id=1, source_target_pairs={{0,1},{1,0},{2,3},{3,2},{4,5},{5,4},{6,7},{7,6},{8,9},{9,8},{10,11... | collective-permute-start | bytes 1572872 | tf_op jit(solution)/shard_map/ppermute | solution.py:180
  215.2 28.0 %collective-permute-start.6 = (bf16[2,4,256,128]{3,2,1,0:T(8,128)(2,1)}, bf16[2,4,256,128]{3,2,1,0:T(8,128)(2,1)S(1)}, u32[]{:S(2)}, u32[]{:S(2)}) collective-permute-start(bf16[2,4,256,128]{3,2,1,0:T(8,128)(2,1)} %collective-permute-done.4.refs_0_), channel_id=1, source_target_pairs={{0,2},{1,3},{2,0},{3,1},{4,6},{5,7},{6,4},{7,5},{8,10},{9,11},{10,... | collective-permute-start | bytes 1572872 | tf_op jit(solution)/shard_map/ppermute | solution.py:180
  220.7 33.8 %collective-permute-start.2 = (bf16[2,4,256,128]{3,2,1,0:T(8,128)(2,1)S(1)}, bf16[2,4,256,128]{3,2,1,0:T(8,128)(2,1)}, u32[]{:S(2)}, u32[]{:S(2)}) collective-permute-start(bf16[2,4,256,128]{3,2,1,0:T(8,128)(2,1)S(1)} %collective-permute-done.refs_0_), channel_id=1, source_target_pairs={{0,2},{1,3},{2,0},{3,1},{4,6},{5,7},{6,4},{7,5},{8,10},{9,11},{10,... | collective-permute-start | bytes 1572872 | tf_op jit(solution)/shard_map/ppermute | solution.py:180
  232.1 24.0 %collective-permute-start.1 = (bf16[2,4,256,128]{3,2,1,0:T(8,128)(2,1)S(1)}, bf16[2,4,256,128]{3,2,1,0:T(8,128)(2,1)}, u32[]{:S(2)}, u32[]{:S(2)}) collective-permute-start(bf16[2,4,256,128]{3,2,1,0:T(8,128)(2,1)S(1)} %collective-permute-done.refs_0_), channel_id=1, source_target_pairs={{0,1},{1,0},{2,3},{3,2},{4,5},{5,4},{6,7},{7,6},{8,9},{9,8},{10,11... | collective-permute-start | bytes 1572872 | tf_op jit(solution)/shard_map/ppermute | solution.py:180
  233.6 26.6 %collective-permute-start.27 = (bf16[2,4,256,128]{3,2,1,0:T(8,128)(2,1)}, bf16[2,4,256,128]{3,2,1,0:T(8,128)(2,1)}, u32[]{:S(2)}, u32[]{:S(2)}) collective-permute-start(bf16[2,4,256,128]{3,2,1,0:T(8,128)(2,1)} %copy-done.11), channel_id=1, source_target_pairs={{0,1},{1,0},{2,3},{3,2},{4,5},{5,4},{6,7},{7,6},{8,9},{9,8},{10,11... | collective-permute-start | bytes 1572872 | tf_op jit(solution)/shard_map/ppermute | solution.py:180
  237.7 28.1 %collective-permute-start.23 = (bf16[2,4,256,128]{3,2,1,0:T(8,128)(2,1)}, bf16[2,4,256,128]{3,2,1,0:T(8,128)(2,1)}, u32[]{:S(2)}, u32[]{:S(2)}) collective-permute-start(bf16[2,4,256,128]{3,2,1,0:T(8,128)(2,1)} %collective-permute-done.21.refs_1_), channel_id=1, source_target_pairs={{0,2},{1,3},{2,0},{3,1},{4,6},{5,7},{6,4},{7,5},{8,10},{9,11},{10,... | collective-permute-start | bytes 1572872 | tf_op jit(solution)/shard_map/ppermute | solution.py:180
  243.2 28.2 %collective-permute-start.19 = (bf16[2,4,256,128]{3,2,1,0:T(8,128)(2,1)}, bf16[2,4,256,128]{3,2,1,0:T(8,128)(2,1)}, u32[]{:S(2)}, u32[]{:S(2)}) collective-permute-start(bf16[2,4,256,128]{3,2,1,0:T(8,128)(2,1)} %collective-permute-done.18.refs_2_), channel_id=1, source_target_pairs={{0,1},{1,0},{2,3},{3,2},{4,5},{5,4},{6,7},{7,6},{8,9},{9,8},{10,11... | collective-permute-start | bytes 1572872 | tf_op jit(solution)/shard_map/ppermute | solution.py:180
  254.6 22.5 %collective-permute-start.15 = (bf16[2,4,256,128]{3,2,1,0:T(8,128)(2,1)}, bf16[2,4,256,128]{3,2,1,0:T(8,128)(2,1)}, u32[]{:S(2)}, u32[]{:S(2)}) collective-permute-start(bf16[2,4,256,128]{3,2,1,0:T(8,128)(2,1)} %collective-permute-done.13.refs_1_), channel_id=1, source_target_pairs={{0,2},{1,3},{2,0},{3,1},{4,6},{5,7},{6,4},{7,5},{8,10},{9,11},{10,... | collective-permute-start | bytes 1572872 | tf_op jit(solution)/shard_map/ppermute | solution.py:180
  256.1 26.6 %collective-permute-start.11 = (bf16[2,4,256,128]{3,2,1,0:T(8,128)(2,1)}, bf16[2,4,256,128]{3,2,1,0:T(8,128)(2,1)}, u32[]{:S(2)}, u32[]{:S(2)}) collective-permute-start(bf16[2,4,256,128]{3,2,1,0:T(8,128)(2,1)} %collective-permute-done.10.refs_2_), channel_id=1, source_target_pairs={{0,1},{1,0},{2,3},{3,2},{4,5},{5,4},{6,7},{7,6},{8,9},{9,8},{10,11... | collective-permute-start | bytes 1572872 | tf_op jit(solution)/shard_map/ppermute | solution.py:180
  260.2 28.1 %collective-permute-start.7 = (bf16[2,4,256,128]{3,2,1,0:T(8,128)(2,1)}, bf16[2,4,256,128]{3,2,1,0:T(8,128)(2,1)}, u32[]{:S(2)}, u32[]{:S(2)}) collective-permute-start(bf16[2,4,256,128]{3,2,1,0:T(8,128)(2,1)} %collective-permute-done.5.refs_1_), channel_id=1, source_target_pairs={{0,2},{1,3},{2,0},{3,1},{4,6},{5,7},{6,4},{7,5},{8,10},{9,11},{10,... | collective-permute-start | bytes 1572872 | tf_op jit(solution)/shard_map/ppermute | solution.py:180
  265.8 28.1 %collective-permute-start.3 = (bf16[2,4,256,128]{3,2,1,0:T(8,128)(2,1)}, bf16[2,4,256,128]{3,2,1,0:T(8,128)(2,1)}, u32[]{:S(2)}, u32[]{:S(2)}) collective-permute-start(bf16[2,4,256,128]{3,2,1,0:T(8,128)(2,1)} %collective-permute-done.2.refs_2_), channel_id=1, source_target_pairs={{0,1},{1,0},{2,3},{3,2},{4,5},{5,4},{6,7},{7,6},{8,9},{9,8},{10,11... | collective-permute-start | bytes 1572872 | tf_op jit(solution)/shard_map/ppermute | solution.py:180
  271.4 61.6 %collective-permute-start.47 = (bf16[4,256,128]{2,1,0:T(8,128)(2,1)}, bf16[4,256,128]{2,1,0:T(8,128)(2,1)}, u32[]{:S(2)}, u32[]{:S(2)}) collective-permute-start(bf16[4,256,128]{2,1,0:T(8,128)(2,1)} %collective-permute-done.46.refs_0_), channel_id=1, source_target_pairs={{0,1},{1,0},{2,3},{3,2},{4,5},{5,4},{6,7},{7,6},{8,9},{9,8},{10,11... | collective-permute-start | bytes 786440 | tf_op jit(solution)/shard_map/ppermute | solution.py:180
  277.0 57.6 %collective-permute-start.43 = (bf16[4,256,128]{2,1,0:T(8,128)(2,1)}, bf16[4,256,128]{2,1,0:T(8,128)(2,1)}, u32[]{:S(2)}, u32[]{:S(2)}) collective-permute-start(bf16[4,256,128]{2,1,0:T(8,128)(2,1)} %collective-permute-done.42.refs_0_), channel_id=1, source_target_pairs={{0,1},{1,0},{2,3},{3,2},{4,5},{5,4},{6,7},{7,6},{8,9},{9,8},{10,11... | collective-permute-start | bytes 786440 | tf_op jit(solution)/shard_map/ppermute | solution.py:180
  282.6 52.5 %collective-permute-start.44 = (bf16[4,256,128]{2,1,0:T(8,128)(2,1)}, bf16[4,256,128]{2,1,0:T(8,128)(2,1)}, u32[]{:S(2)}, u32[]{:S(2)}) collective-permute-start(bf16[4,256,128]{2,1,0:T(8,128)(2,1)} %collective-permute-done.42.refs_0_), channel_id=1, source_target_pairs={{0,2},{1,3},{2,0},{3,1},{4,6},{5,7},{6,4},{7,5},{8,10},{9,11},{10,... | collective-permute-start | bytes 786440 | tf_op jit(solution)/shard_map/ppermute | solution.py:180
  288.3 47.4 %collective-permute-start.40 = (bf16[4,256,128]{2,1,0:T(8,128)(2,1)}, bf16[4,256,128]{2,1,0:T(8,128)(2,1)}, u32[]{:S(2)}, u32[]{:S(2)}) collective-permute-start(bf16[4,256,128]{2,1,0:T(8,128)(2,1)} %collective-permute-done.38.refs_0_), channel_id=1, source_target_pairs={{0,2},{1,3},{2,0},{3,1},{4,6},{5,7},{6,4},{7,5},{8,10},{9,11},{10,... | collective-permute-start | bytes 786440 | tf_op jit(solution)/shard_map/ppermute | solution.py:180
  293.9 43.3 %collective-permute-start.35 = (bf16[4,256,128]{2,1,0:T(8,128)(2,1)}, bf16[4,256,128]{2,1,0:T(8,128)(2,1)}, u32[]{:S(2)}, u32[]{:S(2)}) collective-permute-start(bf16[4,256,128]{2,1,0:T(8,128)(2,1)} %collective-permute-done.34.refs_0_), channel_id=1, source_target_pairs={{0,1},{1,0},{2,3},{3,2},{4,5},{5,4},{6,7},{7,6},{8,9},{9,8},{10,11... | collective-permute-start | bytes 786440 | tf_op jit(solution)/shard_map/ppermute | solution.py:180
  333.0 11.6 %collective-permute-start.61 = (bf16[4,256,128]{2,1,0:T(8,128)(2,1)}, bf16[4,256,128]{2,1,0:T(8,128)(2,1)S(1)}, u32[]{:S(2)}, u32[]{:S(2)}) collective-permute-start(bf16[4,256,128]{2,1,0:T(8,128)(2,1)} %collective-permute-done.59.refs_1_), channel_id=1, source_target_pairs={{0,2},{1,3},{2,0},{3,1},{4,6},{5,7},{6,4},{7,5},{8,10},{9,11},{10,... | collective-permute-start | bytes 786440 | tf_op jit(solution)/shard_map/ppermute | solution.py:180
  335.1 13.0 %collective-permute-start.53 = (bf16[4,256,128]{2,1,0:T(8,128)(2,1)}, bf16[4,256,128]{2,1,0:T(8,128)(2,1)}, u32[]{:S(2)}, u32[]{:S(2)}) collective-permute-start(bf16[4,256,128]{2,1,0:T(8,128)(2,1)} %copy-done.21), channel_id=1, source_target_pairs={{0,2},{1,3},{2,0},{3,1},{4,6},{5,7},{6,4},{7,5},{8,10},{9,11},{10,... | collective-permute-start | bytes 786440 | tf_op jit(solution)/shard_map/ppermute | solution.py:180
  335.6 14.1 %collective-permute-start.49 = (bf16[4,256,128]{2,1,0:T(8,128)(2,1)}, bf16[4,256,128]{2,1,0:T(8,128)(2,1)}, u32[]{:S(2)}, u32[]{:S(2)}) collective-permute-start(bf16[4,256,128]{2,1,0:T(8,128)(2,1)} %copy-done.22), channel_id=1, source_target_pairs={{0,1},{1,0},{2,3},{3,2},{4,5},{5,4},{6,7},{7,6},{8,9},{9,8},{10,11... | collective-permute-start | bytes 786440 | tf_op jit(solution)/shard_map/ppermute | solution.py:180
  337.1 16.7 %collective-permute-start.45 = (bf16[4,256,128]{2,1,0:T(8,128)(2,1)}, bf16[4,256,128]{2,1,0:T(8,128)(2,1)}, u32[]{:S(2)}, u32[]{:S(2)}) collective-permute-start(bf16[4,256,128]{2,1,0:T(8,128)(2,1)} %collective-permute-done.43.refs_1_), channel_id=1, source_target_pairs={{0,2},{1,3},{2,0},{3,1},{4,6},{5,7},{6,4},{7,5},{8,10},{9,11},{10,... | collective-permute-start | bytes 786440 | tf_op jit(solution)/shard_map/ppermute | solution.py:180
  345.3 39.0 %collective-permute-start.32 = (bf16[4,256,128]{2,1,0:T(8,128)(2,1)S(1)}, bf16[4,256,128]{2,1,0:T(8,128)(2,1)}, u32[]{:S(2)}, u32[]{:S(2)}) collective-permute-start(bf16[4,256,128]{2,1,0:T(8,128)(2,1)S(1)} %get-tuple-element.74.refs_0_), channel_id=1, source_target_pairs={{0,2},{1,3},{2,0},{3,1},{4,6},{5,7},{6,4},{7,5},{8,10},{9,11},{10,... | collective-permute-start | bytes 786440 | tf_op jit(solution)/shard_map/ppermute | solution.py:180
  345.8 39.1 %collective-permute-start.39 = (bf16[4,256,128]{2,1,0:T(8,128)(2,1)}, bf16[4,256,128]{2,1,0:T(8,128)(2,1)}, u32[]{:S(2)}, u32[]{:S(2)}) collective-permute-start(bf16[4,256,128]{2,1,0:T(8,128)(2,1)} %collective-permute-done.38.refs_0_), channel_id=1, source_target_pairs={{0,1},{1,0},{2,3},{3,2},{4,5},{5,4},{6,7},{7,6},{8,9},{9,8},{10,11... | collective-permute-start | bytes 786440 | tf_op jit(solution)/shard_map/ppermute | solution.py:180
  348.2 43.3 %collective-permute-start.36 = (bf16[4,256,128]{2,1,0:T(8,128)(2,1)}, bf16[4,256,128]{2,1,0:T(8,128)(2,1)}, u32[]{:S(2)}, u32[]{:S(2)}) collective-permute-start(bf16[4,256,128]{2,1,0:T(8,128)(2,1)} %collective-permute-done.34.refs_0_), channel_id=1, source_target_pairs={{0,2},{1,3},{2,0},{3,1},{4,6},{5,7},{6,4},{7,5},{8,10},{9,11},{10,... | collective-permute-start | bytes 786440 | tf_op jit(solution)/shard_map/ppermute | solution.py:180
  349.7 36.7 %collective-permute-start.41 = (bf16[4,256,128]{2,1,0:T(8,128)(2,1)}, bf16[4,256,128]{2,1,0:T(8,128)(2,1)}, u32[]{:S(2)}, u32[]{:S(2)}) collective-permute-start(bf16[4,256,128]{2,1,0:T(8,128)(2,1)} %collective-permute-done.40.refs_2_), channel_id=1, source_target_pairs={{0,1},{1,0},{2,3},{3,2},{4,5},{5,4},{6,7},{7,6},{8,9},{9,8},{10,11... | collective-permute-start | bytes 786440 | tf_op jit(solution)/shard_map/ppermute | solution.py:180
  353.8 37.6 %collective-permute-start.37 = (bf16[4,256,128]{2,1,0:T(8,128)(2,1)}, bf16[4,256,128]{2,1,0:T(8,128)(2,1)}, u32[]{:S(2)}, u32[]{:S(2)}) collective-permute-start(bf16[4,256,128]{2,1,0:T(8,128)(2,1)} %collective-permute-done.35.refs_1_), channel_id=1, source_target_pairs={{0,2},{1,3},{2,0},{3,1},{4,6},{5,7},{6,4},{7,5},{8,10},{9,11},{10,... | collective-permute-start | bytes 786440 | tf_op jit(solution)/shard_map/ppermute | solution.py:180
  384.3 29.6 %collective-permute-start.31 = (bf16[4,256,128]{2,1,0:T(8,128)(2,1)S(1)}, bf16[4,256,128]{2,1,0:T(8,128)(2,1)S(1)}, u32[]{:S(2)}, u32[]{:S(2)}) collective-permute-start(bf16[4,256,128]{2,1,0:T(8,128)(2,1)S(1)} %get-tuple-element.74.refs_0_), channel_id=1, source_target_pairs={{0,1},{1,0},{2,3},{3,2},{4,5},{5,4},{6,7},{7,6},{8,9},{9,8},{10,11... | collective-permute-start | bytes 786440 | tf_op jit(solution)/shard_map/ppermute | solution.py:180
  384.9 31.2 %collective-permute-start.33 = (bf16[4,256,128]{2,1,0:T(8,128)(2,1)}, bf16[4,256,128]{2,1,0:T(8,128)(2,1)S(1)}, u32[]{:S(2)}, u32[]{:S(2)}) collective-permute-start(bf16[4,256,128]{2,1,0:T(8,128)(2,1)} %collective-permute-done.32.refs_2_), channel_id=1, source_target_pairs={{0,1},{1,0},{2,3},{3,2},{4,5},{5,4},{6,7},{7,6},{8,9},{9,8},{10,11... | collective-permute-start | bytes 786440 | tf_op jit(solution)/shard_map/ppermute | solution.py:180
  396.6 20.9 %collective-permute-start.68 = (f32[256,256]{1,0:T(8,128)}, f32[256,256]{1,0:T(8,128)S(1)}, u32[]{:S(2)}, u32[]{:S(2)}) collective-permute-start(f32[256,256]{1,0:T(8,128)} %get-tuple-element.66), channel_id=1, source_target_pairs={{0,4},{4,0},{8,12},{12,8},{16,20},{20,16},{24,28},{28,24},{1,5},{5... | collective-permute-start | bytes 786440 | tf_op jit(solution)/shard_map/ppermute | solution.py:176
  396.6 23.9 %collective-permute-start.67 = (f32[256,256]{1,0:T(8,128)S(1)}, f32[256,256]{1,0:T(8,128)S(1)}, u32[]{:S(2)}, u32[]{:S(2)}) collective-permute-start(f32[256,256]{1,0:T(8,128)S(1)} %copy-done.34), channel_id=1, source_target_pairs={{0,12},{4,8},{8,4},{12,0},{16,28},{20,24},{24,20},{28,16},{1,13},{... | collective-permute-start | bytes 786440 | tf_op jit(solution)/shard_map/ppermute | solution.py:176
  413.8 13.9 %collective-permute-start.66 = (f32[256,256]{1,0:T(8,128)}, f32[256,256]{1,0:T(8,128)S(1)}, u32[]{:S(2)}, u32[]{:S(2)}) collective-permute-start(f32[256,256]{1,0:T(8,128)} %get-tuple-element.64), channel_id=1, source_target_pairs={{0,8},{4,12},{8,0},{12,4},{16,24},{20,28},{24,16},{28,20},{1,9},{5... | collective-permute-start | bytes 786440 | tf_op jit(solution)/shard_map/ppermute | solution.py:176
  413.9 19.6 %collective-permute-start.65 = (f32[256,256]{1,0:T(8,128)S(1)}, f32[256,256]{1,0:T(8,128)S(1)}, u32[]{:S(2)}, u32[]{:S(2)}) collective-permute-start(f32[256,256]{1,0:T(8,128)S(1)} %copy-done.33), channel_id=1, source_target_pairs={{0,28},{4,24},{8,20},{12,16},{16,12},{20,8},{24,4},{28,0},{1,29},{... | collective-permute-start | bytes 786440 | tf_op jit(solution)/shard_map/ppermute | solution.py:176
  416.1 24.3 %collective-permute-start.64 = (f32[256,256]{1,0:T(8,128)S(1)}, f32[256,256]{1,0:T(8,128)S(1)}, u32[]{:S(2)}, u32[]{:S(2)}) collective-permute-start(f32[256,256]{1,0:T(8,128)S(1)} %copy-done.32), channel_id=1, source_target_pairs={{0,24},{4,28},{8,16},{12,20},{16,8},{20,12},{24,0},{28,4},{1,25},{... | collective-permute-start | bytes 786440 | tf_op jit(solution)/shard_map/ppermute | solution.py:176
  417.5 40.1 %collective-permute-start.63 = (f32[256,256]{1,0:T(8,128)S(1)}, f32[256,256]{1,0:T(8,128)S(1)}, u32[]{:S(2)}, u32[]{:S(2)}) collective-permute-start(f32[256,256]{1,0:T(8,128)S(1)} %copy-done.31), channel_id=1, source_target_pairs={{0,20},{4,16},{8,28},{12,24},{16,4},{20,0},{24,12},{28,8},{1,21},{... | collective-permute-start | bytes 786440 | tf_op jit(solution)/shard_map/ppermute | solution.py:176
  420.5 42.8 %collective-permute-start.62 = (f32[256,256]{1,0:T(8,128)S(1)}, f32[256,256]{1,0:T(8,128)S(1)}, u32[]{:S(2)}, u32[]{:S(2)}) collective-permute-start(f32[256,256]{1,0:T(8,128)S(1)} %copy-done.30), channel_id=1, source_target_pairs={{0,16},{4,20},{8,24},{12,28},{16,0},{20,4},{24,8},{28,12},{1,17},{... | collective-permute-start | bytes 786440 | tf_op jit(solution)/shard_map/ppermute | solution.py:176
  (40 other events, 2033.4 us)

commit v2 on v0

v2 whole, which is shorter than its diff:
```python
import functools

import jax
import jax.numpy as jnp
from jax import lax
from jax.experimental import pallas as pl
from jax.experimental.pallas import tpu as pltpu
from jax.sharding import PartitionSpec as P

FF = 512
GROUPS = 4
EPG = 8
LANES = 128
HERE = (0, 0)
ANYWHERE = pl.BlockSpec(memory_space=pl.ANY)
ROOM = pltpu.CompilerParams(vmem_limit_bytes=63 * 2**20)


def flatten_rows(piece):
    count, experts, rows, hidden = piece.shape
    return piece.transpose(0, 2, 1, 3).reshape(count, rows, experts * hidden)


def restore_rows(gathered, rows):
    parts = lax.axis_size("tp")
    count, total, width = gathered.shape
    blocks = total // (parts * rows)
    ordered = gathered.reshape(count, parts, blocks, rows, width).transpose(0, 2, 1, 3, 4)
    return ordered.reshape(count, total, width)


def activations(normed, gate_local, up_local, column_weight):
    width = normed.shape[1]
    gate_act = jnp.dot(normed, gate_local, preferred_element_type=jnp.float32) * width ** (-0.5)
    up_act = jnp.dot(normed, up_local, preferred_element_type=jnp.float32) * width ** (-0.5)
    return (column_weight * jax.nn.silu(gate_act) * up_act).astype(jnp.bfloat16)


def route_columns(group_choice, inner_choice, route_weight, columns):
    first = lax.axis_index("fs") * columns
    owner = (first + jnp.arange(columns, dtype=jnp.int32)) // FF
    chosen = group_choice[:, None] * EPG + inner_choice
    picked = jnp.where(chosen[:, :, None] == owner[None, None, :], route_weight[:, :, None], 0.0)
    return jnp.sum(picked, axis=1)


def normalize(prompt):
    values = prompt.astype(jnp.float32)
    mean = jnp.mean(values * values, axis=1, keepdims=True)
    return (values * lax.rsqrt(mean + 1e-06)).astype(jnp.bfloat16)


def general_shards(
    prompt, norm_gain, gate_master, up_master, down_master, group_choice, inner_choice, route_weight
):
    scale = norm_gain[None, :, None]
    gate_cast = (gate_master * scale).astype(jnp.bfloat16)
    up_cast = (up_master * scale).astype(jnp.bfloat16)
    down_cast = down_master.astype(jnp.bfloat16)
    rows = gate_master.shape[1] // lax.axis_size("tp")
    normed = normalize(prompt)
    stacked = jnp.stack([gate_cast, up_cast, down_cast])
    widened = lax.all_to_all(stacked, "tp", split_axis=2, concat_axis=3, tiled=True)
    moved = lax.all_to_all(flatten_rows(widened), "fs", split_axis=2, concat_axis=1, tiled=True)
    served = restore_rows(lax.all_gather(moved, "tp", axis=1, tiled=True), rows)
    gate_local, up_local, down_local = (served[0], served[1], served[2])
    column_weight = route_columns(group_choice, inner_choice, route_weight, gate_local.shape[1])
    scaled = activations(normed, gate_local, up_local, column_weight)
    summed = lax.psum_scatter(
        lax.dot_general(
            down_local, scaled, (((1,), (1,)), ((), ())), preferred_element_type=jnp.float32
        ),
        "fs",
        scatter_dimension=0,
        tiled=True,
    )
    mixed = (summed * FF ** (-0.5)).T.astype(jnp.bfloat16)
    return (gate_local, up_local, down_local, mixed)


def partner(index, offset, ways, sign):
    chips, core = offset
    chip = lax.rem(index // 2 + (chips if sign > 0 else ways // 2 - chips), ways // 2)
    return chip * 2 + (index % 2 if core == 0 else 1 - index % 2)


def receiver(offset):
    return partner(lax.axis_index("fs"), offset, lax.axis_size("fs"), 1)


def sender(offset):
    return partner(lax.axis_index("fs"), offset, lax.axis_size("fs"), -1)


def cast_kernel(steps, gain_ref, gate_ref, up_ref, *refs):
    outs, (gate_buf, up_buf, out_buf, in_sem, out_sem) = refs[: len(steps)], refs[len(steps) :]
    held, rows, hidden = gate_buf.shape[1:]
    loads, stores = [], []
    for i, step in enumerate(steps):
        experts = pl.ds(receiver(step) * held, held)
        pair = [
            pltpu.make_async_copy(gate_ref.at[experts], gate_buf.at[i], in_sem.at[i, 0]),
            pltpu.make_async_copy(up_ref.at[experts], up_buf.at[i], in_sem.at[i, 1]),
        ]
        for copy in pair:
            copy.start()
        loads.append(pair)
    gain = jnp.broadcast_to(gain_ref[...], (hidden, rows)).T
    for i, out in enumerate(outs):
        for which, source in enumerate((gate_buf, up_buf)):
            loads[i][which].wait()
            for e in range(held):
                out_buf[i, which, e] = (source[i, e] * gain).astype(jnp.bfloat16)
        stores.append(pltpu.make_async_copy(out_buf.at[i], out, out_sem.at[i]))
        stores[i].start()
    for copy in stores:
        copy.wait()


def cast_pairs(steps, norm_gain, gate_master, up_master, held):
    _, rows, hidden = gate_master.shape
    count = len(steps)
    piece = jax.ShapeDtypeStruct((2, held, rows, hidden), jnp.bfloat16)
    return pl.pallas_call(
        functools.partial(cast_kernel, steps),
        in_specs=[pl.BlockSpec(memory_space=pltpu.VMEM), ANYWHERE, ANYWHERE],
        out_specs=[ANYWHERE] * count,
        out_shape=[piece] * count,
        scratch_shapes=[
            pltpu.VMEM((count, held, rows, hidden), jnp.float32),
            pltpu.VMEM((count, held, rows, hidden), jnp.float32),
            pltpu.VMEM((count, *piece.shape), jnp.bfloat16),
            pltpu.SemaphoreType.DMA((count, 2)),
            pltpu.SemaphoreType.DMA((count,)),
        ],
        compiler_params=ROOM,
    )(norm_gain[None, :], gate_master, up_master)


def column_of(expert, swap, hidden):
    return pl.multiple_of((expert * 4 + (lax.axis_index("tp") ^ swap)) * hidden, LANES)


def lay_pair_kernel(step, *refs):
    parts, (gate_out, up_out, held_buf, in_sem, out_sem) = refs[:4], refs[-5:]
    _, held, rows, hidden = parts[0].shape
    first = pl.multiple_of(sender(step) * rows, LANES)
    loads, stores = [], []
    for which in range(2):
        for swap, part in enumerate(parts):
            loads.append(
                pltpu.make_async_copy(
                    part.at[which], held_buf.at[which, swap], in_sem.at[which, swap]
                )
            )
            loads[-1].start()
    for which, out in enumerate((gate_out, up_out)):
        for swap in range(4):
            loads[which * 4 + swap].wait()
            for e in range(held):
                place = out.at[pl.ds(first, rows), pl.ds(column_of(e, swap, hidden), hidden)]
                stores.append(
                    pltpu.make_async_copy(
                        held_buf.at[which, swap, e], place, out_sem.at[which, swap, e]
                    )
                )
                stores[-1].start()
    for copy in stores:
        copy.wait()


def lay_pair(step, parts, outs, total):
    _, held, rows, hidden = parts[0].shape
    fresh = outs is None
    shape = jax.ShapeDtypeStruct((total, held * 4 * hidden), jnp.bfloat16)
    return pl.pallas_call(
        functools.partial(lay_pair_kernel, step),
        in_specs=[ANYWHERE] * (4 if fresh else 6),
        out_specs=[ANYWHERE, ANYWHERE],
        out_shape=[shape, shape],
        scratch_shapes=[
            pltpu.VMEM((2, 4, held, rows, hidden), jnp.bfloat16),
            pltpu.SemaphoreType.DMA((2, 4)),
            pltpu.SemaphoreType.DMA((2, 4, held)),
        ],
        input_output_aliases={} if fresh else {4: 0, 5: 1},
        compiler_params=ROOM,
    )(*parts, *(() if fresh else outs))


def lay_down_kernel(step, sums, factor, *refs):
    parts, scaled_ref, others = refs[:4], refs[4], refs[5 : 5 + sums]
    out, result_ref, held_buf, block, scaled_buf, sum_buf, in_sem, sum_sem, sems = refs[-9:]
    held, rows, hidden = parts[0].shape
    first = pl.multiple_of(sender(step) * rows, LANES)
    loads = [
        pltpu.make_async_copy(part, held_buf.at[swap], in_sem.at[swap])
        for swap, part in enumerate(parts)
    ]
    loads.append(pltpu.make_async_copy(scaled_ref, scaled_buf, sems.at[0]))
    for i, other in enumerate(others):
        loads.append(pltpu.make_async_copy(other, sum_buf.at[i], sum_sem.at[i]))
    for copy in loads:
        copy.start()
    for swap in range(4):
        loads[swap].wait()
        for e in range(held):
            block[:, pl.ds(column_of(e, swap, hidden), hidden)] = held_buf[swap, e]
    store = pltpu.make_async_copy(block, out.at[pl.ds(first, rows), :], sems.at[1])
    store.start()
    loads[4].wait()
    product = lax.dot_general(
        scaled_buf[...], block[...], (((1,), (1,)), ((), ())), preferred_element_type=jnp.float32
    )
    if sums:
        for i in range(sums):
            loads[5 + i].wait()
            product += sum_buf[i].astype(jnp.float32)
        product *= factor
    result_ref[...] = product.astype(result_ref.dtype)
    store.wait()


def lay_down(step, parts, scaled, others, out, total):
    held, rows, hidden = parts[0].shape
    width = held * 4 * hidden
    tokens = scaled.shape[0]
    fresh = out is None
    sums = len(others)
    return pl.pallas_call(
        functools.partial(lay_down_kernel, step, sums, FF ** (-0.5)),
        in_specs=[ANYWHERE] * (5 + sums + (0 if fresh else 1)),
        out_specs=[ANYWHERE, pl.BlockSpec(memory_space=pltpu.VMEM)],
        out_shape=[
            jax.ShapeDtypeStruct((total, width), jnp.bfloat16),
            jax.ShapeDtypeStruct((tokens, rows), jnp.bfloat16),
        ],
        scratch_shapes=[
            pltpu.VMEM((4, held, rows, hidden), jnp.bfloat16),
            pltpu.VMEM((rows, width), jnp.bfloat16),
            pltpu.VMEM((tokens, width), jnp.bfloat16),
            pltpu.VMEM((max(sums, 1), tokens, rows), jnp.bfloat16),
            pltpu.SemaphoreType.DMA((4,)),
            pltpu.SemaphoreType.DMA((max(sums, 1),)),
            pltpu.SemaphoreType.DMA((2,)),
        ],
        input_output_aliases={} if fresh else {5 + sums: 0},
        compiler_params=ROOM,
    )(*parts, scaled, *others, *(() if fresh else (out,)))


def act_kernel(normed_ref, gate_ref, up_ref, chosen_ref, weight_ref, out_ref):
    owner = lax.axis_index("fs") * pl.num_programs(0) + pl.program_id(0)
    picked = jnp.where(chosen_ref[...] == owner, weight_ref[...], 0.0)
    weight = jnp.sum(picked, axis=1, keepdims=True)
    normed = normed_ref[...]
    factor = normed.shape[1] ** (-0.5)
    gate = jnp.dot(normed, gate_ref[...], preferred_element_type=jnp.float32) * factor
    up = jnp.dot(normed, up_ref[...], preferred_element_type=jnp.float32) * factor
    out_ref[...] = (weight * (gate / (1.0 + jnp.exp(-gate))) * up).astype(jnp.bfloat16)


def act(normed, gate_local, up_local, chosen, route_weight, held):
    tokens, width = normed.shape
    block = gate_local.shape[1] // held
    whole = lambda array: pl.BlockSpec(array.shape, lambda e: (0, 0))
    columns = pl.BlockSpec((width, block), lambda e: (0, e))
    return pl.pallas_call(
        act_kernel,
        grid=(held,),
        in_specs=[whole(normed), columns, columns, whole(chosen), whole(route_weight)],
        out_specs=pl.BlockSpec((tokens, block), lambda e: (0, e)),
        out_shape=jax.ShapeDtypeStruct((tokens, held * block), jnp.bfloat16),
        compiler_params=ROOM,
    )(normed, gate_local, up_local, chosen, route_weight)


def fs_send(value, offset, sign):
    ways = lax.axis_size("fs")
    chips = offset[0] if sign > 0 else ways // 2 - offset[0]
    pairs = [
        (i, (i // 2 + chips) % (ways // 2) * 2 + (i % 2 ^ offset[1])) for i in range(ways)
    ]
    return lax.ppermute(value, "fs", pairs)


def tp_swap(value, step):
    return lax.ppermute(value, "tp", [(i, i ^ step) for i in range(lax.axis_size("tp"))])


def plan(ways):
    chips = ways // 2
    apart = []
    for near in range(1, chips // 2 + 1):
        both = [near] if 2 * near == chips else [near, chips - near]
        apart += [(far, core) for core in range(2) for far in both]
    pair = [(False, offset) for offset in [(0, 0), (0, 1)] + apart]
    return pair + [(True, offset) for offset in apart + [(0, 1), (0, 0)]]


def turns(pieces):
    seen = {True: 0, False: 0}
    result = []
    for down, _ in pieces:
        result.append(seen[down] % 2 == 0)
        seen[down] += 1
    return result


def exchange_shards(
    prompt, norm_gain, gate_master, up_master, down_master, group_choice, inner_choice, route_weight
):
    ways = lax.axis_size("fs")
    experts, rows, _ = gate_master.shape
    held, total = experts // ways, rows * ways
    pieces = plan(ways)

    cast = cast_pairs((HERE,), norm_gain, gate_master, up_master, held)
    others = tuple(offset for down, offset in pieces[1:] if not down)
    cast += cast_pairs(others, norm_gain, gate_master, up_master, held)

    own, left, right, last = ({}, {}, {}, {})
    turn = turns(pieces)
    for index, (down, step) in enumerate(pieces):
        if down:
            cut = lax.dynamic_slice_in_dim(down_master, receiver(step) * held, held, 0)
            piece = cut.astype(jnp.bfloat16)
        else:
            piece = cast[index]
        if step != HERE:
            piece = fs_send(piece, step, 1)
        own[index] = piece
        left[index] = tp_swap(piece, 1)
        right[index] = tp_swap(piece, 2)
        last[index] = tp_swap(left[index], 2) if turn[index] else tp_swap(right[index], 1)

    pair_out, down_out, scaled, sums = None, None, None, ()
    for index, (down, step) in enumerate(pieces):
        parts = own[index], left[index], right[index], last[index]
        if not down:
            pair_out = lay_pair(step, parts, pair_out, total)
            continue
        if scaled is None:
            normed, chosen = normalize(prompt), group_choice[:, None] * EPG + inner_choice
            scaled = act(normed, *pair_out, chosen, route_weight, held)
        down_out, result = lay_down(
            step, parts, scaled, sums if step == HERE else (), down_out, total
        )
        if step != HERE:
            sums += (fs_send(result, step, -1),)
    return (*pair_out, down_out, result)


def solution(mesh):
    in_specs = (
        P("tp", None),
        P("fs"),
        P(None, "fs", "tp"),
        P(None, "fs", "tp"),
        P(None, "fs", "tp"),
        P("tp"),
        P("tp", None),
        P("tp", None),
    )
    out_specs = (P(None, "fs"), P(None, "fs"), P(None, "fs"), P("tp", "fs"))
    wrap = functools.partial(
        jax.shard_map, mesh=mesh, in_specs=in_specs, out_specs=out_specs, check_vma=False
    )
    ways, parts = mesh.shape["fs"], mesh.shape["tp"]
    whole_experts = ways & (ways - 1) == 0 and ways >= 4 and (GROUPS * EPG) % ways == 0
    if not (whole_experts and parts == 4 and FF % (parts * LANES) == 0):
        return wrap(general_shards)

    return wrap(exchange_shards)
```

time: 669 us -> 419 us (0.63)
  blocking collectives: 220 us -> 0 us
  local copies, waits for them, and re-layouts: 142 us -> 6.09 us
  starting transfers between devices: 0.3 us -> 77.2 us
  Pallas kernels: 0 us -> 63 us
  matrix products: 19 us -> 0 us
  between operations: 14.1 us -> 1.47 us
  other arithmetic: 12 us -> 4.7 us
    ppermute x0 -> x69, waiting for transfers between devices: none -> 266 us  [the longest x48 148 us: tp_swap(): lax.ppermute(value, 'tp', [(i, i ^ step) for i in range(lax.axis_size('tp...]
    all_gather x1 -> x0, waiting for transfers between devices: 224 us -> none  [shards(): served = restore_rows(lax.all_gather(moved, 'tp', axis=1, tiled=True), rows)]
    all_to_all x2 -> x0, blocking collectives: 220 us -> none  [the longest x1 144 us: shards(): lax.all_to_all(flatten_rows(widened), 'fs', split_axis=2, concat_axis=1,...]
    ppermute x0 -> x69, starting transfers between devices: none -> 77.2 us  [the longest x48 53.4 us: tp_swap(): lax.ppermute(value, 'tp', [(i, i ^ step) for i in range(lax.axis_size('tp...]
    pallas_call x0 -> x19, Pallas kernels: none -> 63 us  [the longest x8 24.1 us: lay_down(): pl.pallas_call(functools.partial(lay_down_kernel, step, sums, FF ** (-0.5...]
    slice x4 -> x0, local copies, waits for them, and re-layouts: 42.1 us -> none  [shards(): gate_local, up_local, down_local = (served[0], served[1], served[2])]
    all_to_all x3 -> x0, local copies, waits for them, and re-layouts: 40.9 us -> none  [the longest x1 23.2 us: shards(): lax.all_to_all(flatten_rows(widened), 'fs', split_axis=2, concat_axis=1,...]
    reduce_scatter x1 -> x0, waiting for transfers between devices: 36.2 us -> none  [shards(): lax.psum_scatter(lax.dot_general(down_local, scaled, (((1,), (1,)), ((),...]
  transfers between devices with their start and end apart: 2 -> 69, of which waited for: 2 -> 38; matrix products, arithmetic and copies ran while one was open for 0% -> 1% of each run, Pallas kernels for 0% -> 14%
where the time goes in v2:
time: 419 us; the launch traced here: 418 us
  waiting for transfers between devices  266 us (63%)
  starting transfers between devices  77.2 us (18%)
  Pallas kernels  63 us (15%)
  local copies, waits for them, and re-layouts  6.09 us (1%)
  other arithmetic  4.7 us (1%)
    ppermute x48, waiting for transfers between devices, tp_swap(): lax.ppermute(value, 'tp', [(i, i ^ step) for i in range(lax.axis_size('tp...  148 us
    ppermute x21, waiting for transfers between devices, fs_send(): return lax.ppermute(value, 'fs', pairs)  118 us
    ppermute x48, starting transfers between devices, tp_swap(): lax.ppermute(value, 'tp', [(i, i ^ step) for i in range(lax.axis_size('tp...  53.4 us
    pallas_call x8, Pallas kernels, lay_down(): pl.pallas_call(functools.partial(lay_down_kernel, step, sums, FF ** (-0.5...  24.1 us
    ppermute x21, starting transfers between devices, fs_send(): return lax.ppermute(value, 'fs', pairs)  23.8 us
    pallas_call x8, Pallas kernels, lay_pair(): pl.pallas_call(functools.partial(lay_pair_kernel, step), in_specs=[ANYWHE...  20.7 us
    pallas_call x1, Pallas kernels, act(): pl.pallas_call(act_kernel, grid=(held,), in_specs=[whole(normed), columns...  9.77 us
  transfers between devices with their start and end apart: 69, of which 38 were waited for; matrix products, arithmetic and copies ran while one was open for 1% of the time, Pallas kernels for 14%

profile of v2, /device:TPU:0, one launch (start us, length us, event | category | flops | bytes accessed | tf_op | source)
XLA Modules:
  0.0 418.1 jit_solution(12175375580939435848)
XLA Ops:
  0.7 3.3 dynamic-slice_convert_fusion
  4.1 3.1 collective-permute-start.34
  7.1 2.1 collective-permute-start.39
  9.2 3.5 collective-permute-start.49
  12.8 3.7 collective-permute-done.34.refs_0_
  16.5 5.7 %collective-permute-done.39.refs_0_ = bf16[4,256,128]{2,1,0:T(8,128)(2,1)} collective-permute-done((bf16[4,256,128]{2,1,0:T(8,128)(2,1)S(1)}, bf16[4,256,128]{2,1,0:T(8,128)(2,1)}, u32[]{:S(2)}, u32[]{:S(2)}) %collective-permute-start.39) | collective-permute-done | bytes 262176 | tf_op jit(solution)/shard_map/ppermute | solution.py:284
  23.2 2.8 shard_map.112.refs_0_
  27.5 5.5 %shard_map.111 = (bf16[2,4,256,128]{3,2,1,0:T(8,128)(2,1)}, bf16[2,4,256,128]{3,2,1,0:T(8,128)(2,1)}, bf16[2,4,256,128]{3,2,1,0:T(8,128)(2,1)}, bf16[2,4,256,128...) custom-call(f32[1,256]{1,0:T(1,128)} %bitcast.2, ...), custom_call_target="tpu_custom_call" | custom-call | tf_op jit(solution)/shard_map/pallas_call | solution.py:124
  33.1 1.6 collective-permute-start.29
  34.7 14.7 %collective-permute-done.54.refs_0_ = bf16[4,256,128]{2,1,0:T(8,128)(2,1)} collective-permute-done((bf16[4,256,128]{2,1,0:T(8,128)(2,1)}, bf16[4,256,128]{2,1,0:T(8,128)(2,1)}, u32[]{:S(2)}, u32[]{:S(2)}) %collective-permute-start.54) | collective-permute-done | bytes 262176 | tf_op jit(solution)/shard_map/ppermute | solution.py:284
  49.4 5.4 %collective-permute-done.59.refs_0_ = bf16[4,256,128]{2,1,0:T(8,128)(2,1)} collective-permute-done((bf16[4,256,128]{2,1,0:T(8,128)(2,1)}, bf16[4,256,128]{2,1,0:T(8,128)(2,1)}, u32[]{:S(2)}, u32[]{:S(2)}) %collective-permute-start.59) | collective-permute-done | bytes 262176 | tf_op jit(solution)/shard_map/ppermute | solution.py:284
  56.3 6.9 %collective-permute-done.32.refs_2_ = bf16[4,256,128]{2,1,0:T(8,128)(2,1)} collective-permute-done((bf16[4,256,128]{2,1,0:T(8,128)(2,1)S(1)}, bf16[4,256,128]{2,1,0:T(8,128)(2,1)}, u32[]{:S(2)}, u32[]{:S(2)}) %collective-permute-start.32) | collective-permute-done | bytes 262176 | tf_op jit(solution)/shard_map/ppermute | solution.py:288
  63.2 3.5 collective-permute-start.16
  67.6 3.5 collective-permute-start.8
  72.1 10.9 %collective-permute-done.16.refs_0_ = bf16[2,4,256,128]{3,2,1,0:T(8,128)(2,1)S(1)} collective-permute-done((bf16[2,4,256,128]{3,2,1,0:T(8,128)(2,1)}, bf16[2,4,256,128]{3,2,1,0:T(8,128)(2,1)S(1)}, u32[]{:S(2)}, u32[]{:S(2)}) %collective-permute-start.16) | collective-permute-done | bytes 524320 | tf_op jit(solution)/shard_map/ppermute | solution.py:284
  84.4 8.1 %collective-permute-done.12.refs_0_ = bf16[2,4,256,128]{3,2,1,0:T(8,128)(2,1)S(1)} collective-permute-done((bf16[2,4,256,128]{3,2,1,0:T(8,128)(2,1)}, bf16[2,4,256,128]{3,2,1,0:T(8,128)(2,1)S(1)}, u32[]{:S(2)}, u32[]{:S(2)}) %collective-permute-start.12) | collective-permute-done | bytes 524320 | tf_op jit(solution)/shard_map/ppermute | solution.py:284
  94.1 10.3 %collective-permute-done.8.refs_0_ = bf16[2,4,256,128]{3,2,1,0:T(8,128)(2,1)S(1)} collective-permute-done((bf16[2,4,256,128]{3,2,1,0:T(8,128)(2,1)}, bf16[2,4,256,128]{3,2,1,0:T(8,128)(2,1)S(1)}, u32[]{:S(2)}, u32[]{:S(2)}) %collective-permute-start.8) | collective-permute-done | bytes 524320 | tf_op jit(solution)/shard_map/ppermute | solution.py:284
  105.9 32.4 %collective-permute-done.4.refs_0_ = bf16[2,4,256,128]{3,2,1,0:T(8,128)(2,1)S(1)} collective-permute-done((bf16[2,4,256,128]{3,2,1,0:T(8,128)(2,1)}, bf16[2,4,256,128]{3,2,1,0:T(8,128)(2,1)S(1)}, u32[]{:S(2)}, u32[]{:S(2)}) %collective-permute-start.4) | collective-permute-done | bytes 524320 | tf_op jit(solution)/shard_map/ppermute | solution.py:284
  139.7 9.6 %collective-permute-done.refs_0_ = bf16[2,4,256,128]{3,2,1,0:T(8,128)(2,1)S(1)} collective-permute-done((bf16[2,4,256,128]{3,2,1,0:T(8,128)(2,1)}, bf16[2,4,256,128]{3,2,1,0:T(8,128)(2,1)S(1)}, u32[]{:S(2)}, u32[]{:S(2)}) %collective-permute-start) | collective-permute-done | bytes 524320 | tf_op jit(solution)/shard_map/ppermute | solution.py:284
  155.1 3.6 collective-permute-done.45.refs_1_
  161.7 4.1 collective-permute-done.51.refs_2_
  167.8 2.1 collective-permute-done.55.refs_1_
  172.9 4.2 %collective-permute-done.61.refs_2_ = bf16[4,256,128]{2,1,0:T(8,128)(2,1)} collective-permute-done((bf16[4,256,128]{2,1,0:T(8,128)(2,1)}, bf16[4,256,128]{2,1,0:T(8,128)(2,1)}, u32[]{:S(2)}, u32[]{:S(2)}) %collective-permute-start.61) | collective-permute-done | bytes 262176 | tf_op jit(solution)/shard_map/ppermute | solution.py:288
  179.2 2.1 collective-permute-done.65.refs_1_
  184.3 2.5 collective-permute-done.42.refs_3_
  188.3 22.4 %collective-permute-done.47.refs_3_ = bf16[4,256,128]{2,1,0:T(8,128)(2,1)S(1)} collective-permute-done((bf16[4,256,128]{2,1,0:T(8,128)(2,1)S(1)}, bf16[4,256,128]{2,1,0:T(8,128)(2,1)S(1)}, u32[]{:S(2)}, u32[]{:S(2)}) %collective-permute-start.47) | collective-permute-done | bytes 262176 | tf_op jit(solution)/shard_map/ppermute | solution.py:288
  212.8 2.5 collective-permute-done.57.refs_3_
  217.8 7.7 %collective-permute-done.25.refs_1_ = bf16[2,4,256,128]{3,2,1,0:T(8,128)(2,1)S(1)} collective-permute-done((bf16[2,4,256,128]{3,2,1,0:T(8,128)(2,1)S(1)}, bf16[2,4,256,128]{3,2,1,0:T(8,128)(2,1)S(1)}, u32[]{:S(2)}, u32[]{:S(2)}) %collective-permute-start.25) | collective-permute-done | bytes 524320 | tf_op jit(solution)/shard_map/ppermute | solution.py:288
  226.1 10.7 %collective-permute-done.21.refs_1_ = bf16[2,4,256,128]{3,2,1,0:T(8,128)(2,1)S(1)} collective-permute-done((bf16[2,4,256,128]{3,2,1,0:T(8,128)(2,1)S(1)}, bf16[2,4,256,128]{3,2,1,0:T(8,128)(2,1)S(1)}, u32[]{:S(2)}, u32[]{:S(2)}) %collective-permute-start.21) | collective-permute-done | bytes 524320 | tf_op jit(solution)/shard_map/ppermute | solution.py:288
  238.8 2.5 collective-permute-done.18.refs_2_
  241.8 6.2 %collective-permute-done.17.refs_1_ = bf16[2,4,256,128]{3,2,1,0:T(8,128)(2,1)S(1)} collective-permute-done((bf16[2,4,256,128]{3,2,1,0:T(8,128)(2,1)S(1)}, bf16[2,4,256,128]{3,2,1,0:T(8,128)(2,1)S(1)}, u32[]{:S(2)}, u32[]{:S(2)}) %collective-permute-start.17) | collective-permute-done | bytes 524320 | tf_op jit(solution)/shard_map/ppermute | solution.py:288
  248.6 10.7 %collective-permute-done.13.refs_1_ = bf16[2,4,256,128]{3,2,1,0:T(8,128)(2,1)S(1)} collective-permute-done((bf16[2,4,256,128]{3,2,1,0:T(8,128)(2,1)S(1)}, bf16[2,4,256,128]{3,2,1,0:T(8,128)(2,1)S(1)}, u32[]{:S(2)}, u32[]{:S(2)}) %collective-permute-start.13) | collective-permute-done | bytes 524320 | tf_op jit(solution)/shard_map/ppermute | solution.py:288
  261.3 2.5 collective-permute-done.10.refs_2_
  264.3 6.2 %collective-permute-done.9.refs_1_ = bf16[2,4,256,128]{3,2,1,0:T(8,128)(2,1)S(1)} collective-permute-done((bf16[2,4,256,128]{3,2,1,0:T(8,128)(2,1)S(1)}, bf16[2,4,256,128]{3,2,1,0:T(8,128)(2,1)S(1)}, u32[]{:S(2)}, u32[]{:S(2)}) %collective-permute-start.9) | collective-permute-done | bytes 524320 | tf_op jit(solution)/shard_map/ppermute | solution.py:288
  271.0 10.7 %collective-permute-done.5.refs_1_ = bf16[2,4,256,128]{3,2,1,0:T(8,128)(2,1)S(1)} collective-permute-done((bf16[2,4,256,128]{3,2,1,0:T(8,128)(2,1)S(1)}, bf16[2,4,256,128]{3,2,1,0:T(8,128)(2,1)S(1)}, u32[]{:S(2)}, u32[]{:S(2)}) %collective-permute-start.5) | collective-permute-done | bytes 524320 | tf_op jit(solution)/shard_map/ppermute | solution.py:288
  287.7 5.2 %collective-permute-done.1.refs_1_ = bf16[2,4,256,128]{3,2,1,0:T(8,128)(2,1)S(1)} collective-permute-done((bf16[2,4,256,128]{3,2,1,0:T(8,128)(2,1)S(1)}, bf16[2,4,256,128]{3,2,1,0:T(8,128)(2,1)S(1)}, u32[]{:S(2)}, u32[]{:S(2)}) %collective-permute-start.1) | collective-permute-done | bytes 524320 | tf_op jit(solution)/shard_map/ppermute | solution.py:288
  293.5 10.6 %collective-permute-done.27.refs_3_ = bf16[2,4,256,128]{3,2,1,0:T(8,128)(2,1)S(1)} collective-permute-done((bf16[2,4,256,128]{3,2,1,0:T(8,128)(2,1)S(1)}, bf16[2,4,256,128]{3,2,1,0:T(8,128)(2,1)S(1)}, u32[]{:S(2)}, u32[]{:S(2)}) %collective-permute-start.27) | collective-permute-done | bytes 524320 | tf_op jit(solution)/shard_map/ppermute | solution.py:288
  306.4 2.4 fusion.1.normed_ref
  308.8 6.6 %collective-permute-done.19.refs_3_ = bf16[2,4,256,128]{3,2,1,0:T(8,128)(2,1)S(1)} collective-permute-done((bf16[2,4,256,128]{3,2,1,0:T(8,128)(2,1)S(1)}, bf16[2,4,256,128]{3,2,1,0:T(8,128)(2,1)S(1)}, u32[]{:S(2)}, u32[]{:S(2)}) %collective-permute-start.19) | collective-permute-done | bytes 524320 | tf_op jit(solution)/shard_map/ppermute | solution.py:288
  317.6 9.1 %collective-permute-done.11.refs_3_ = bf16[2,4,256,128]{3,2,1,0:T(8,128)(2,1)S(1)} collective-permute-done((bf16[2,4,256,128]{3,2,1,0:T(8,128)(2,1)S(1)}, bf16[2,4,256,128]{3,2,1,0:T(8,128)(2,1)S(1)}, u32[]{:S(2)}, u32[]{:S(2)}) %collective-permute-start.11) | collective-permute-done | bytes 524320 | tf_op jit(solution)/shard_map/ppermute | solution.py:288
  329.8 8.2 %collective-permute-done.3.refs_3_ = bf16[2,4,256,128]{3,2,1,0:T(8,128)(2,1)} collective-permute-done((bf16[2,4,256,128]{3,2,1,0:T(8,128)(2,1)S(1)}, bf16[2,4,256,128]{3,2,1,0:T(8,128)(2,1)}, u32[]{:S(2)}, u32[]{:S(2)}) %collective-permute-start.3) | collective-permute-done | bytes 524320 | tf_op jit(solution)/shard_map/ppermute | solution.py:288
  339.3 2.6 shard_map.113
  341.9 2.6 shard_map.114
  344.5 2.6 shard_map.115
  347.1 2.6 shard_map.116
  349.7 2.6 shard_map.117
  352.3 2.6 shard_map.118
  354.9 2.6 shard_map.119
  357.5 2.6 shard_map.120
  360.1 9.8 %shard_map.121.refs_4_ = bf16[256,2048]{1,0:T(8,128)(2,1)} custom-call(bf16[256,2048]{1,0:T(8,128)(2,1)} %fusion.1.normed_ref, bf16[2048,2048]{1,0:T(8,128)(2,1)} %get-tuple-element.39.gate_ref, bf16[2048,2048]{1,0:T(8,128)(2,1)} %get-tuple-element.40.up_ref, s32[256,2]{1,0:T(8,128)} %broadcast_add_fusion.chosen_ref, f32[256,2]{1,0:T(8,128)} %copy.37.weight_ref), custom_call_target="tpu_custom_call" | custom-call | tf_op jit(solution)/shard_map/pallas_call | solution.py:268
  369.9 2.9 shard_map.122
  372.9 3.0 shard_map.123
  375.8 2.9 shard_map.124
  378.8 3.0 shard_map.125
  381.7 3.0 shard_map.126
  384.7 3.0 shard_map.127
  387.7 3.0 shard_map.128
  390.9 2.9 collective-permute-start.58
  393.8 3.5 collective-permute-start.48
  397.4 5.9 %collective-permute-done.63.refs_10_ = bf16[256,256]{1,0:T(8,128)(2,1)S(1)} collective-permute-done((bf16[256,256]{1,0:T(8,128)(2,1)S(1)}, bf16[256,256]{1,0:T(8,128)(2,1)S(1)}, u32[]{:S(2)}, u32[]{:S(2)}) %collective-permute-start.63) | collective-permute-done | bytes 131104 | tf_op jit(solution)/shard_map/ppermute | solution.py:284
  403.3 5.7 %collective-permute-done.58.refs_9_ = bf16[256,256]{1,0:T(8,128)(2,1)S(1)} collective-permute-done((bf16[256,256]{1,0:T(8,128)(2,1)}, bf16[256,256]{1,0:T(8,128)(2,1)S(1)}, u32[]{:S(2)}, u32[]{:S(2)}) %collective-permute-start.58) | collective-permute-done | bytes 131104 | tf_op jit(solution)/shard_map/ppermute | solution.py:284
  408.9 2.1 collective-permute-done.48.refs_7_
  411.0 2.8 collective-permute-done.38.refs_5_
  414.5 3.5 shard_map.129
  (213 shorter events, 59.8 us)
Async XLA Ops:
  4.1 12.4 %collective-permute-start.34 = (bf16[4,256,128]{2,1,0:T(8,128)(2,1)S(1)}, bf16[4,256,128]{2,1,0:T(8,128)(2,1)}, u32[]{:S(2)}, u32[]{:S(2)}) collective-permute-start(bf16[4,256,128]{2,1,0:T(8,128)(2,1)S(1)} %get-tuple-element.87), channel_id=1, source_target_pairs={{0,8},{4,12},{8,16},{12,20},{16,24},{20,28},{24,0},{28,4},{1,9},{5... | collective-permute-start | bytes 786440 | tf_op jit(solution)/shard_map/ppermute | solution.py:284
  7.1 15.0 %collective-permute-start.39 = (bf16[4,256,128]{2,1,0:T(8,128)(2,1)S(1)}, bf16[4,256,128]{2,1,0:T(8,128)(2,1)}, u32[]{:S(2)}, u32[]{:S(2)}) collective-permute-start(bf16[4,256,128]{2,1,0:T(8,128)(2,1)S(1)} %get-tuple-element.86), channel_id=1, source_target_pairs={{0,24},{4,28},{8,0},{12,4},{16,8},{20,12},{24,16},{28,20},{1,25},{... | collective-permute-start | bytes 786440 | tf_op jit(solution)/shard_map/ppermute | solution.py:284
  9.2 16.9 %collective-permute-start.44 = (bf16[4,256,128]{2,1,0:T(8,128)(2,1)}, bf16[4,256,128]{2,1,0:T(8,128)(2,1)}, u32[]{:S(2)}, u32[]{:S(2)}) collective-permute-start(bf16[4,256,128]{2,1,0:T(8,128)(2,1)} %get-tuple-element.85), channel_id=1, source_target_pairs={{0,12},{4,8},{8,20},{12,16},{16,28},{20,24},{24,4},{28,0},{1,13},{... | collective-permute-start | bytes 786440 | tf_op jit(solution)/shard_map/ppermute | solution.py:284
  9.2 23.9 %collective-permute-start.49 = (bf16[4,256,128]{2,1,0:T(8,128)(2,1)}, bf16[4,256,128]{2,1,0:T(8,128)(2,1)}, u32[]{:S(2)}, u32[]{:S(2)}) collective-permute-start(bf16[4,256,128]{2,1,0:T(8,128)(2,1)} %get-tuple-element.84), channel_id=1, source_target_pairs={{0,28},{4,24},{8,4},{12,0},{16,12},{20,8},{24,20},{28,16},{1,29},{... | collective-permute-start | bytes 786440 | tf_op jit(solution)/shard_map/ppermute | solution.py:284
  12.7 36.6 %collective-permute-start.54 = (bf16[4,256,128]{2,1,0:T(8,128)(2,1)}, bf16[4,256,128]{2,1,0:T(8,128)(2,1)}, u32[]{:S(2)}, u32[]{:S(2)}) collective-permute-start(bf16[4,256,128]{2,1,0:T(8,128)(2,1)} %get-tuple-element.83), channel_id=1, source_target_pairs={{0,16},{4,20},{8,24},{12,28},{16,0},{20,4},{24,8},{28,12},{1,17},{... | collective-permute-start | bytes 786440 | tf_op jit(solution)/shard_map/ppermute | solution.py:284
  16.5 38.3 %collective-permute-start.59 = (bf16[4,256,128]{2,1,0:T(8,128)(2,1)}, bf16[4,256,128]{2,1,0:T(8,128)(2,1)}, u32[]{:S(2)}, u32[]{:S(2)}) collective-permute-start(bf16[4,256,128]{2,1,0:T(8,128)(2,1)} %get-tuple-element.89), channel_id=1, source_target_pairs={{0,20},{4,16},{8,28},{12,24},{16,4},{20,0},{24,12},{28,8},{1,21},{... | collective-permute-start | bytes 786440 | tf_op jit(solution)/shard_map/ppermute | solution.py:284
  22.1 32.7 %collective-permute-start.64 = (bf16[4,256,128]{2,1,0:T(8,128)(2,1)}, bf16[4,256,128]{2,1,0:T(8,128)(2,1)}, u32[]{:S(2)}, u32[]{:S(2)}) collective-permute-start(bf16[4,256,128]{2,1,0:T(8,128)(2,1)} %get-tuple-element.82), channel_id=1, source_target_pairs={{0,4},{4,0},{8,12},{12,8},{16,20},{20,16},{24,28},{28,24},{1,5},{5... | collective-permute-start | bytes 786440 | tf_op jit(solution)/shard_map/ppermute | solution.py:284
  26.1 40.7 %collective-permute-start.28 = (bf16[2,4,256,128]{3,2,1,0:T(8,128)(2,1)}, bf16[2,4,256,128]{3,2,1,0:T(8,128)(2,1)}, u32[]{:S(2)}, u32[]{:S(2)}) collective-permute-start(bf16[2,4,256,128]{3,2,1,0:T(8,128)(2,1)} %shard_map.112.refs_0_), channel_id=1, source_target_pairs={{0,1},{1,0},{2,3},{3,2},{4,5},{5,4},{6,7},{7,6},{8,9},{9,8},{10,11... | collective-permute-start | bytes 1572872 | tf_op jit(solution)/shard_map/ppermute | solution.py:288
  33.1 33.7 %collective-permute-start.29 = (bf16[2,4,256,128]{3,2,1,0:T(8,128)(2,1)S(1)}, bf16[2,4,256,128]{3,2,1,0:T(8,128)(2,1)S(1)}, u32[]{:S(2)}, u32[]{:S(2)}) collective-permute-start(bf16[2,4,256,128]{3,2,1,0:T(8,128)(2,1)S(1)} %copy-done), channel_id=1, source_target_pairs={{0,2},{1,3},{2,0},{3,1},{4,6},{5,7},{6,4},{7,5},{8,10},{9,11},{10,... | collective-permute-start | bytes 1572872 | tf_op jit(solution)/shard_map/ppermute | solution.py:288
  49.4 21.7 %collective-permute-start.24 = (bf16[2,4,256,128]{3,2,1,0:T(8,128)(2,1)}, bf16[2,4,256,128]{3,2,1,0:T(8,128)(2,1)S(1)}, u32[]{:S(2)}, u32[]{:S(2)}) collective-permute-start(bf16[2,4,256,128]{3,2,1,0:T(8,128)(2,1)} %get-tuple-element.49), channel_id=1, source_target_pairs={{0,4},{4,0},{8,12},{12,8},{16,20},{20,16},{24,28},{28,24},{1,5},{5... | collective-permute-start | bytes 1572872 | tf_op jit(solution)/shard_map/ppermute | solution.py:284
  54.8 16.9 %collective-permute-start.20 = (bf16[2,4,256,128]{3,2,1,0:T(8,128)(2,1)}, bf16[2,4,256,128]{3,2,1,0:T(8,128)(2,1)S(1)}, u32[]{:S(2)}, u32[]{:S(2)}) collective-permute-start(bf16[2,4,256,128]{3,2,1,0:T(8,128)(2,1)} %get-tuple-element.48), channel_id=1, source_target_pairs={{0,8},{4,12},{8,16},{12,20},{16,24},{20,28},{24,0},{28,4},{1,9},{5... | collective-permute-start | bytes 1572872 | tf_op jit(solution)/shard_map/ppermute | solution.py:284
  63.2 19.7 %collective-permute-start.16 = (bf16[2,4,256,128]{3,2,1,0:T(8,128)(2,1)}, bf16[2,4,256,128]{3,2,1,0:T(8,128)(2,1)S(1)}, u32[]{:S(2)}, u32[]{:S(2)}) collective-permute-start(bf16[2,4,256,128]{3,2,1,0:T(8,128)(2,1)} %get-tuple-element.47), channel_id=1, source_target_pairs={{0,24},{4,28},{8,0},{12,4},{16,8},{20,12},{24,16},{28,20},{1,25},{... | collective-permute-start | bytes 1572872 | tf_op jit(solution)/shard_map/ppermute | solution.py:284
  66.8 25.8 %collective-permute-start.12 = (bf16[2,4,256,128]{3,2,1,0:T(8,128)(2,1)}, bf16[2,4,256,128]{3,2,1,0:T(8,128)(2,1)S(1)}, u32[]{:S(2)}, u32[]{:S(2)}) collective-permute-start(bf16[2,4,256,128]{3,2,1,0:T(8,128)(2,1)} %get-tuple-element.46), channel_id=1, source_target_pairs={{0,12},{4,8},{8,20},{12,16},{16,28},{20,24},{24,4},{28,0},{1,13},{... | collective-permute-start | bytes 1572872 | tf_op jit(solution)/shard_map/ppermute | solution.py:284
  67.6 36.8 %collective-permute-start.8 = (bf16[2,4,256,128]{3,2,1,0:T(8,128)(2,1)}, bf16[2,4,256,128]{3,2,1,0:T(8,128)(2,1)S(1)}, u32[]{:S(2)}, u32[]{:S(2)}) collective-permute-start(bf16[2,4,256,128]{3,2,1,0:T(8,128)(2,1)} %get-tuple-element.45), channel_id=1, source_target_pairs={{0,28},{4,24},{8,4},{12,0},{16,12},{20,8},{24,20},{28,16},{1,29},{... | collective-permute-start | bytes 1572872 | tf_op jit(solution)/shard_map/ppermute | solution.py:284
  71.1 67.2 %collective-permute-start.4 = (bf16[2,4,256,128]{3,2,1,0:T(8,128)(2,1)}, bf16[2,4,256,128]{3,2,1,0:T(8,128)(2,1)S(1)}, u32[]{:S(2)}, u32[]{:S(2)}) collective-permute-start(bf16[2,4,256,128]{3,2,1,0:T(8,128)(2,1)} %get-tuple-element.44), channel_id=1, source_target_pairs={{0,16},{4,20},{8,24},{12,28},{16,0},{20,4},{24,8},{28,12},{1,17},{... | collective-permute-start | bytes 1572872 | tf_op jit(solution)/shard_map/ppermute | solution.py:284
  71.7 77.7 %collective-permute-start = (bf16[2,4,256,128]{3,2,1,0:T(8,128)(2,1)}, bf16[2,4,256,128]{3,2,1,0:T(8,128)(2,1)S(1)}, u32[]{:S(2)}, u32[]{:S(2)}) collective-permute-start(bf16[2,4,256,128]{3,2,1,0:T(8,128)(2,1)} %get-tuple-element.43), channel_id=1, source_target_pairs={{0,20},{4,16},{8,28},{12,24},{16,4},{20,0},{24,12},{28,8},{1,21},{... | collective-permute-start | bytes 1572872 | tf_op jit(solution)/shard_map/ppermute | solution.py:284
  82.9 67.9 %collective-permute-start.35 = (bf16[4,256,128]{2,1,0:T(8,128)(2,1)}, bf16[4,256,128]{2,1,0:T(8,128)(2,1)S(1)}, u32[]{:S(2)}, u32[]{:S(2)}) collective-permute-start(bf16[4,256,128]{2,1,0:T(8,128)(2,1)} %collective-permute-done.34.refs_0_), channel_id=1, source_target_pairs={{0,1},{1,0},{2,3},{3,2},{4,5},{5,4},{6,7},{7,6},{8,9},{9,8},{10,11... | collective-permute-start | bytes 786440 | tf_op jit(solution)/shard_map/ppermute | solution.py:288
  92.5 59.8 %collective-permute-start.36 = (bf16[4,256,128]{2,1,0:T(8,128)(2,1)}, bf16[4,256,128]{2,1,0:T(8,128)(2,1)S(1)}, u32[]{:S(2)}, u32[]{:S(2)}) collective-permute-start(bf16[4,256,128]{2,1,0:T(8,128)(2,1)} %collective-permute-done.34.refs_0_), channel_id=1, source_target_pairs={{0,2},{1,3},{2,0},{3,1},{4,6},{5,7},{6,4},{7,5},{8,10},{9,11},{10,... | collective-permute-start | bytes 786440 | tf_op jit(solution)/shard_map/ppermute | solution.py:288
  104.3 48.7 %collective-permute-start.41 = (bf16[4,256,128]{2,1,0:T(8,128)(2,1)}, bf16[4,256,128]{2,1,0:T(8,128)(2,1)S(1)}, u32[]{:S(2)}, u32[]{:S(2)}) collective-permute-start(bf16[4,256,128]{2,1,0:T(8,128)(2,1)} %collective-permute-done.39.refs_0_), channel_id=1, source_target_pairs={{0,2},{1,3},{2,0},{3,1},{4,6},{5,7},{6,4},{7,5},{8,10},{9,11},{10,... | collective-permute-start | bytes 786440 | tf_op jit(solution)/shard_map/ppermute | solution.py:288
  138.3 15.3 %collective-permute-start.40 = (bf16[4,256,128]{2,1,0:T(8,128)(2,1)}, bf16[4,256,128]{2,1,0:T(8,128)(2,1)S(1)}, u32[]{:S(2)}, u32[]{:S(2)}) collective-permute-start(bf16[4,256,128]{2,1,0:T(8,128)(2,1)} %collective-permute-done.39.refs_0_), channel_id=1, source_target_pairs={{0,1},{1,0},{2,3},{3,2},{4,5},{5,4},{6,7},{7,6},{8,9},{9,8},{10,11... | collective-permute-start | bytes 786440 | tf_op jit(solution)/shard_map/ppermute | solution.py:288
  152.3 13.5 %collective-permute-start.51 = (bf16[4,256,128]{2,1,0:T(8,128)(2,1)}, bf16[4,256,128]{2,1,0:T(8,128)(2,1)S(1)}, u32[]{:S(2)}, u32[]{:S(2)}) collective-permute-start(bf16[4,256,128]{2,1,0:T(8,128)(2,1)} %collective-permute-done.49.refs_0_), channel_id=1, source_target_pairs={{0,2},{1,3},{2,0},{3,1},{4,6},{5,7},{6,4},{7,5},{8,10},{9,11},{10,... | collective-permute-start | bytes 786440 | tf_op jit(solution)/shard_map/ppermute | solution.py:288
  153.0 13.3 %collective-permute-start.50 = (bf16[4,256,128]{2,1,0:T(8,128)(2,1)}, bf16[4,256,128]{2,1,0:T(8,128)(2,1)S(1)}, u32[]{:S(2)}, u32[]{:S(2)}) collective-permute-start(bf16[4,256,128]{2,1,0:T(8,128)(2,1)} %collective-permute-done.49.refs_0_), channel_id=1, source_target_pairs={{0,1},{1,0},{2,3},{3,2},{4,5},{5,4},{6,7},{7,6},{8,9},{9,8},{10,11... | collective-permute-start | bytes 786440 | tf_op jit(solution)/shard_map/ppermute | solution.py:288
  153.6 16.3 %collective-permute-start.55 = (bf16[4,256,128]{2,1,0:T(8,128)(2,1)}, bf16[4,256,128]{2,1,0:T(8,128)(2,1)S(1)}, u32[]{:S(2)}, u32[]{:S(2)}) collective-permute-start(bf16[4,256,128]{2,1,0:T(8,128)(2,1)} %collective-permute-done.54.refs_0_), channel_id=1, source_target_pairs={{0,1},{1,0},{2,3},{3,2},{4,5},{5,4},{6,7},{7,6},{8,9},{9,8},{10,11... | collective-permute-start | bytes 786440 | tf_op jit(solution)/shard_map/ppermute | solution.py:288
  158.7 12.8 %collective-permute-start.56 = (bf16[4,256,128]{2,1,0:T(8,128)(2,1)}, bf16[4,256,128]{2,1,0:T(8,128)(2,1)S(1)}, u32[]{:S(2)}, u32[]{:S(2)}) collective-permute-start(bf16[4,256,128]{2,1,0:T(8,128)(2,1)} %collective-permute-done.54.refs_0_), channel_id=1, source_target_pairs={{0,2},{1,3},{2,0},{3,1},{4,6},{5,7},{6,4},{7,5},{8,10},{9,11},{10,... | collective-permute-start | bytes 786440 | tf_op jit(solution)/shard_map/ppermute | solution.py:288
  160.2 16.9 %collective-permute-start.61 = (bf16[4,256,128]{2,1,0:T(8,128)(2,1)}, bf16[4,256,128]{2,1,0:T(8,128)(2,1)}, u32[]{:S(2)}, u32[]{:S(2)}) collective-permute-start(bf16[4,256,128]{2,1,0:T(8,128)(2,1)} %collective-permute-done.59.refs_0_), channel_id=1, source_target_pairs={{0,2},{1,3},{2,0},{3,1},{4,6},{5,7},{6,4},{7,5},{8,10},{9,11},{10,... | collective-permute-start | bytes 786440 | tf_op jit(solution)/shard_map/ppermute | solution.py:288
  165.8 12.9 %collective-permute-start.60 = (bf16[4,256,128]{2,1,0:T(8,128)(2,1)}, bf16[4,256,128]{2,1,0:T(8,128)(2,1)S(1)}, u32[]{:S(2)}, u32[]{:S(2)}) collective-permute-start(bf16[4,256,128]{2,1,0:T(8,128)(2,1)} %collective-permute-done.59.refs_0_), channel_id=1, source_target_pairs={{0,1},{1,0},{2,3},{3,2},{4,5},{5,4},{6,7},{7,6},{8,9},{9,8},{10,11... | collective-permute-start | bytes 786440 | tf_op jit(solution)/shard_map/ppermute | solution.py:288
  166.4 14.9 %collective-permute-start.65 = (bf16[4,256,128]{2,1,0:T(8,128)(2,1)}, bf16[4,256,128]{2,1,0:T(8,128)(2,1)}, u32[]{:S(2)}, u32[]{:S(2)}) collective-permute-start(bf16[4,256,128]{2,1,0:T(8,128)(2,1)} %collective-permute-done.64.refs_0_), channel_id=1, source_target_pairs={{0,1},{1,0},{2,3},{3,2},{4,5},{5,4},{6,7},{7,6},{8,9},{9,8},{10,11... | collective-permute-start | bytes 786440 | tf_op jit(solution)/shard_map/ppermute | solution.py:288
  170.0 12.9 %collective-permute-start.37 = (bf16[4,256,128]{2,1,0:T(8,128)(2,1)S(1)}, bf16[4,256,128]{2,1,0:T(8,128)(2,1)}, u32[]{:S(2)}, u32[]{:S(2)}) collective-permute-start(bf16[4,256,128]{2,1,0:T(8,128)(2,1)S(1)} %collective-permute-done.35.refs_1_), channel_id=1, source_target_pairs={{0,2},{1,3},{2,0},{3,1},{4,6},{5,7},{6,4},{7,5},{8,10},{9,11},{10,... | collective-permute-start | bytes 786440 | tf_op jit(solution)/shard_map/ppermute | solution.py:288
  171.5 15.3 %collective-permute-start.42 = (bf16[4,256,128]{2,1,0:T(8,128)(2,1)S(1)}, bf16[4,256,128]{2,1,0:T(8,128)(2,1)S(1)}, u32[]{:S(2)}, u32[]{:S(2)}) collective-permute-start(bf16[4,256,128]{2,1,0:T(8,128)(2,1)S(1)} %collective-permute-done.41.refs_2_), channel_id=1, source_target_pairs={{0,1},{1,0},{2,3},{3,2},{4,5},{5,4},{6,7},{7,6},{8,9},{9,8},{10,11... | collective-permute-start | bytes 786440 | tf_op jit(solution)/shard_map/ppermute | solution.py:288
  177.1 39.6 %collective-permute-start.30 = (bf16[2,4,256,128]{3,2,1,0:T(8,128)(2,1)}, bf16[2,4,256,128]{3,2,1,0:T(8,128)(2,1)S(1)}, u32[]{:S(2)}, u32[]{:S(2)}) collective-permute-start(bf16[2,4,256,128]{3,2,1,0:T(8,128)(2,1)} %collective-permute-done.28.refs_1_), channel_id=1, source_target_pairs={{0,2},{1,3},{2,0},{3,1},{4,6},{5,7},{6,4},{7,5},{8,10},{9,11},{10,... | collective-permute-start | bytes 1572872 | tf_op jit(solution)/shard_map/ppermute | solution.py:288
  178.7 38.6 %collective-permute-start.26 = (bf16[2,4,256,128]{3,2,1,0:T(8,128)(2,1)S(1)}, bf16[2,4,256,128]{3,2,1,0:T(8,128)(2,1)S(1)}, u32[]{:S(2)}, u32[]{:S(2)}) collective-permute-start(bf16[2,4,256,128]{3,2,1,0:T(8,128)(2,1)S(1)} %collective-permute-done.24.refs_0_), channel_id=1, source_target_pairs={{0,2},{1,3},{2,0},{3,1},{4,6},{5,7},{6,4},{7,5},{8,10},{9,11},{10,... | collective-permute-start | bytes 1572872 | tf_op jit(solution)/shard_map/ppermute | solution.py:288
  181.3 29.4 %collective-permute-start.47 = (bf16[4,256,128]{2,1,0:T(8,128)(2,1)S(1)}, bf16[4,256,128]{2,1,0:T(8,128)(2,1)S(1)}, u32[]{:S(2)}, u32[]{:S(2)}) collective-permute-start(bf16[4,256,128]{2,1,0:T(8,128)(2,1)S(1)} %collective-permute-done.45.refs_1_), channel_id=1, source_target_pairs={{0,2},{1,3},{2,0},{3,1},{4,6},{5,7},{6,4},{7,5},{8,10},{9,11},{10,... | collective-permute-start | bytes 786440 | tf_op jit(solution)/shard_map/ppermute | solution.py:288
  182.8 28.5 %collective-permute-start.52 = (bf16[4,256,128]{2,1,0:T(8,128)(2,1)S(1)}, bf16[4,256,128]{2,1,0:T(8,128)(2,1)S(1)}, u32[]{:S(2)}, u32[]{:S(2)}) collective-permute-start(bf16[4,256,128]{2,1,0:T(8,128)(2,1)S(1)} %collective-permute-done.51.refs_2_), channel_id=1, source_target_pairs={{0,1},{1,0},{2,3},{3,2},{4,5},{5,4},{6,7},{7,6},{8,9},{9,8},{10,11... | collective-permute-start | bytes 786440 | tf_op jit(solution)/shard_map/ppermute | solution.py:288
  186.8 28.4 %collective-permute-start.57 = (bf16[4,256,128]{2,1,0:T(8,128)(2,1)S(1)}, bf16[4,256,128]{2,1,0:T(8,128)(2,1)S(1)}, u32[]{:S(2)}, u32[]{:S(2)}) collective-permute-start(bf16[4,256,128]{2,1,0:T(8,128)(2,1)S(1)} %collective-permute-done.55.refs_1_), channel_id=1, source_target_pairs={{0,2},{1,3},{2,0},{3,1},{4,6},{5,7},{6,4},{7,5},{8,10},{9,11},{10,... | collective-permute-start | bytes 786440 | tf_op jit(solution)/shard_map/ppermute | solution.py:288
  210.7 14.8 %collective-permute-start.25 = (bf16[2,4,256,128]{3,2,1,0:T(8,128)(2,1)S(1)}, bf16[2,4,256,128]{3,2,1,0:T(8,128)(2,1)S(1)}, u32[]{:S(2)}, u32[]{:S(2)}) collective-permute-start(bf16[2,4,256,128]{3,2,1,0:T(8,128)(2,1)S(1)} %collective-permute-done.24.refs_0_), channel_id=1, source_target_pairs={{0,1},{1,0},{2,3},{3,2},{4,5},{5,4},{6,7},{7,6},{8,9},{9,8},{10,11... | collective-permute-start | bytes 1572872 | tf_op jit(solution)/shard_map/ppermute | solution.py:288
  211.3 25.4 %collective-permute-start.21 = (bf16[2,4,256,128]{3,2,1,0:T(8,128)(2,1)S(1)}, bf16[2,4,256,128]{3,2,1,0:T(8,128)(2,1)S(1)}, u32[]{:S(2)}, u32[]{:S(2)}) collective-permute-start(bf16[2,4,256,128]{3,2,1,0:T(8,128)(2,1)S(1)} %collective-permute-done.20.refs_0_), channel_id=1, source_target_pairs={{0,1},{1,0},{2,3},{3,2},{4,5},{5,4},{6,7},{7,6},{8,9},{9,8},{10,11... | collective-permute-start | bytes 1572872 | tf_op jit(solution)/shard_map/ppermute | solution.py:288
  215.2 23.1 %collective-permute-start.22 = (bf16[2,4,256,128]{3,2,1,0:T(8,128)(2,1)S(1)}, bf16[2,4,256,128]{3,2,1,0:T(8,128)(2,1)S(1)}, u32[]{:S(2)}, u32[]{:S(2)}) collective-permute-start(bf16[2,4,256,128]{3,2,1,0:T(8,128)(2,1)S(1)} %collective-permute-done.20.refs_0_), channel_id=1, source_target_pairs={{0,2},{1,3},{2,0},{3,1},{4,6},{5,7},{6,4},{7,5},{8,10},{9,11},{10,... | collective-permute-start | bytes 1572872 | tf_op jit(solution)/shard_map/ppermute | solution.py:288
  216.7 24.5 %collective-permute-start.18 = (bf16[2,4,256,128]{3,2,1,0:T(8,128)(2,1)S(1)}, bf16[2,4,256,128]{3,2,1,0:T(8,128)(2,1)S(1)}, u32[]{:S(2)}, u32[]{:S(2)}) collective-permute-start(bf16[2,4,256,128]{3,2,1,0:T(8,128)(2,1)S(1)} %collective-permute-done.16.refs_0_), channel_id=1, source_target_pairs={{0,2},{1,3},{2,0},{3,1},{4,6},{5,7},{6,4},{7,5},{8,10},{9,11},{10,... | collective-permute-start | bytes 1572872 | tf_op jit(solution)/shard_map/ppermute | solution.py:288
  217.3 30.7 %collective-permute-start.17 = (bf16[2,4,256,128]{3,2,1,0:T(8,128)(2,1)S(1)}, bf16[2,4,256,128]{3,2,1,0:T(8,128)(2,1)S(1)}, u32[]{:S(2)}, u32[]{:S(2)}) collective-permute-start(bf16[2,4,256,128]{3,2,1,0:T(8,128)(2,1)S(1)} %collective-permute-done.16.refs_0_), channel_id=1, source_target_pairs={{0,1},{1,0},{2,3},{3,2},{4,5},{5,4},{6,7},{7,6},{8,9},{9,8},{10,11... | collective-permute-start | bytes 1572872 | tf_op jit(solution)/shard_map/ppermute | solution.py:288
  225.5 33.7 %collective-permute-start.13 = (bf16[2,4,256,128]{3,2,1,0:T(8,128)(2,1)S(1)}, bf16[2,4,256,128]{3,2,1,0:T(8,128)(2,1)S(1)}, u32[]{:S(2)}, u32[]{:S(2)}) collective-permute-start(bf16[2,4,256,128]{3,2,1,0:T(8,128)(2,1)S(1)} %collective-permute-done.12.refs_0_), channel_id=1, source_target_pairs={{0,1},{1,0},{2,3},{3,2},{4,5},{5,4},{6,7},{7,6},{8,9},{9,8},{10,11... | collective-permute-start | bytes 1572872 | tf_op jit(solution)/shard_map/ppermute | solution.py:288
  236.8 24.0 %collective-permute-start.14 = (bf16[2,4,256,128]{3,2,1,0:T(8,128)(2,1)S(1)}, bf16[2,4,256,128]{3,2,1,0:T(8,128)(2,1)S(1)}, u32[]{:S(2)}, u32[]{:S(2)}) collective-permute-start(bf16[2,4,256,128]{3,2,1,0:T(8,128)(2,1)S(1)} %collective-permute-done.12.refs_0_), channel_id=1, source_target_pairs={{0,2},{1,3},{2,0},{3,1},{4,6},{5,7},{6,4},{7,5},{8,10},{9,11},{10,... | collective-permute-start | bytes 1572872 | tf_op jit(solution)/shard_map/ppermute | solution.py:288
  238.3 25.4 %collective-permute-start.10 = (bf16[2,4,256,128]{3,2,1,0:T(8,128)(2,1)S(1)}, bf16[2,4,256,128]{3,2,1,0:T(8,128)(2,1)S(1)}, u32[]{:S(2)}, u32[]{:S(2)}) collective-permute-start(bf16[2,4,256,128]{3,2,1,0:T(8,128)(2,1)S(1)} %collective-permute-done.8.refs_0_), channel_id=1, source_target_pairs={{0,2},{1,3},{2,0},{3,1},{4,6},{5,7},{6,4},{7,5},{8,10},{9,11},{10,... | collective-permute-start | bytes 1572872 | tf_op jit(solution)/shard_map/ppermute | solution.py:288
  241.2 29.2 %collective-permute-start.9 = (bf16[2,4,256,128]{3,2,1,0:T(8,128)(2,1)S(1)}, bf16[2,4,256,128]{3,2,1,0:T(8,128)(2,1)S(1)}, u32[]{:S(2)}, u32[]{:S(2)}) collective-permute-start(bf16[2,4,256,128]{3,2,1,0:T(8,128)(2,1)S(1)} %collective-permute-done.8.refs_0_), channel_id=1, source_target_pairs={{0,1},{1,0},{2,3},{3,2},{4,5},{5,4},{6,7},{7,6},{8,9},{9,8},{10,11... | collective-permute-start | bytes 1572872 | tf_op jit(solution)/shard_map/ppermute | solution.py:288
  248.0 33.7 %collective-permute-start.5 = (bf16[2,4,256,128]{3,2,1,0:T(8,128)(2,1)S(1)}, bf16[2,4,256,128]{3,2,1,0:T(8,128)(2,1)S(1)}, u32[]{:S(2)}, u32[]{:S(2)}) collective-permute-start(bf16[2,4,256,128]{3,2,1,0:T(8,128)(2,1)S(1)} %collective-permute-done.4.refs_0_), channel_id=1, source_target_pairs={{0,1},{1,0},{2,3},{3,2},{4,5},{5,4},{6,7},{7,6},{8,9},{9,8},{10,11... | collective-permute-start | bytes 1572872 | tf_op jit(solution)/shard_map/ppermute | solution.py:288
  259.2 25.7 %collective-permute-start.6 = (bf16[2,4,256,128]{3,2,1,0:T(8,128)(2,1)S(1)}, bf16[2,4,256,128]{3,2,1,0:T(8,128)(2,1)S(1)}, u32[]{:S(2)}, u32[]{:S(2)}) collective-permute-start(bf16[2,4,256,128]{3,2,1,0:T(8,128)(2,1)S(1)} %collective-permute-done.4.refs_0_), channel_id=1, source_target_pairs={{0,2},{1,3},{2,0},{3,1},{4,6},{5,7},{6,4},{7,5},{8,10},{9,11},{10,... | collective-permute-start | bytes 1572872 | tf_op jit(solution)/shard_map/ppermute | solution.py:288
  260.8 25.4 %collective-permute-start.2 = (bf16[2,4,256,128]{3,2,1,0:T(8,128)(2,1)S(1)}, bf16[2,4,256,128]{3,2,1,0:T(8,128)(2,1)S(1)}, u32[]{:S(2)}, u32[]{:S(2)}) collective-permute-start(bf16[2,4,256,128]{3,2,1,0:T(8,128)(2,1)S(1)} %collective-permute-done.refs_0_), channel_id=1, source_target_pairs={{0,2},{1,3},{2,0},{3,1},{4,6},{5,7},{6,4},{7,5},{8,10},{9,11},{10,... | collective-permute-start | bytes 1572872 | tf_op jit(solution)/shard_map/ppermute | solution.py:288
  263.7 29.2 %collective-permute-start.1 = (bf16[2,4,256,128]{3,2,1,0:T(8,128)(2,1)S(1)}, bf16[2,4,256,128]{3,2,1,0:T(8,128)(2,1)S(1)}, u32[]{:S(2)}, u32[]{:S(2)}) collective-permute-start(bf16[2,4,256,128]{3,2,1,0:T(8,128)(2,1)S(1)} %collective-permute-done.refs_0_), channel_id=1, source_target_pairs={{0,1},{1,0},{2,3},{3,2},{4,5},{5,4},{6,7},{7,6},{8,9},{9,8},{10,11... | collective-permute-start | bytes 1572872 | tf_op jit(solution)/shard_map/ppermute | solution.py:288
  270.5 33.7 %collective-permute-start.27 = (bf16[2,4,256,128]{3,2,1,0:T(8,128)(2,1)S(1)}, bf16[2,4,256,128]{3,2,1,0:T(8,128)(2,1)S(1)}, u32[]{:S(2)}, u32[]{:S(2)}) collective-permute-start(bf16[2,4,256,128]{3,2,1,0:T(8,128)(2,1)S(1)} %collective-permute-done.26.refs_2_), channel_id=1, source_target_pairs={{0,1},{1,0},{2,3},{3,2},{4,5},{5,4},{6,7},{7,6},{8,9},{9,8},{10,11... | collective-permute-start | bytes 1572872 | tf_op jit(solution)/shard_map/ppermute | solution.py:288
  281.9 23.8 %collective-permute-start.23 = (bf16[2,4,256,128]{3,2,1,0:T(8,128)(2,1)S(1)}, bf16[2,4,256,128]{3,2,1,0:T(8,128)(2,1)S(1)}, u32[]{:S(2)}, u32[]{:S(2)}) collective-permute-start(bf16[2,4,256,128]{3,2,1,0:T(8,128)(2,1)S(1)} %collective-permute-done.21.refs_1_), channel_id=1, source_target_pairs={{0,2},{1,3},{2,0},{3,1},{4,6},{5,7},{6,4},{7,5},{8,10},{9,11},{10,... | collective-permute-start | bytes 1572872 | tf_op jit(solution)/shard_map/ppermute | solution.py:288
  285.0 30.4 %collective-permute-start.19 = (bf16[2,4,256,128]{3,2,1,0:T(8,128)(2,1)S(1)}, bf16[2,4,256,128]{3,2,1,0:T(8,128)(2,1)S(1)}, u32[]{:S(2)}, u32[]{:S(2)}) collective-permute-start(bf16[2,4,256,128]{3,2,1,0:T(8,128)(2,1)S(1)} %collective-permute-done.18.refs_2_), channel_id=1, source_target_pairs={{0,1},{1,0},{2,3},{3,2},{4,5},{5,4},{6,7},{7,6},{8,9},{9,8},{10,11... | collective-permute-start | bytes 1572872 | tf_op jit(solution)/shard_map/ppermute | solution.py:288
  286.2 30.7 %collective-permute-start.15 = (bf16[2,4,256,128]{3,2,1,0:T(8,128)(2,1)S(1)}, bf16[2,4,256,128]{3,2,1,0:T(8,128)(2,1)S(1)}, u32[]{:S(2)}, u32[]{:S(2)}) collective-permute-start(bf16[2,4,256,128]{3,2,1,0:T(8,128)(2,1)S(1)} %collective-permute-done.13.refs_1_), channel_id=1, source_target_pairs={{0,2},{1,3},{2,0},{3,1},{4,6},{5,7},{6,4},{7,5},{8,10},{9,11},{10,... | collective-permute-start | bytes 1572872 | tf_op jit(solution)/shard_map/ppermute | solution.py:288
  292.9 33.7 %collective-permute-start.11 = (bf16[2,4,256,128]{3,2,1,0:T(8,128)(2,1)S(1)}, bf16[2,4,256,128]{3,2,1,0:T(8,128)(2,1)S(1)}, u32[]{:S(2)}, u32[]{:S(2)}) collective-permute-start(bf16[2,4,256,128]{3,2,1,0:T(8,128)(2,1)S(1)} %collective-permute-done.10.refs_2_), channel_id=1, source_target_pairs={{0,1},{1,0},{2,3},{3,2},{4,5},{5,4},{6,7},{7,6},{8,9},{9,8},{10,11... | collective-permute-start | bytes 1572872 | tf_op jit(solution)/shard_map/ppermute | solution.py:288
  304.2 25.0 %collective-permute-start.7 = (bf16[2,4,256,128]{3,2,1,0:T(8,128)(2,1)S(1)}, bf16[2,4,256,128]{3,2,1,0:T(8,128)(2,1)}, u32[]{:S(2)}, u32[]{:S(2)}) collective-permute-start(bf16[2,4,256,128]{3,2,1,0:T(8,128)(2,1)S(1)} %collective-permute-done.5.refs_1_), channel_id=1, source_target_pairs={{0,2},{1,3},{2,0},{3,1},{4,6},{5,7},{6,4},{7,5},{8,10},{9,11},{10,... | collective-permute-start | bytes 1572872 | tf_op jit(solution)/shard_map/ppermute | solution.py:288
  305.7 32.2 %collective-permute-start.3 = (bf16[2,4,256,128]{3,2,1,0:T(8,128)(2,1)S(1)}, bf16[2,4,256,128]{3,2,1,0:T(8,128)(2,1)}, u32[]{:S(2)}, u32[]{:S(2)}) collective-permute-start(bf16[2,4,256,128]{3,2,1,0:T(8,128)(2,1)S(1)} %collective-permute-done.2.refs_2_), channel_id=1, source_target_pairs={{0,1},{1,0},{2,3},{3,2},{4,5},{5,4},{6,7},{7,6},{8,9},{9,8},{10,11... | collective-permute-start | bytes 1572872 | tf_op jit(solution)/shard_map/ppermute | solution.py:288
  315.4 72.3 %collective-permute-start.66 = (bf16[4,256,128]{2,1,0:T(8,128)(2,1)}, bf16[4,256,128]{2,1,0:T(8,128)(2,1)}, u32[]{:S(2)}, u32[]{:S(2)}) collective-permute-start(bf16[4,256,128]{2,1,0:T(8,128)(2,1)} %collective-permute-done.64.refs_0_), channel_id=1, source_target_pairs={{0,2},{1,3},{2,0},{3,1},{4,6},{5,7},{6,4},{7,5},{8,10},{9,11},{10,... | collective-permute-start | bytes 786440 | tf_op jit(solution)/shard_map/ppermute | solution.py:288
  316.9 67.8 %collective-permute-start.62 = (bf16[4,256,128]{2,1,0:T(8,128)(2,1)}, bf16[4,256,128]{2,1,0:T(8,128)(2,1)}, u32[]{:S(2)}, u32[]{:S(2)}) collective-permute-start(bf16[4,256,128]{2,1,0:T(8,128)(2,1)} %collective-permute-done.61.refs_2_), channel_id=1, source_target_pairs={{0,1},{1,0},{2,3},{3,2},{4,5},{5,4},{6,7},{7,6},{8,9},{9,8},{10,11... | collective-permute-start | bytes 786440 | tf_op jit(solution)/shard_map/ppermute | solution.py:288
  326.6 61.0 %collective-permute-start.67 = (bf16[4,256,128]{2,1,0:T(8,128)(2,1)}, bf16[4,256,128]{2,1,0:T(8,128)(2,1)}, u32[]{:S(2)}, u32[]{:S(2)}) collective-permute-start(bf16[4,256,128]{2,1,0:T(8,128)(2,1)} %collective-permute-done.65.refs_1_), channel_id=1, source_target_pairs={{0,2},{1,3},{2,0},{3,1},{4,6},{5,7},{6,4},{7,5},{8,10},{9,11},{10,... | collective-permute-start | bytes 786440 | tf_op jit(solution)/shard_map/ppermute | solution.py:288
  329.2 64.6 %collective-permute-start.31 = (bf16[4,256,128]{2,1,0:T(8,128)(2,1)S(1)}, bf16[4,256,128]{2,1,0:T(8,128)(2,1)}, u32[]{:S(2)}, u32[]{:S(2)}) collective-permute-start(bf16[4,256,128]{2,1,0:T(8,128)(2,1)S(1)} %get-tuple-element.88.refs_0_), channel_id=1, source_target_pairs={{0,1},{1,0},{2,3},{3,2},{4,5},{5,4},{6,7},{7,6},{8,9},{9,8},{10,11... | collective-permute-start | bytes 786440 | tf_op jit(solution)/shard_map/ppermute | solution.py:288
  338.0 55.8 %collective-permute-start.33 = (bf16[4,256,128]{2,1,0:T(8,128)(2,1)}, bf16[4,256,128]{2,1,0:T(8,128)(2,1)}, u32[]{:S(2)}, u32[]{:S(2)}) collective-permute-start(bf16[4,256,128]{2,1,0:T(8,128)(2,1)} %collective-permute-done.32.refs_2_), channel_id=1, source_target_pairs={{0,1},{1,0},{2,3},{3,2},{4,5},{5,4},{6,7},{7,6},{8,9},{9,8},{10,11... | collective-permute-start | bytes 786440 | tf_op jit(solution)/shard_map/ppermute | solution.py:288
  390.8 12.5 %collective-permute-start.63 = (bf16[256,256]{1,0:T(8,128)(2,1)S(1)}, bf16[256,256]{1,0:T(8,128)(2,1)S(1)}, u32[]{:S(2)}, u32[]{:S(2)}) collective-permute-start(bf16[256,256]{1,0:T(8,128)(2,1)S(1)} %copy-done.55), channel_id=1, source_target_pairs={{0,20},{4,16},{8,28},{12,24},{16,4},{20,0},{24,12},{28,8},{1,21},{... | collective-permute-start | bytes 393224 | tf_op jit(solution)/shard_map/ppermute | solution.py:284
  390.9 18.1 %collective-permute-start.58 = (bf16[256,256]{1,0:T(8,128)(2,1)}, bf16[256,256]{1,0:T(8,128)(2,1)S(1)}, u32[]{:S(2)}, u32[]{:S(2)}) collective-permute-start(bf16[256,256]{1,0:T(8,128)(2,1)} %get-tuple-element.74), channel_id=1, source_target_pairs={{0,16},{4,20},{8,24},{12,28},{16,0},{20,4},{24,8},{28,12},{1,17},{... | collective-permute-start | bytes 393224 | tf_op jit(solution)/shard_map/ppermute | solution.py:284
  393.8 15.1 %collective-permute-start.53 = (bf16[256,256]{1,0:T(8,128)(2,1)}, bf16[256,256]{1,0:T(8,128)(2,1)S(1)}, u32[]{:S(2)}, u32[]{:S(2)}) collective-permute-start(bf16[256,256]{1,0:T(8,128)(2,1)} %get-tuple-element.72), channel_id=1, source_target_pairs={{0,12},{4,8},{8,20},{12,16},{16,28},{20,24},{24,4},{28,0},{1,13},{... | collective-permute-start | bytes 393224 | tf_op jit(solution)/shard_map/ppermute | solution.py:284
  393.8 17.2 %collective-permute-start.48 = (bf16[256,256]{1,0:T(8,128)(2,1)}, bf16[256,256]{1,0:T(8,128)(2,1)S(1)}, u32[]{:S(2)}, u32[]{:S(2)}) collective-permute-start(bf16[256,256]{1,0:T(8,128)(2,1)} %get-tuple-element.70), channel_id=1, source_target_pairs={{0,28},{4,24},{8,4},{12,0},{16,12},{20,8},{24,20},{28,16},{1,29},{... | collective-permute-start | bytes 393224 | tf_op jit(solution)/shard_map/ppermute | solution.py:284
  397.4 13.7 %collective-permute-start.43 = (bf16[256,256]{1,0:T(8,128)(2,1)}, bf16[256,256]{1,0:T(8,128)(2,1)S(1)}, u32[]{:S(2)}, u32[]{:S(2)}) collective-permute-start(bf16[256,256]{1,0:T(8,128)(2,1)} %get-tuple-element.68), channel_id=1, source_target_pairs={{0,8},{4,12},{8,16},{12,20},{16,24},{20,28},{24,0},{28,4},{1,9},{5... | collective-permute-start | bytes 393224 | tf_op jit(solution)/shard_map/ppermute | solution.py:284
  (61 other events, 4601.7 us)

commit v3 on v2

--- a/solution.py
+++ b/solution.py
@@ -13,7 +13,7 @@
 LANES = 128
 HERE = (0, 0)
 ANYWHERE = pl.BlockSpec(memory_space=pl.ANY)
-ROOM = pltpu.CompilerParams(vmem_limit_bytes=63 * 2**20)
+ROOM = pltpu.CompilerParams(vmem_limit_bytes=67_000_000)
 
 
 def flatten_rows(piece):
@@ -135,6 +135,43 @@
         ],
         compiler_params=ROOM,
     )(norm_gain[None, :], gate_master, up_master)
+
+
+def cast_down_kernel(steps, down_ref, *refs):
+    outs, (down_buf, out_buf, in_sem, out_sem) = refs[: len(steps)], refs[len(steps) :]
+    held = down_buf.shape[1]
+    loads, stores = [], []
+    for i, step in enumerate(steps):
+        experts = pl.ds(receiver(step) * held, held)
+        loads.append(pltpu.make_async_copy(down_ref.at[experts], down_buf.at[i], in_sem.at[i]))
+        loads[i].start()
+    for i, out in enumerate(outs):
+        loads[i].wait()
+        for e in range(held):
+            out_buf[i, e] = down_buf[i, e].astype(jnp.bfloat16)
+        stores.append(pltpu.make_async_copy(out_buf.at[i], out, out_sem.at[i]))
+        stores[i].start()
+    for copy in stores:
+        copy.wait()
+
+
+def cast_down(steps, down_master, held):
+    _, rows, hidden = down_master.shape
+    count = len(steps)
+    piece = jax.ShapeDtypeStruct((held, rows, hidden), jnp.bfloat16)
+    return pl.pallas_call(
+        functools.partial(cast_down_kernel, steps),
+        in_specs=[ANYWHERE],
+        out_specs=[ANYWHERE] * count,
+        out_shape=[piece] * count,
+        scratch_shapes=[
+            pltpu.VMEM((count, *piece.shape), jnp.float32),
+            pltpu.VMEM((count, *piece.shape), jnp.bfloat16),
+            pltpu.SemaphoreType.DMA((count,)),
+            pltpu.SemaphoreType.DMA((count,)),
+        ],
+        compiler_params=ROOM,
+    )(down_master)
 
 
 def column_of(expert, swap, hidden):
@@ -249,30 +286,60 @@
     )(*parts, scaled, *others, *(() if fresh else (out,)))
 
 
-def act_kernel(normed_ref, gate_ref, up_ref, chosen_ref, weight_ref, out_ref):
-    owner = lax.axis_index("fs") * pl.num_programs(0) + pl.program_id(0)
-    picked = jnp.where(chosen_ref[...] == owner, weight_ref[...], 0.0)
-    weight = jnp.sum(picked, axis=1, keepdims=True)
+def ready_kernel(held, prompt_ref, group_ref, inner_ref, route_ref, normed_ref, weight_ref):
+    values = prompt_ref[...].astype(jnp.float32)
+    mean = jnp.mean(values * values, axis=1, keepdims=True)
+    normed_ref[...] = (values * lax.rsqrt(mean + 1e-06)).astype(jnp.bfloat16)
+    chosen = group_ref[...] * EPG + inner_ref[...]
+    for e in range(held):
+        owner = lax.axis_index("fs") * held + e
+        picked = jnp.where(chosen == owner, route_ref[...], 0.0)
+        row = jnp.sum(picked, axis=0, keepdims=True)
+        weight_ref[e] = jnp.broadcast_to(row, (LANES, row.shape[1])).T
+
+
+def ready(prompt, group_choice, inner_choice, route_weight, held):
+    tokens = prompt.shape[0]
+    near = pl.BlockSpec(memory_space=pltpu.VMEM)
+    return pl.pallas_call(
+        functools.partial(ready_kernel, held),
+        in_specs=[near] * 4,
+        out_specs=[near] * 2,
+        out_shape=[
+            jax.ShapeDtypeStruct(prompt.shape, jnp.bfloat16),
+            jax.ShapeDtypeStruct((held, tokens, LANES), jnp.float32),
+        ],
+        compiler_params=ROOM,
+    )(prompt, group_choice[None, :], inner_choice.T, route_weight.T)
+
+
+def act_kernel(normed_ref, gate_ref, up_ref, weight_ref, out_ref):
     normed = normed_ref[...]
     factor = normed.shape[1] ** (-0.5)
     gate = jnp.dot(normed, gate_ref[...], preferred_element_type=jnp.float32) * factor
     up = jnp.dot(normed, up_ref[...], preferred_element_type=jnp.float32) * factor
+    weight = jnp.concatenate([weight_ref[0]] * (gate.shape[1] // LANES), axis=1)
     out_ref[...] = (weight * (gate / (1.0 + jnp.exp(-gate))) * up).astype(jnp.bfloat16)
 
 
-def act(normed, gate_local, up_local, chosen, route_weight, held):
+def act(normed, gate_local, up_local, weight):
     tokens, width = normed.shape
+    held = weight.shape[0]
     block = gate_local.shape[1] // held
-    whole = lambda array: pl.BlockSpec(array.shape, lambda e: (0, 0))
     columns = pl.BlockSpec((width, block), lambda e: (0, e))
     return pl.pallas_call(
         act_kernel,
         grid=(held,),
-        in_specs=[whole(normed), columns, columns, whole(chosen), whole(route_weight)],
+        in_specs=[
+            pl.BlockSpec(normed.shape, lambda e: (0, 0)),
+            columns,
+            columns,
+            pl.BlockSpec((1, tokens, LANES), lambda e: (e, 0, 0)),
+        ],
         out_specs=pl.BlockSpec((tokens, block), lambda e: (0, e)),
         out_shape=jax.ShapeDtypeStruct((tokens, held * block), jnp.bfloat16),
         compiler_params=ROOM,
-    )(normed, gate_local, up_local, chosen, route_weight)
+    )(normed, gate_local, up_local, weight)
 
 
 def fs_send(value, offset, sign):
@@ -295,6 +362,7 @@
         both = [near] if 2 * near == chips else [near, chips - near]
         apart += [(far, core) for core in range(2) for far in both]
     pair = [(False, offset) for offset in [(0, 0), (0, 1)] + apart]
+    apart.sort(key=lambda offset: -min(offset[0], chips - offset[0]))
     return pair + [(True, offset) for offset in apart + [(0, 1), (0, 0)]]
 
 
@@ -318,15 +386,13 @@
     cast = cast_pairs((HERE,), norm_gain, gate_master, up_master, held)
     others = tuple(offset for down, offset in pieces[1:] if not down)
     cast += cast_pairs(others, norm_gain, gate_master, up_master, held)
+    normed, weight = ready(prompt, group_choice, inner_choice, route_weight, held)
+    cast += cast_down(tuple(offset for down, offset in pieces if down), down_master, held)
 
     own, left, right, last = ({}, {}, {}, {})
     turn = turns(pieces)
     for index, (down, step) in enumerate(pieces):
-        if down:
-            cut = lax.dynamic_slice_in_dim(down_master, receiver(step) * held, held, 0)
-            piece = cut.astype(jnp.bfloat16)
-        else:
-            piece = cast[index]
+        piece = cast[index]
         if step != HERE:
             piece = fs_send(piece, step, 1)
         own[index] = piece
@@ -341,8 +407,7 @@
             pair_out = lay_pair(step, parts, pair_out, total)
             continue
         if scaled is None:
-            normed, chosen = normalize(prompt), group_choice[:, None] * EPG + inner_choice
-            scaled = act(normed, *pair_out, chosen, route_weight, held)
+            scaled = act(normed, *pair_out, weight)
         down_out, result = lay_down(
             step, parts, scaled, sums if step == HERE else (), down_out, total
         )

time: 419 us -> 430 us (1.026)
  starting transfers between devices: 77.2 us -> 89.6 us
  Pallas kernels: 63 us -> 70.3 us
  local copies, waits for them, and re-layouts: 6.09 us -> 0.96 us
  other arithmetic: 4.7 us -> 0 us
    pallas_call x1 -> x3, Pallas kernels: 9.77 us -> 17.2 us  [the longest x1 11.1 us: act(): pl.pallas_call(act_kernel, grid=(held,), in_specs=[pl.BlockSpec(normed.sh...]
    ppermute x21, starting transfers between devices: 23.8 us -> 30.3 us  [fs_send(): return lax.ppermute(value, 'fs', pairs)]
    ppermute x48, starting transfers between devices: 53.4 us -> 59.4 us  [tp_swap(): lax.ppermute(value, 'tp', [(i, i ^ step) for i in range(lax.axis_size('tp...]
  transfers between devices with their start and end apart: 69 -> 69, of which waited for: 38 -> 35; matrix products, arithmetic and copies ran while one was open for 1% -> 0% of each run, Pallas kernels for 14% -> 15%
where the time goes in v3:
time: 430 us
  waiting for transfers between devices  268 us (62%)
  starting transfers between devices  89.6 us (21%)
  Pallas kernels  70.3 us (16%)
    ppermute x48, waiting for transfers between devices, tp_swap(): lax.ppermute(value, 'tp', [(i, i ^ step) for i in range(lax.axis_size('tp...  152 us
    ppermute x21, waiting for transfers between devices, fs_send(): return lax.ppermute(value, 'fs', pairs)  116 us
    ppermute x48, starting transfers between devices, tp_swap(): lax.ppermute(value, 'tp', [(i, i ^ step) for i in range(lax.axis_size('tp...  59.4 us
    ppermute x21, starting transfers between devices, fs_send(): return lax.ppermute(value, 'fs', pairs)  30.3 us
    pallas_call x8, Pallas kernels, lay_down(): pl.pallas_call(functools.partial(lay_down_kernel, step, sums, FF ** (-0.5...  24.1 us
    pallas_call x8, Pallas kernels, lay_pair(): pl.pallas_call(functools.partial(lay_pair_kernel, step), in_specs=[ANYWHE...  20.7 us
    pallas_call x1, Pallas kernels, act(): pl.pallas_call(act_kernel, grid=(held,), in_specs=[pl.BlockSpec(normed.sh...  11.1 us
  transfers between devices with their start and end apart: 69, of which 35 were waited for; matrix products, arithmetic and copies ran while one was open for 0% of the time, Pallas kernels for 15%

profile of v3, /device:TPU:0, one launch (start us, length us, event | category | flops | bytes accessed | tf_op | source)
XLA Modules:
  0.0 429.7 jit_solution(8251407931547939130)
XLA Ops:
  0.6 3.3 shard_map.121
  4.0 4.1 collective-permute-start.34
  9.7 2.2 collective-permute-start.49
  11.9 21.3 %collective-permute-done.34.refs_0_ = bf16[4,256,128]{2,1,0:T(8,128)(2,1)} collective-permute-done((bf16[4,256,128]{2,1,0:T(8,128)(2,1)}, bf16[4,256,128]{2,1,0:T(8,128)(2,1)}, u32[]{:S(2)}, u32[]{:S(2)}) %collective-permute-start.34) | collective-permute-done | bytes 262176 | tf_op jit(solution)/shard_map/ppermute | solution.py:351
  33.3 8.8 %collective-permute-done.39.refs_0_ = bf16[4,256,128]{2,1,0:T(8,128)(2,1)} collective-permute-done((bf16[4,256,128]{2,1,0:T(8,128)(2,1)}, bf16[4,256,128]{2,1,0:T(8,128)(2,1)}, u32[]{:S(2)}, u32[]{:S(2)}) %collective-permute-start.39) | collective-permute-done | bytes 262176 | tf_op jit(solution)/shard_map/ppermute | solution.py:351
  43.5 2.7 shard_map.112.refs_0_
  46.3 1.9 collective-permute-start.28
  48.2 5.5 %shard_map.111 = (bf16[2,4,256,128]{3,2,1,0:T(8,128)(2,1)}, bf16[2,4,256,128]{3,2,1,0:T(8,128)(2,1)}, bf16[2,4,256,128]{3,2,1,0:T(8,128)(2,1)}, bf16[2,4,256,128...) custom-call(f32[1,256]{1,0:T(1,128)} %bitcast.5, ...), custom_call_target="tpu_custom_call" | custom-call | tf_op jit(solution)/shard_map/pallas_call | solution.py:124
  55.3 2.7 collective-permute-start.20
  58.5 14.8 %collective-permute-done.32.refs_2_ = bf16[4,256,128]{2,1,0:T(8,128)(2,1)} collective-permute-done((bf16[4,256,128]{2,1,0:T(8,128)(2,1)}, bf16[4,256,128]{2,1,0:T(8,128)(2,1)}, u32[]{:S(2)}, u32[]{:S(2)}) %collective-permute-start.32) | collective-permute-done | bytes 262176 | tf_op jit(solution)/shard_map/ppermute | solution.py:355
  75.0 3.1 collective-permute-start.8
  78.1 2.2 collective-permute-start.4
  80.3 2.1 collective-permute-start
  82.4 7.4 %collective-permute-done.16.refs_0_ = bf16[2,4,256,128]{3,2,1,0:T(8,128)(2,1)S(1)} collective-permute-done((bf16[2,4,256,128]{3,2,1,0:T(8,128)(2,1)}, bf16[2,4,256,128]{3,2,1,0:T(8,128)(2,1)S(1)}, u32[]{:S(2)}, u32[]{:S(2)}) %collective-permute-start.16) | collective-permute-done | bytes 524320 | tf_op jit(solution)/shard_map/ppermute | solution.py:351
  90.3 8.8 %collective-permute-done.12.refs_0_ = bf16[2,4,256,128]{3,2,1,0:T(8,128)(2,1)S(1)} collective-permute-done((bf16[2,4,256,128]{3,2,1,0:T(8,128)(2,1)}, bf16[2,4,256,128]{3,2,1,0:T(8,128)(2,1)S(1)}, u32[]{:S(2)}, u32[]{:S(2)}) %collective-permute-start.12) | collective-permute-done | bytes 524320 | tf_op jit(solution)/shard_map/ppermute | solution.py:351
  100.7 7.8 %collective-permute-done.8.refs_0_ = bf16[2,4,256,128]{3,2,1,0:T(8,128)(2,1)S(1)} collective-permute-done((bf16[2,4,256,128]{3,2,1,0:T(8,128)(2,1)}, bf16[2,4,256,128]{3,2,1,0:T(8,128)(2,1)S(1)}, u32[]{:S(2)}, u32[]{:S(2)}) %collective-permute-start.8) | collective-permute-done | bytes 524320 | tf_op jit(solution)/shard_map/ppermute | solution.py:351
  110.0 36.9 %collective-permute-done.4.refs_0_ = bf16[2,4,256,128]{3,2,1,0:T(8,128)(2,1)S(1)} collective-permute-done((bf16[2,4,256,128]{3,2,1,0:T(8,128)(2,1)}, bf16[2,4,256,128]{3,2,1,0:T(8,128)(2,1)S(1)}, u32[]{:S(2)}, u32[]{:S(2)}) %collective-permute-start.4) | collective-permute-done | bytes 524320 | tf_op jit(solution)/shard_map/ppermute | solution.py:351
  147.4 6.9 %collective-permute-done.refs_0_ = bf16[2,4,256,128]{3,2,1,0:T(8,128)(2,1)S(1)} collective-permute-done((bf16[2,4,256,128]{3,2,1,0:T(8,128)(2,1)}, bf16[2,4,256,128]{3,2,1,0:T(8,128)(2,1)S(1)}, u32[]{:S(2)}, u32[]{:S(2)}) %collective-permute-start) | collective-permute-done | bytes 524320 | tf_op jit(solution)/shard_map/ppermute | solution.py:351
  158.9 4.0 collective-permute-done.45.refs_1_
  165.3 4.1 collective-permute-done.51.refs_2_
  171.4 2.8 collective-permute-done.55.refs_1_
  176.5 4.2 collective-permute-done.61.refs_2_
  182.8 2.7 collective-permute-done.65.refs_1_
  187.8 3.2 collective-permute-done.42.refs_3_
  192.6 21.8 %collective-permute-done.47.refs_3_ = bf16[4,256,128]{2,1,0:T(8,128)(2,1)S(1)} collective-permute-done((bf16[4,256,128]{2,1,0:T(8,128)(2,1)S(1)}, bf16[4,256,128]{2,1,0:T(8,128)(2,1)S(1)}, u32[]{:S(2)}, u32[]{:S(2)}) %collective-permute-start.47) | collective-permute-done | bytes 262176 | tf_op jit(solution)/shard_map/ppermute | solution.py:355
  216.4 3.5 collective-permute-done.57.refs_3_
  223.8 5.2 %collective-permute-done.25.refs_1_ = bf16[2,4,256,128]{3,2,1,0:T(8,128)(2,1)S(1)} collective-permute-done((bf16[2,4,256,128]{3,2,1,0:T(8,128)(2,1)S(1)}, bf16[2,4,256,128]{3,2,1,0:T(8,128)(2,1)S(1)}, u32[]{:S(2)}, u32[]{:S(2)}) %collective-permute-start.25) | collective-permute-done | bytes 524320 | tf_op jit(solution)/shard_map/ppermute | solution.py:355
  230.5 9.7 %collective-permute-done.21.refs_1_ = bf16[2,4,256,128]{3,2,1,0:T(8,128)(2,1)S(1)} collective-permute-done((bf16[2,4,256,128]{3,2,1,0:T(8,128)(2,1)S(1)}, bf16[2,4,256,128]{3,2,1,0:T(8,128)(2,1)S(1)}, u32[]{:S(2)}, u32[]{:S(2)}) %collective-permute-start.21) | collective-permute-done | bytes 524320 | tf_op jit(solution)/shard_map/ppermute | solution.py:355
  242.3 3.7 collective-permute-done.18.refs_2_
  247.5 4.0 collective-permute-done.17.refs_1_
  253.0 9.7 %collective-permute-done.13.refs_1_ = bf16[2,4,256,128]{3,2,1,0:T(8,128)(2,1)S(1)} collective-permute-done((bf16[2,4,256,128]{3,2,1,0:T(8,128)(2,1)S(1)}, bf16[2,4,256,128]{3,2,1,0:T(8,128)(2,1)S(1)}, u32[]{:S(2)}, u32[]{:S(2)}) %collective-permute-start.13) | collective-permute-done | bytes 524320 | tf_op jit(solution)/shard_map/ppermute | solution.py:355
  264.8 3.7 collective-permute-done.10.refs_2_
  269.9 4.0 collective-permute-done.9.refs_1_
  275.5 9.7 %collective-permute-done.5.refs_1_ = bf16[2,4,256,128]{3,2,1,0:T(8,128)(2,1)S(1)} collective-permute-done((bf16[2,4,256,128]{3,2,1,0:T(8,128)(2,1)S(1)}, bf16[2,4,256,128]{3,2,1,0:T(8,128)(2,1)S(1)}, u32[]{:S(2)}, u32[]{:S(2)}) %collective-permute-start.5) | collective-permute-done | bytes 524320 | tf_op jit(solution)/shard_map/ppermute | solution.py:355
  288.2 2.7 collective-permute-done.2.refs_2_
  292.4 4.0 collective-permute-done.1.refs_1_
  297.9 9.7 %collective-permute-done.27.refs_3_ = bf16[2,4,256,128]{3,2,1,0:T(8,128)(2,1)S(1)} collective-permute-done((bf16[2,4,256,128]{3,2,1,0:T(8,128)(2,1)S(1)}, bf16[2,4,256,128]{3,2,1,0:T(8,128)(2,1)S(1)}, u32[]{:S(2)}, u32[]{:S(2)}) %collective-permute-start.27) | collective-permute-done | bytes 524320 | tf_op jit(solution)/shard_map/ppermute | solution.py:355
  310.8 8.1 %collective-permute-done.19.refs_3_ = bf16[2,4,256,128]{3,2,1,0:T(8,128)(2,1)S(1)} collective-permute-done((bf16[2,4,256,128]{3,2,1,0:T(8,128)(2,1)S(1)}, bf16[2,4,256,128]{3,2,1,0:T(8,128)(2,1)S(1)}, u32[]{:S(2)}, u32[]{:S(2)}) %collective-permute-start.19) | collective-permute-done | bytes 524320 | tf_op jit(solution)/shard_map/ppermute | solution.py:355
  322.0 8.1 %collective-permute-done.11.refs_3_ = bf16[2,4,256,128]{3,2,1,0:T(8,128)(2,1)S(1)} collective-permute-done((bf16[2,4,256,128]{3,2,1,0:T(8,128)(2,1)S(1)}, bf16[2,4,256,128]{3,2,1,0:T(8,128)(2,1)S(1)}, u32[]{:S(2)}, u32[]{:S(2)}) %collective-permute-start.11) | collective-permute-done | bytes 524320 | tf_op jit(solution)/shard_map/ppermute | solution.py:355
  333.3 8.1 %collective-permute-done.3.refs_3_ = bf16[2,4,256,128]{3,2,1,0:T(8,128)(2,1)S(1)} collective-permute-done((bf16[2,4,256,128]{3,2,1,0:T(8,128)(2,1)S(1)}, bf16[2,4,256,128]{3,2,1,0:T(8,128)(2,1)S(1)}, u32[]{:S(2)}, u32[]{:S(2)}) %collective-permute-start.3) | collective-permute-done | bytes 524320 | tf_op jit(solution)/shard_map/ppermute | solution.py:355
  343.0 2.8 shard_map.122
  345.7 2.6 shard_map.113
  348.3 2.6 shard_map.114
  350.9 2.6 shard_map.115
  353.5 2.6 shard_map.116
  356.1 2.6 shard_map.117
  358.7 2.6 shard_map.118
  361.3 2.6 shard_map.119
  363.9 2.6 shard_map.120
  366.5 11.1 %shard_map.123.refs_4_ = bf16[256,2048]{1,0:T(8,128)(2,1)} custom-call(bf16[256,2048]{1,0:T(8,128)(2,1)} %get-tuple-element.77.normed_ref, bf16[2048,2048]{1,0:T(8,128)(2,1)} %get-tuple-element.49.gate_ref, bf16[2048,2048]{1,0:T(8,128)(2,1)} %get-tuple-element.50.up_ref, f32[4,256,128]{2,1,0:T(8,128)} %get-tuple-element.78.weight_ref), custom_call_target="tpu_custom_call" | custom-call | tf_op jit(solution)/shard_map/pallas_call | solution.py:330
  377.6 2.9 shard_map.124
  380.6 3.0 shard_map.125
  383.5 2.9 shard_map.126
  386.5 3.0 shard_map.127
  389.4 3.0 shard_map.128
  392.4 3.0 shard_map.129
  395.4 3.0 shard_map.130
  398.6 3.5 collective-permute-start.58
  402.1 3.8 collective-permute-start.48
  406.0 2.3 collective-permute-start.38
  408.3 4.4 %collective-permute-done.53.refs_8_ = bf16[256,256]{1,0:T(8,128)(2,1)} collective-permute-done((bf16[256,256]{1,0:T(8,128)(2,1)}, bf16[256,256]{1,0:T(8,128)(2,1)}, u32[]{:S(2)}, u32[]{:S(2)}) %collective-permute-start.53) | collective-permute-done | bytes 131104 | tf_op jit(solution)/shard_map/ppermute | solution.py:351
  413.5 9.8 %collective-permute-done.43.refs_6_ = bf16[256,256]{1,0:T(8,128)(2,1)} collective-permute-done((bf16[256,256]{1,0:T(8,128)(2,1)}, bf16[256,256]{1,0:T(8,128)(2,1)}, u32[]{:S(2)}, u32[]{:S(2)}) %collective-permute-start.43) | collective-permute-done | bytes 131104 | tf_op jit(solution)/shard_map/ppermute | solution.py:351
  423.3 2.8 collective-permute-done.38.refs_5_
  426.1 3.5 shard_map.131
  (181 shorter events, 63.6 us)
Async XLA Ops:
  4.0 29.3 %collective-permute-start.34 = (bf16[4,256,128]{2,1,0:T(8,128)(2,1)}, bf16[4,256,128]{2,1,0:T(8,128)(2,1)}, u32[]{:S(2)}, u32[]{:S(2)}) collective-permute-start(bf16[4,256,128]{2,1,0:T(8,128)(2,1)} %get-tuple-element.79), channel_id=1, source_target_pairs={{0,16},{4,20},{8,24},{12,28},{16,0},{20,4},{24,8},{28,12},{1,17},{... | collective-permute-start | bytes 786440 | tf_op jit(solution)/shard_map/ppermute | solution.py:351
  8.1 34.0 %collective-permute-start.39 = (bf16[4,256,128]{2,1,0:T(8,128)(2,1)}, bf16[4,256,128]{2,1,0:T(8,128)(2,1)}, u32[]{:S(2)}, u32[]{:S(2)}) collective-permute-start(bf16[4,256,128]{2,1,0:T(8,128)(2,1)} %get-tuple-element.81), channel_id=1, source_target_pairs={{0,20},{4,16},{8,28},{12,24},{16,4},{20,0},{24,12},{28,8},{1,21},{... | collective-permute-start | bytes 786440 | tf_op jit(solution)/shard_map/ppermute | solution.py:351
  8.1 38.2 %collective-permute-start.44 = (bf16[4,256,128]{2,1,0:T(8,128)(2,1)}, bf16[4,256,128]{2,1,0:T(8,128)(2,1)}, u32[]{:S(2)}, u32[]{:S(2)}) collective-permute-start(bf16[4,256,128]{2,1,0:T(8,128)(2,1)} %get-tuple-element.84), channel_id=1, source_target_pairs={{0,8},{4,12},{8,16},{12,20},{16,24},{20,28},{24,0},{28,4},{1,9},{5... | collective-permute-start | bytes 786440 | tf_op jit(solution)/shard_map/ppermute | solution.py:351
  9.7 44.0 %collective-permute-start.49 = (bf16[4,256,128]{2,1,0:T(8,128)(2,1)}, bf16[4,256,128]{2,1,0:T(8,128)(2,1)}, u32[]{:S(2)}, u32[]{:S(2)}) collective-permute-start(bf16[4,256,128]{2,1,0:T(8,128)(2,1)} %get-tuple-element.87), channel_id=1, source_target_pairs={{0,24},{4,28},{8,0},{12,4},{16,8},{20,12},{24,16},{28,20},{1,25},{... | collective-permute-start | bytes 786440 | tf_op jit(solution)/shard_map/ppermute | solution.py:351
  11.9 43.4 %collective-permute-start.54 = (bf16[4,256,128]{2,1,0:T(8,128)(2,1)}, bf16[4,256,128]{2,1,0:T(8,128)(2,1)}, u32[]{:S(2)}, u32[]{:S(2)}) collective-permute-start(bf16[4,256,128]{2,1,0:T(8,128)(2,1)} %get-tuple-element.90), channel_id=1, source_target_pairs={{0,12},{4,8},{8,20},{12,16},{16,28},{20,24},{24,4},{28,0},{1,13},{... | collective-permute-start | bytes 786440 | tf_op jit(solution)/shard_map/ppermute | solution.py:351
  33.3 22.0 %collective-permute-start.59 = (bf16[4,256,128]{2,1,0:T(8,128)(2,1)}, bf16[4,256,128]{2,1,0:T(8,128)(2,1)}, u32[]{:S(2)}, u32[]{:S(2)}) collective-permute-start(bf16[4,256,128]{2,1,0:T(8,128)(2,1)} %get-tuple-element.93), channel_id=1, source_target_pairs={{0,28},{4,24},{8,4},{12,0},{16,12},{20,8},{24,20},{28,16},{1,29},{... | collective-permute-start | bytes 786440 | tf_op jit(solution)/shard_map/ppermute | solution.py:351
  42.1 15.9 %collective-permute-start.64 = (bf16[4,256,128]{2,1,0:T(8,128)(2,1)}, bf16[4,256,128]{2,1,0:T(8,128)(2,1)}, u32[]{:S(2)}, u32[]{:S(2)}) collective-permute-start(bf16[4,256,128]{2,1,0:T(8,128)(2,1)} %get-tuple-element.96), channel_id=1, source_target_pairs={{0,4},{4,0},{8,12},{12,8},{16,20},{20,16},{24,28},{28,24},{1,5},{5... | collective-permute-start | bytes 786440 | tf_op jit(solution)/shard_map/ppermute | solution.py:351
  46.3 27.0 %collective-permute-start.28 = (bf16[2,4,256,128]{3,2,1,0:T(8,128)(2,1)}, bf16[2,4,256,128]{3,2,1,0:T(8,128)(2,1)}, u32[]{:S(2)}, u32[]{:S(2)}) collective-permute-start(bf16[2,4,256,128]{3,2,1,0:T(8,128)(2,1)} %shard_map.112.refs_0_), channel_id=1, source_target_pairs={{0,1},{1,0},{2,3},{3,2},{4,5},{5,4},{6,7},{7,6},{8,9},{9,8},{10,11... | collective-permute-start | bytes 1572872 | tf_op jit(solution)/shard_map/ppermute | solution.py:355
  53.7 20.5 %collective-permute-start.29 = (bf16[2,4,256,128]{3,2,1,0:T(8,128)(2,1)}, bf16[2,4,256,128]{3,2,1,0:T(8,128)(2,1)S(1)}, u32[]{:S(2)}, u32[]{:S(2)}) collective-permute-start(bf16[2,4,256,128]{3,2,1,0:T(8,128)(2,1)} %shard_map.112.refs_0_), channel_id=1, source_target_pairs={{0,2},{1,3},{2,0},{3,1},{4,6},{5,7},{6,4},{7,5},{8,10},{9,11},{10,... | collective-permute-start | bytes 1572872 | tf_op jit(solution)/shard_map/ppermute | solution.py:355
  55.3 22.8 %collective-permute-start.24 = (bf16[2,4,256,128]{3,2,1,0:T(8,128)(2,1)}, bf16[2,4,256,128]{3,2,1,0:T(8,128)(2,1)S(1)}, u32[]{:S(2)}, u32[]{:S(2)}) collective-permute-start(bf16[2,4,256,128]{3,2,1,0:T(8,128)(2,1)} %get-tuple-element.59), channel_id=1, source_target_pairs={{0,4},{4,0},{8,12},{12,8},{16,20},{20,16},{24,28},{28,24},{1,5},{5... | collective-permute-start | bytes 1572872 | tf_op jit(solution)/shard_map/ppermute | solution.py:351
  55.3 25.0 %collective-permute-start.20 = (bf16[2,4,256,128]{3,2,1,0:T(8,128)(2,1)}, bf16[2,4,256,128]{3,2,1,0:T(8,128)(2,1)S(1)}, u32[]{:S(2)}, u32[]{:S(2)}) collective-permute-start(bf16[2,4,256,128]{3,2,1,0:T(8,128)(2,1)} %get-tuple-element.58), channel_id=1, source_target_pairs={{0,8},{4,12},{8,16},{12,20},{16,24},{20,28},{24,0},{28,4},{1,9},{5... | collective-permute-start | bytes 1572872 | tf_op jit(solution)/shard_map/ppermute | solution.py:351
  58.0 15.3 %collective-permute-start.32 = (bf16[4,256,128]{2,1,0:T(8,128)(2,1)}, bf16[4,256,128]{2,1,0:T(8,128)(2,1)}, u32[]{:S(2)}, u32[]{:S(2)}) collective-permute-start(bf16[4,256,128]{2,1,0:T(8,128)(2,1)} %get-tuple-element.76.refs_0_), channel_id=1, source_target_pairs={{0,2},{1,3},{2,0},{3,1},{4,6},{5,7},{6,4},{7,5},{8,10},{9,11},{10,... | collective-permute-start | bytes 786440 | tf_op jit(solution)/shard_map/ppermute | solution.py:355
  73.2 16.5 %collective-permute-start.16 = (bf16[2,4,256,128]{3,2,1,0:T(8,128)(2,1)}, bf16[2,4,256,128]{3,2,1,0:T(8,128)(2,1)S(1)}, u32[]{:S(2)}, u32[]{:S(2)}) collective-permute-start(bf16[2,4,256,128]{3,2,1,0:T(8,128)(2,1)} %get-tuple-element.57), channel_id=1, source_target_pairs={{0,24},{4,28},{8,0},{12,4},{16,8},{20,12},{24,16},{28,20},{1,25},{... | collective-permute-start | bytes 1572872 | tf_op jit(solution)/shard_map/ppermute | solution.py:351
  73.3 25.9 %collective-permute-start.12 = (bf16[2,4,256,128]{3,2,1,0:T(8,128)(2,1)}, bf16[2,4,256,128]{3,2,1,0:T(8,128)(2,1)S(1)}, u32[]{:S(2)}, u32[]{:S(2)}) collective-permute-start(bf16[2,4,256,128]{3,2,1,0:T(8,128)(2,1)} %get-tuple-element.56), channel_id=1, source_target_pairs={{0,12},{4,8},{8,20},{12,16},{16,28},{20,24},{24,4},{28,0},{1,13},{... | collective-permute-start | bytes 1572872 | tf_op jit(solution)/shard_map/ppermute | solution.py:351
  75.0 33.4 %collective-permute-start.8 = (bf16[2,4,256,128]{3,2,1,0:T(8,128)(2,1)}, bf16[2,4,256,128]{3,2,1,0:T(8,128)(2,1)S(1)}, u32[]{:S(2)}, u32[]{:S(2)}) collective-permute-start(bf16[2,4,256,128]{3,2,1,0:T(8,128)(2,1)} %get-tuple-element.55), channel_id=1, source_target_pairs={{0,28},{4,24},{8,4},{12,0},{16,12},{20,8},{24,20},{28,16},{1,29},{... | collective-permute-start | bytes 1572872 | tf_op jit(solution)/shard_map/ppermute | solution.py:351
  78.1 68.8 %collective-permute-start.4 = (bf16[2,4,256,128]{3,2,1,0:T(8,128)(2,1)}, bf16[2,4,256,128]{3,2,1,0:T(8,128)(2,1)S(1)}, u32[]{:S(2)}, u32[]{:S(2)}) collective-permute-start(bf16[2,4,256,128]{3,2,1,0:T(8,128)(2,1)} %get-tuple-element.54), channel_id=1, source_target_pairs={{0,16},{4,20},{8,24},{12,28},{16,0},{20,4},{24,8},{28,12},{1,17},{... | collective-permute-start | bytes 1572872 | tf_op jit(solution)/shard_map/ppermute | solution.py:351
  80.3 74.0 %collective-permute-start = (bf16[2,4,256,128]{3,2,1,0:T(8,128)(2,1)}, bf16[2,4,256,128]{3,2,1,0:T(8,128)(2,1)S(1)}, u32[]{:S(2)}, u32[]{:S(2)}) collective-permute-start(bf16[2,4,256,128]{3,2,1,0:T(8,128)(2,1)} %get-tuple-element.53), channel_id=1, source_target_pairs={{0,20},{4,16},{8,28},{12,24},{16,4},{20,0},{24,12},{28,8},{1,21},{... | collective-permute-start | bytes 1572872 | tf_op jit(solution)/shard_map/ppermute | solution.py:351
  89.8 65.1 %collective-permute-start.35 = (bf16[4,256,128]{2,1,0:T(8,128)(2,1)}, bf16[4,256,128]{2,1,0:T(8,128)(2,1)S(1)}, u32[]{:S(2)}, u32[]{:S(2)}) collective-permute-start(bf16[4,256,128]{2,1,0:T(8,128)(2,1)} %collective-permute-done.34.refs_0_), channel_id=1, source_target_pairs={{0,1},{1,0},{2,3},{3,2},{4,5},{5,4},{6,7},{7,6},{8,9},{9,8},{10,11... | collective-permute-start | bytes 786440 | tf_op jit(solution)/shard_map/ppermute | solution.py:355
  99.1 57.2 %collective-permute-start.36 = (bf16[4,256,128]{2,1,0:T(8,128)(2,1)}, bf16[4,256,128]{2,1,0:T(8,128)(2,1)}, u32[]{:S(2)}, u32[]{:S(2)}) collective-permute-start(bf16[4,256,128]{2,1,0:T(8,128)(2,1)} %collective-permute-done.34.refs_0_), channel_id=1, source_target_pairs={{0,2},{1,3},{2,0},{3,1},{4,6},{5,7},{6,4},{7,5},{8,10},{9,11},{10,... | collective-permute-start | bytes 786440 | tf_op jit(solution)/shard_map/ppermute | solution.py:355
  108.4 48.4 %collective-permute-start.41 = (bf16[4,256,128]{2,1,0:T(8,128)(2,1)}, bf16[4,256,128]{2,1,0:T(8,128)(2,1)S(1)}, u32[]{:S(2)}, u32[]{:S(2)}) collective-permute-start(bf16[4,256,128]{2,1,0:T(8,128)(2,1)} %collective-permute-done.39.refs_0_), channel_id=1, source_target_pairs={{0,2},{1,3},{2,0},{3,1},{4,6},{5,7},{6,4},{7,5},{8,10},{9,11},{10,... | collective-permute-start | bytes 786440 | tf_op jit(solution)/shard_map/ppermute | solution.py:355
  146.9 11.5 %collective-permute-start.40 = (bf16[4,256,128]{2,1,0:T(8,128)(2,1)}, bf16[4,256,128]{2,1,0:T(8,128)(2,1)S(1)}, u32[]{:S(2)}, u32[]{:S(2)}) collective-permute-start(bf16[4,256,128]{2,1,0:T(8,128)(2,1)} %collective-permute-done.39.refs_0_), channel_id=1, source_target_pairs={{0,1},{1,0},{2,3},{3,2},{4,5},{5,4},{6,7},{7,6},{8,9},{9,8},{10,11... | collective-permute-start | bytes 786440 | tf_op jit(solution)/shard_map/ppermute | solution.py:355
  156.4 13.0 %collective-permute-start.51 = (bf16[4,256,128]{2,1,0:T(8,128)(2,1)}, bf16[4,256,128]{2,1,0:T(8,128)(2,1)S(1)}, u32[]{:S(2)}, u32[]{:S(2)}) collective-permute-start(bf16[4,256,128]{2,1,0:T(8,128)(2,1)} %collective-permute-done.49.refs_0_), channel_id=1, source_target_pairs={{0,2},{1,3},{2,0},{3,1},{4,6},{5,7},{6,4},{7,5},{8,10},{9,11},{10,... | collective-permute-start | bytes 786440 | tf_op jit(solution)/shard_map/ppermute | solution.py:355
  156.9 14.0 %collective-permute-start.50 = (bf16[4,256,128]{2,1,0:T(8,128)(2,1)}, bf16[4,256,128]{2,1,0:T(8,128)(2,1)S(1)}, u32[]{:S(2)}, u32[]{:S(2)}) collective-permute-start(bf16[4,256,128]{2,1,0:T(8,128)(2,1)} %collective-permute-done.49.refs_0_), channel_id=1, source_target_pairs={{0,1},{1,0},{2,3},{3,2},{4,5},{5,4},{6,7},{7,6},{8,9},{9,8},{10,11... | collective-permute-start | bytes 786440 | tf_op jit(solution)/shard_map/ppermute | solution.py:355
  158.4 15.8 %collective-permute-start.55 = (bf16[4,256,128]{2,1,0:T(8,128)(2,1)}, bf16[4,256,128]{2,1,0:T(8,128)(2,1)S(1)}, u32[]{:S(2)}, u32[]{:S(2)}) collective-permute-start(bf16[4,256,128]{2,1,0:T(8,128)(2,1)} %collective-permute-done.54.refs_0_), channel_id=1, source_target_pairs={{0,1},{1,0},{2,3},{3,2},{4,5},{5,4},{6,7},{7,6},{8,9},{9,8},{10,11... | collective-permute-start | bytes 786440 | tf_op jit(solution)/shard_map/ppermute | solution.py:355
  162.9 12.8 %collective-permute-start.56 = (bf16[4,256,128]{2,1,0:T(8,128)(2,1)}, bf16[4,256,128]{2,1,0:T(8,128)(2,1)S(1)}, u32[]{:S(2)}, u32[]{:S(2)}) collective-permute-start(bf16[4,256,128]{2,1,0:T(8,128)(2,1)} %collective-permute-done.54.refs_0_), channel_id=1, source_target_pairs={{0,2},{1,3},{2,0},{3,1},{4,6},{5,7},{6,4},{7,5},{8,10},{9,11},{10,... | collective-permute-start | bytes 786440 | tf_op jit(solution)/shard_map/ppermute | solution.py:355
  164.5 16.3 %collective-permute-start.61 = (bf16[4,256,128]{2,1,0:T(8,128)(2,1)}, bf16[4,256,128]{2,1,0:T(8,128)(2,1)}, u32[]{:S(2)}, u32[]{:S(2)}) collective-permute-start(bf16[4,256,128]{2,1,0:T(8,128)(2,1)} %collective-permute-done.59.refs_0_), channel_id=1, source_target_pairs={{0,2},{1,3},{2,0},{3,1},{4,6},{5,7},{6,4},{7,5},{8,10},{9,11},{10,... | collective-permute-start | bytes 786440 | tf_op jit(solution)/shard_map/ppermute | solution.py:355
  169.4 12.9 %collective-permute-start.60 = (bf16[4,256,128]{2,1,0:T(8,128)(2,1)}, bf16[4,256,128]{2,1,0:T(8,128)(2,1)S(1)}, u32[]{:S(2)}, u32[]{:S(2)}) collective-permute-start(bf16[4,256,128]{2,1,0:T(8,128)(2,1)} %collective-permute-done.59.refs_0_), channel_id=1, source_target_pairs={{0,1},{1,0},{2,3},{3,2},{4,5},{5,4},{6,7},{7,6},{8,9},{9,8},{10,11... | collective-permute-start | bytes 786440 | tf_op jit(solution)/shard_map/ppermute | solution.py:355
  170.9 14.6 %collective-permute-start.65 = (bf16[4,256,128]{2,1,0:T(8,128)(2,1)}, bf16[4,256,128]{2,1,0:T(8,128)(2,1)}, u32[]{:S(2)}, u32[]{:S(2)}) collective-permute-start(bf16[4,256,128]{2,1,0:T(8,128)(2,1)} %collective-permute-done.64.refs_0_), channel_id=1, source_target_pairs={{0,1},{1,0},{2,3},{3,2},{4,5},{5,4},{6,7},{7,6},{8,9},{9,8},{10,11... | collective-permute-start | bytes 786440 | tf_op jit(solution)/shard_map/ppermute | solution.py:355
  174.2 12.9 %collective-permute-start.37 = (bf16[4,256,128]{2,1,0:T(8,128)(2,1)S(1)}, bf16[4,256,128]{2,1,0:T(8,128)(2,1)}, u32[]{:S(2)}, u32[]{:S(2)}) collective-permute-start(bf16[4,256,128]{2,1,0:T(8,128)(2,1)S(1)} %collective-permute-done.35.refs_1_), channel_id=1, source_target_pairs={{0,2},{1,3},{2,0},{3,1},{4,6},{5,7},{6,4},{7,5},{8,10},{9,11},{10,... | collective-permute-start | bytes 786440 | tf_op jit(solution)/shard_map/ppermute | solution.py:355
  175.7 15.3 %collective-permute-start.42 = (bf16[4,256,128]{2,1,0:T(8,128)(2,1)S(1)}, bf16[4,256,128]{2,1,0:T(8,128)(2,1)S(1)}, u32[]{:S(2)}, u32[]{:S(2)}) collective-permute-start(bf16[4,256,128]{2,1,0:T(8,128)(2,1)S(1)} %collective-permute-done.41.refs_2_), channel_id=1, source_target_pairs={{0,1},{1,0},{2,3},{3,2},{4,5},{5,4},{6,7},{7,6},{8,9},{9,8},{10,11... | collective-permute-start | bytes 786440 | tf_op jit(solution)/shard_map/ppermute | solution.py:355
  180.7 40.7 %collective-permute-start.30 = (bf16[2,4,256,128]{3,2,1,0:T(8,128)(2,1)}, bf16[2,4,256,128]{3,2,1,0:T(8,128)(2,1)}, u32[]{:S(2)}, u32[]{:S(2)}) collective-permute-start(bf16[2,4,256,128]{3,2,1,0:T(8,128)(2,1)} %collective-permute-done.28.refs_1_), channel_id=1, source_target_pairs={{0,2},{1,3},{2,0},{3,1},{4,6},{5,7},{6,4},{7,5},{8,10},{9,11},{10,... | collective-permute-start | bytes 1572872 | tf_op jit(solution)/shard_map/ppermute | solution.py:355
  182.3 39.9 %collective-permute-start.26 = (bf16[2,4,256,128]{3,2,1,0:T(8,128)(2,1)S(1)}, bf16[2,4,256,128]{3,2,1,0:T(8,128)(2,1)S(1)}, u32[]{:S(2)}, u32[]{:S(2)}) collective-permute-start(bf16[2,4,256,128]{3,2,1,0:T(8,128)(2,1)S(1)} %collective-permute-done.24.refs_0_), channel_id=1, source_target_pairs={{0,2},{1,3},{2,0},{3,1},{4,6},{5,7},{6,4},{7,5},{8,10},{9,11},{10,... | collective-permute-start | bytes 1572872 | tf_op jit(solution)/shard_map/ppermute | solution.py:355
  185.5 28.8 %collective-permute-start.47 = (bf16[4,256,128]{2,1,0:T(8,128)(2,1)S(1)}, bf16[4,256,128]{2,1,0:T(8,128)(2,1)S(1)}, u32[]{:S(2)}, u32[]{:S(2)}) collective-permute-start(bf16[4,256,128]{2,1,0:T(8,128)(2,1)S(1)} %collective-permute-done.45.refs_1_), channel_id=1, source_target_pairs={{0,2},{1,3},{2,0},{3,1},{4,6},{5,7},{6,4},{7,5},{8,10},{9,11},{10,... | collective-permute-start | bytes 786440 | tf_op jit(solution)/shard_map/ppermute | solution.py:355
  187.0 28.8 %collective-permute-start.52 = (bf16[4,256,128]{2,1,0:T(8,128)(2,1)S(1)}, bf16[4,256,128]{2,1,0:T(8,128)(2,1)S(1)}, u32[]{:S(2)}, u32[]{:S(2)}) collective-permute-start(bf16[4,256,128]{2,1,0:T(8,128)(2,1)S(1)} %collective-permute-done.51.refs_2_), channel_id=1, source_target_pairs={{0,1},{1,0},{2,3},{3,2},{4,5},{5,4},{6,7},{7,6},{8,9},{9,8},{10,11... | collective-permute-start | bytes 786440 | tf_op jit(solution)/shard_map/ppermute | solution.py:355
  191.0 28.9 %collective-permute-start.57 = (bf16[4,256,128]{2,1,0:T(8,128)(2,1)S(1)}, bf16[4,256,128]{2,1,0:T(8,128)(2,1)S(1)}, u32[]{:S(2)}, u32[]{:S(2)}) collective-permute-start(bf16[4,256,128]{2,1,0:T(8,128)(2,1)S(1)} %collective-permute-done.55.refs_1_), channel_id=1, source_target_pairs={{0,2},{1,3},{2,0},{3,1},{4,6},{5,7},{6,4},{7,5},{8,10},{9,11},{10,... | collective-permute-start | bytes 786440 | tf_op jit(solution)/shard_map/ppermute | solution.py:355
  214.3 14.7 %collective-permute-start.25 = (bf16[2,4,256,128]{3,2,1,0:T(8,128)(2,1)S(1)}, bf16[2,4,256,128]{3,2,1,0:T(8,128)(2,1)S(1)}, u32[]{:S(2)}, u32[]{:S(2)}) collective-permute-start(bf16[2,4,256,128]{3,2,1,0:T(8,128)(2,1)S(1)} %collective-permute-done.24.refs_0_), channel_id=1, source_target_pairs={{0,1},{1,0},{2,3},{3,2},{4,5},{5,4},{6,7},{7,6},{8,9},{9,8},{10,11... | collective-permute-start | bytes 1572872 | tf_op jit(solution)/shard_map/ppermute | solution.py:355
  215.8 24.4 %collective-permute-start.21 = (bf16[2,4,256,128]{3,2,1,0:T(8,128)(2,1)S(1)}, bf16[2,4,256,128]{3,2,1,0:T(8,128)(2,1)S(1)}, u32[]{:S(2)}, u32[]{:S(2)}) collective-permute-start(bf16[2,4,256,128]{3,2,1,0:T(8,128)(2,1)S(1)} %collective-permute-done.20.refs_0_), channel_id=1, source_target_pairs={{0,1},{1,0},{2,3},{3,2},{4,5},{5,4},{6,7},{7,6},{8,9},{9,8},{10,11... | collective-permute-start | bytes 1572872 | tf_op jit(solution)/shard_map/ppermute | solution.py:355
  219.9 21.8 %collective-permute-start.22 = (bf16[2,4,256,128]{3,2,1,0:T(8,128)(2,1)S(1)}, bf16[2,4,256,128]{3,2,1,0:T(8,128)(2,1)S(1)}, u32[]{:S(2)}, u32[]{:S(2)}) collective-permute-start(bf16[2,4,256,128]{3,2,1,0:T(8,128)(2,1)S(1)} %collective-permute-done.20.refs_0_), channel_id=1, source_target_pairs={{0,2},{1,3},{2,0},{3,1},{4,6},{5,7},{6,4},{7,5},{8,10},{9,11},{10,... | collective-permute-start | bytes 1572872 | tf_op jit(solution)/shard_map/ppermute | solution.py:355
  221.5 24.5 %collective-permute-start.18 = (bf16[2,4,256,128]{3,2,1,0:T(8,128)(2,1)S(1)}, bf16[2,4,256,128]{3,2,1,0:T(8,128)(2,1)S(1)}, u32[]{:S(2)}, u32[]{:S(2)}) collective-permute-start(bf16[2,4,256,128]{3,2,1,0:T(8,128)(2,1)S(1)} %collective-permute-done.16.refs_0_), channel_id=1, source_target_pairs={{0,2},{1,3},{2,0},{3,1},{4,6},{5,7},{6,4},{7,5},{8,10},{9,11},{10,... | collective-permute-start | bytes 1572872 | tf_op jit(solution)/shard_map/ppermute | solution.py:355
  222.2 29.3 %collective-permute-start.17 = (bf16[2,4,256,128]{3,2,1,0:T(8,128)(2,1)S(1)}, bf16[2,4,256,128]{3,2,1,0:T(8,128)(2,1)S(1)}, u32[]{:S(2)}, u32[]{:S(2)}) collective-permute-start(bf16[2,4,256,128]{3,2,1,0:T(8,128)(2,1)S(1)} %collective-permute-done.16.refs_0_), channel_id=1, source_target_pairs={{0,1},{1,0},{2,3},{3,2},{4,5},{5,4},{6,7},{7,6},{8,9},{9,8},{10,11... | collective-permute-start | bytes 1572872 | tf_op jit(solution)/shard_map/ppermute | solution.py:355
  229.0 33.7 %collective-permute-start.13 = (bf16[2,4,256,128]{3,2,1,0:T(8,128)(2,1)S(1)}, bf16[2,4,256,128]{3,2,1,0:T(8,128)(2,1)S(1)}, u32[]{:S(2)}, u32[]{:S(2)}) collective-permute-start(bf16[2,4,256,128]{3,2,1,0:T(8,128)(2,1)S(1)} %collective-permute-done.12.refs_0_), channel_id=1, source_target_pairs={{0,1},{1,0},{2,3},{3,2},{4,5},{5,4},{6,7},{7,6},{8,9},{9,8},{10,11... | collective-permute-start | bytes 1572872 | tf_op jit(solution)/shard_map/ppermute | solution.py:355
  240.3 24.0 %collective-permute-start.14 = (bf16[2,4,256,128]{3,2,1,0:T(8,128)(2,1)S(1)}, bf16[2,4,256,128]{3,2,1,0:T(8,128)(2,1)S(1)}, u32[]{:S(2)}, u32[]{:S(2)}) collective-permute-start(bf16[2,4,256,128]{3,2,1,0:T(8,128)(2,1)S(1)} %collective-permute-done.12.refs_0_), channel_id=1, source_target_pairs={{0,2},{1,3},{2,0},{3,1},{4,6},{5,7},{6,4},{7,5},{8,10},{9,11},{10,... | collective-permute-start | bytes 1572872 | tf_op jit(solution)/shard_map/ppermute | solution.py:355
  241.8 26.7 %collective-permute-start.10 = (bf16[2,4,256,128]{3,2,1,0:T(8,128)(2,1)S(1)}, bf16[2,4,256,128]{3,2,1,0:T(8,128)(2,1)S(1)}, u32[]{:S(2)}, u32[]{:S(2)}) collective-permute-start(bf16[2,4,256,128]{3,2,1,0:T(8,128)(2,1)S(1)} %collective-permute-done.8.refs_0_), channel_id=1, source_target_pairs={{0,2},{1,3},{2,0},{3,1},{4,6},{5,7},{6,4},{7,5},{8,10},{9,11},{10,... | collective-permute-start | bytes 1572872 | tf_op jit(solution)/shard_map/ppermute | solution.py:355
  246.0 28.0 %collective-permute-start.9 = (bf16[2,4,256,128]{3,2,1,0:T(8,128)(2,1)S(1)}, bf16[2,4,256,128]{3,2,1,0:T(8,128)(2,1)S(1)}, u32[]{:S(2)}, u32[]{:S(2)}) collective-permute-start(bf16[2,4,256,128]{3,2,1,0:T(8,128)(2,1)S(1)} %collective-permute-done.8.refs_0_), channel_id=1, source_target_pairs={{0,1},{1,0},{2,3},{3,2},{4,5},{5,4},{6,7},{7,6},{8,9},{9,8},{10,11... | collective-permute-start | bytes 1572872 | tf_op jit(solution)/shard_map/ppermute | solution.py:355
  251.5 33.7 %collective-permute-start.5 = (bf16[2,4,256,128]{3,2,1,0:T(8,128)(2,1)S(1)}, bf16[2,4,256,128]{3,2,1,0:T(8,128)(2,1)S(1)}, u32[]{:S(2)}, u32[]{:S(2)}) collective-permute-start(bf16[2,4,256,128]{3,2,1,0:T(8,128)(2,1)S(1)} %collective-permute-done.4.refs_0_), channel_id=1, source_target_pairs={{0,1},{1,0},{2,3},{3,2},{4,5},{5,4},{6,7},{7,6},{8,9},{9,8},{10,11... | collective-permute-start | bytes 1572872 | tf_op jit(solution)/shard_map/ppermute | solution.py:355
  262.7 24.0 %collective-permute-start.6 = (bf16[2,4,256,128]{3,2,1,0:T(8,128)(2,1)S(1)}, bf16[2,4,256,128]{3,2,1,0:T(8,128)(2,1)S(1)}, u32[]{:S(2)}, u32[]{:S(2)}) collective-permute-start(bf16[2,4,256,128]{3,2,1,0:T(8,128)(2,1)S(1)} %collective-permute-done.4.refs_0_), channel_id=1, source_target_pairs={{0,2},{1,3},{2,0},{3,1},{4,6},{5,7},{6,4},{7,5},{8,10},{9,11},{10,... | collective-permute-start | bytes 1572872 | tf_op jit(solution)/shard_map/ppermute | solution.py:355
  264.3 26.7 %collective-permute-start.2 = (bf16[2,4,256,128]{3,2,1,0:T(8,128)(2,1)S(1)}, bf16[2,4,256,128]{3,2,1,0:T(8,128)(2,1)S(1)}, u32[]{:S(2)}, u32[]{:S(2)}) collective-permute-start(bf16[2,4,256,128]{3,2,1,0:T(8,128)(2,1)S(1)} %collective-permute-done.refs_0_), channel_id=1, source_target_pairs={{0,2},{1,3},{2,0},{3,1},{4,6},{5,7},{6,4},{7,5},{8,10},{9,11},{10,... | collective-permute-start | bytes 1572872 | tf_op jit(solution)/shard_map/ppermute | solution.py:355
  268.5 28.0 %collective-permute-start.1 = (bf16[2,4,256,128]{3,2,1,0:T(8,128)(2,1)S(1)}, bf16[2,4,256,128]{3,2,1,0:T(8,128)(2,1)S(1)}, u32[]{:S(2)}, u32[]{:S(2)}) collective-permute-start(bf16[2,4,256,128]{3,2,1,0:T(8,128)(2,1)S(1)} %collective-permute-done.refs_0_), channel_id=1, source_target_pairs={{0,1},{1,0},{2,3},{3,2},{4,5},{5,4},{6,7},{7,6},{8,9},{9,8},{10,11... | collective-permute-start | bytes 1572872 | tf_op jit(solution)/shard_map/ppermute | solution.py:355
  274.0 33.7 %collective-permute-start.27 = (bf16[2,4,256,128]{3,2,1,0:T(8,128)(2,1)S(1)}, bf16[2,4,256,128]{3,2,1,0:T(8,128)(2,1)S(1)}, u32[]{:S(2)}, u32[]{:S(2)}) collective-permute-start(bf16[2,4,256,128]{3,2,1,0:T(8,128)(2,1)S(1)} %collective-permute-done.26.refs_2_), channel_id=1, source_target_pairs={{0,1},{1,0},{2,3},{3,2},{4,5},{5,4},{6,7},{7,6},{8,9},{9,8},{10,11... | collective-permute-start | bytes 1572872 | tf_op jit(solution)/shard_map/ppermute | solution.py:355
  285.2 24.0 %collective-permute-start.23 = (bf16[2,4,256,128]{3,2,1,0:T(8,128)(2,1)S(1)}, bf16[2,4,256,128]{3,2,1,0:T(8,128)(2,1)S(1)}, u32[]{:S(2)}, u32[]{:S(2)}) collective-permute-start(bf16[2,4,256,128]{3,2,1,0:T(8,128)(2,1)S(1)} %collective-permute-done.21.refs_1_), channel_id=1, source_target_pairs={{0,2},{1,3},{2,0},{3,1},{4,6},{5,7},{6,4},{7,5},{8,10},{9,11},{10,... | collective-permute-start | bytes 1572872 | tf_op jit(solution)/shard_map/ppermute | solution.py:355
  286.7 32.2 %collective-permute-start.19 = (bf16[2,4,256,128]{3,2,1,0:T(8,128)(2,1)S(1)}, bf16[2,4,256,128]{3,2,1,0:T(8,128)(2,1)S(1)}, u32[]{:S(2)}, u32[]{:S(2)}) collective-permute-start(bf16[2,4,256,128]{3,2,1,0:T(8,128)(2,1)S(1)} %collective-permute-done.18.refs_2_), channel_id=1, source_target_pairs={{0,1},{1,0},{2,3},{3,2},{4,5},{5,4},{6,7},{7,6},{8,9},{9,8},{10,11... | collective-permute-start | bytes 1572872 | tf_op jit(solution)/shard_map/ppermute | solution.py:355
  290.9 29.5 %collective-permute-start.15 = (bf16[2,4,256,128]{3,2,1,0:T(8,128)(2,1)S(1)}, bf16[2,4,256,128]{3,2,1,0:T(8,128)(2,1)S(1)}, u32[]{:S(2)}, u32[]{:S(2)}) collective-permute-start(bf16[2,4,256,128]{3,2,1,0:T(8,128)(2,1)S(1)} %collective-permute-done.13.refs_1_), channel_id=1, source_target_pairs={{0,2},{1,3},{2,0},{3,1},{4,6},{5,7},{6,4},{7,5},{8,10},{9,11},{10,... | collective-permute-start | bytes 1572872 | tf_op jit(solution)/shard_map/ppermute | solution.py:355
  296.4 33.7 %collective-permute-start.11 = (bf16[2,4,256,128]{3,2,1,0:T(8,128)(2,1)S(1)}, bf16[2,4,256,128]{3,2,1,0:T(8,128)(2,1)S(1)}, u32[]{:S(2)}, u32[]{:S(2)}) collective-permute-start(bf16[2,4,256,128]{3,2,1,0:T(8,128)(2,1)S(1)} %collective-permute-done.10.refs_2_), channel_id=1, source_target_pairs={{0,1},{1,0},{2,3},{3,2},{4,5},{5,4},{6,7},{7,6},{8,9},{9,8},{10,11... | collective-permute-start | bytes 1572872 | tf_op jit(solution)/shard_map/ppermute | solution.py:355
  307.7 24.0 %collective-permute-start.7 = (bf16[2,4,256,128]{3,2,1,0:T(8,128)(2,1)S(1)}, bf16[2,4,256,128]{3,2,1,0:T(8,128)(2,1)S(1)}, u32[]{:S(2)}, u32[]{:S(2)}) collective-permute-start(bf16[2,4,256,128]{3,2,1,0:T(8,128)(2,1)S(1)} %collective-permute-done.5.refs_1_), channel_id=1, source_target_pairs={{0,2},{1,3},{2,0},{3,1},{4,6},{5,7},{6,4},{7,5},{8,10},{9,11},{10,... | collective-permute-start | bytes 1572872 | tf_op jit(solution)/shard_map/ppermute | solution.py:355
  309.2 32.2 %collective-permute-start.3 = (bf16[2,4,256,128]{3,2,1,0:T(8,128)(2,1)S(1)}, bf16[2,4,256,128]{3,2,1,0:T(8,128)(2,1)S(1)}, u32[]{:S(2)}, u32[]{:S(2)}) collective-permute-start(bf16[2,4,256,128]{3,2,1,0:T(8,128)(2,1)S(1)} %collective-permute-done.2.refs_2_), channel_id=1, source_target_pairs={{0,1},{1,0},{2,3},{3,2},{4,5},{5,4},{6,7},{7,6},{8,9},{9,8},{10,11... | collective-permute-start | bytes 1572872 | tf_op jit(solution)/shard_map/ppermute | solution.py:355
  318.9 73.5 %collective-permute-start.62 = (bf16[4,256,128]{2,1,0:T(8,128)(2,1)}, bf16[4,256,128]{2,1,0:T(8,128)(2,1)}, u32[]{:S(2)}, u32[]{:S(2)}) collective-permute-start(bf16[4,256,128]{2,1,0:T(8,128)(2,1)} %collective-permute-done.61.refs_2_), channel_id=1, source_target_pairs={{0,1},{1,0},{2,3},{3,2},{4,5},{5,4},{6,7},{7,6},{8,9},{9,8},{10,11... | collective-permute-start | bytes 786440 | tf_op jit(solution)/shard_map/ppermute | solution.py:355
  320.4 74.9 %collective-permute-start.66 = (bf16[4,256,128]{2,1,0:T(8,128)(2,1)}, bf16[4,256,128]{2,1,0:T(8,128)(2,1)}, u32[]{:S(2)}, u32[]{:S(2)}) collective-permute-start(bf16[4,256,128]{2,1,0:T(8,128)(2,1)} %collective-permute-done.64.refs_0_), channel_id=1, source_target_pairs={{0,2},{1,3},{2,0},{3,1},{4,6},{5,7},{6,4},{7,5},{8,10},{9,11},{10,... | collective-permute-start | bytes 786440 | tf_op jit(solution)/shard_map/ppermute | solution.py:355
  330.2 65.2 %collective-permute-start.67 = (bf16[4,256,128]{2,1,0:T(8,128)(2,1)}, bf16[4,256,128]{2,1,0:T(8,128)(2,1)}, u32[]{:S(2)}, u32[]{:S(2)}) collective-permute-start(bf16[4,256,128]{2,1,0:T(8,128)(2,1)} %collective-permute-done.65.refs_1_), channel_id=1, source_target_pairs={{0,2},{1,3},{2,0},{3,1},{4,6},{5,7},{6,4},{7,5},{8,10},{9,11},{10,... | collective-permute-start | bytes 786440 | tf_op jit(solution)/shard_map/ppermute | solution.py:355
  331.7 70.4 %collective-permute-start.31 = (bf16[4,256,128]{2,1,0:T(8,128)(2,1)}, bf16[4,256,128]{2,1,0:T(8,128)(2,1)}, u32[]{:S(2)}, u32[]{:S(2)}) collective-permute-start(bf16[4,256,128]{2,1,0:T(8,128)(2,1)} %get-tuple-element.76.refs_0_), channel_id=1, source_target_pairs={{0,1},{1,0},{2,3},{3,2},{4,5},{5,4},{6,7},{7,6},{8,9},{9,8},{10,11... | collective-permute-start | bytes 786440 | tf_op jit(solution)/shard_map/ppermute | solution.py:355
  341.4 60.7 %collective-permute-start.33 = (bf16[4,256,128]{2,1,0:T(8,128)(2,1)}, bf16[4,256,128]{2,1,0:T(8,128)(2,1)}, u32[]{:S(2)}, u32[]{:S(2)}) collective-permute-start(bf16[4,256,128]{2,1,0:T(8,128)(2,1)} %collective-permute-done.32.refs_2_), channel_id=1, source_target_pairs={{0,1},{1,0},{2,3},{3,2},{4,5},{5,4},{6,7},{7,6},{8,9},{9,8},{10,11... | collective-permute-start | bytes 786440 | tf_op jit(solution)/shard_map/ppermute | solution.py:355
  402.1 10.6 %collective-permute-start.53 = (bf16[256,256]{1,0:T(8,128)(2,1)}, bf16[256,256]{1,0:T(8,128)(2,1)}, u32[]{:S(2)}, u32[]{:S(2)}) collective-permute-start(bf16[256,256]{1,0:T(8,128)(2,1)} %get-tuple-element.89), channel_id=1, source_target_pairs={{0,8},{4,12},{8,16},{12,20},{16,24},{20,28},{24,0},{28,4},{1,9},{5... | collective-permute-start | bytes 393224 | tf_op jit(solution)/shard_map/ppermute | solution.py:351
  402.1 11.4 %collective-permute-start.48 = (bf16[256,256]{1,0:T(8,128)(2,1)}, bf16[256,256]{1,0:T(8,128)(2,1)}, u32[]{:S(2)}, u32[]{:S(2)}) collective-permute-start(bf16[256,256]{1,0:T(8,128)(2,1)} %get-tuple-element.86), channel_id=1, source_target_pairs={{0,24},{4,28},{8,0},{12,4},{16,8},{20,12},{24,16},{28,20},{1,25},{... | collective-permute-start | bytes 393224 | tf_op jit(solution)/shard_map/ppermute | solution.py:351
  405.9 17.4 %collective-permute-start.43 = (bf16[256,256]{1,0:T(8,128)(2,1)}, bf16[256,256]{1,0:T(8,128)(2,1)}, u32[]{:S(2)}, u32[]{:S(2)}) collective-permute-start(bf16[256,256]{1,0:T(8,128)(2,1)} %get-tuple-element.83), channel_id=1, source_target_pairs={{0,20},{4,16},{8,28},{12,24},{16,4},{20,0},{24,12},{28,8},{1,21},{... | collective-permute-start | bytes 393224 | tf_op jit(solution)/shard_map/ppermute | solution.py:351
  406.0 20.1 %collective-permute-start.38 = (bf16[256,256]{1,0:T(8,128)(2,1)}, bf16[256,256]{1,0:T(8,128)(2,1)}, u32[]{:S(2)}, u32[]{:S(2)}) collective-permute-start(bf16[256,256]{1,0:T(8,128)(2,1)} %get-tuple-element.80), channel_id=1, source_target_pairs={{0,16},{4,20},{8,24},{12,28},{16,0},{20,4},{24,8},{28,12},{1,17},{... | collective-permute-start | bytes 393224 | tf_op jit(solution)/shard_map/ppermute | solution.py:351
  (48 other events, 2941.3 us)

commit v4 on v3

--- a/solution.py
+++ b/solution.py
@@ -230,32 +230,47 @@
     out, result_ref, held_buf, block, scaled_buf, sum_buf, in_sem, sum_sem, sems = refs[-9:]
     held, rows, hidden = parts[0].shape
     first = pl.multiple_of(sender(step) * rows, LANES)
-    loads = [
-        pltpu.make_async_copy(part, held_buf.at[swap], in_sem.at[swap])
-        for swap, part in enumerate(parts)
-    ]
-    loads.append(pltpu.make_async_copy(scaled_ref, scaled_buf, sems.at[0]))
+    half, width = held // 2, scaled_buf.shape[1] // 2
+    loads = []
+    for side in range(2):
+        experts, columns = pl.ds(side * half, half), pl.ds(side * width, width)
+        for swap, part in enumerate(parts):
+            place = held_buf.at[swap, experts]
+            loads.append(
+                pltpu.make_async_copy(part.at[experts], place, in_sem.at[side, swap])
+            )
+        place = scaled_buf.at[:, columns]
+        loads.append(pltpu.make_async_copy(scaled_ref.at[:, columns], place, sems.at[side]))
     for i, other in enumerate(others):
         loads.append(pltpu.make_async_copy(other, sum_buf.at[i], sum_sem.at[i]))
     for copy in loads:
         copy.start()
-    for swap in range(4):
-        loads[swap].wait()
-        for e in range(held):
-            block[:, pl.ds(column_of(e, swap, hidden), hidden)] = held_buf[swap, e]
-    store = pltpu.make_async_copy(block, out.at[pl.ds(first, rows), :], sems.at[1])
-    store.start()
-    loads[4].wait()
-    product = lax.dot_general(
-        scaled_buf[...], block[...], (((1,), (1,)), ((), ())), preferred_element_type=jnp.float32
-    )
+    product, stores = None, []
+    for side in range(2):
+        columns = pl.ds(side * width, width)
+        for swap in range(4):
+            loads[side * 5 + swap].wait()
+            for e in range(side * half, (side + 1) * half):
+                block[:, pl.ds(column_of(e, swap, hidden), hidden)] = held_buf[swap, e]
+        place = out.at[pl.ds(first, rows), columns]
+        stores.append(pltpu.make_async_copy(block.at[:, columns], place, sems.at[2 + side]))
+        stores[side].start()
+        loads[side * 5 + 4].wait()
+        dot = lax.dot_general(
+            scaled_buf[:, columns],
+            block[:, columns],
+            (((1,), (1,)), ((), ())),
+            preferred_element_type=jnp.float32,
+        )
+        product = dot if product is None else product + dot
     if sums:
         for i in range(sums):
-            loads[5 + i].wait()
+            loads[10 + i].wait()
             product += sum_buf[i].astype(jnp.float32)
         product *= factor
     result_ref[...] = product.astype(result_ref.dtype)
-    store.wait()
+    for copy in stores:
+        copy.wait()
 
 
 def lay_down(step, parts, scaled, others, out, total):
@@ -277,9 +292,9 @@
             pltpu.VMEM((rows, width), jnp.bfloat16),
             pltpu.VMEM((tokens, width), jnp.bfloat16),
             pltpu.VMEM((max(sums, 1), tokens, rows), jnp.bfloat16),
+            pltpu.SemaphoreType.DMA((2, 4)),
+            pltpu.SemaphoreType.DMA((max(sums, 1),)),
             pltpu.SemaphoreType.DMA((4,)),
-            pltpu.SemaphoreType.DMA((max(sums, 1),)),
-            pltpu.SemaphoreType.DMA((2,)),
         ],
         input_output_aliases={} if fresh else {5 + sums: 0},
         compiler_params=ROOM,
@@ -432,7 +447,7 @@
         jax.shard_map, mesh=mesh, in_specs=in_specs, out_specs=out_specs, check_vma=False
     )
     ways, parts = mesh.shape["fs"], mesh.shape["tp"]
-    whole_experts = ways & (ways - 1) == 0 and ways >= 4 and (GROUPS * EPG) % ways == 0
+    whole_experts = ways & (ways - 1) == 0 and ways >= 4 and (GROUPS * EPG) % (2 * ways) == 0
     if not (whole_experts and parts == 4 and FF % (parts * LANES) == 0):
         return wrap(general_shards)
 

time: 430 us -> 432 us (level)
  no operation moved by 1% of the time
where the time goes in v4:
time: 432 us; the launch traced here: 431 us
  waiting for transfers between devices  268 us (62%)
  starting transfers between devices  89.6 us (21%)
  Pallas kernels  72 us (17%)
    ppermute x48, waiting for transfers between devices, tp_swap(): lax.ppermute(value, 'tp', [(i, i ^ step) for i in range(lax.axis_size('tp...  152 us
    ppermute x21, waiting for transfers between devices, fs_send(): return lax.ppermute(value, 'fs', pairs)  116 us
    ppermute x48, starting transfers between devices, tp_swap(): lax.ppermute(value, 'tp', [(i, i ^ step) for i in range(lax.axis_size('tp...  59.4 us
    ppermute x21, starting transfers between devices, fs_send(): return lax.ppermute(value, 'fs', pairs)  30.3 us
    pallas_call x8, Pallas kernels, lay_down(): pl.pallas_call(functools.partial(lay_down_kernel, step, sums, FF ** (-0.5...  25.6 us
    pallas_call x8, Pallas kernels, lay_pair(): pl.pallas_call(functools.partial(lay_pair_kernel, step), in_specs=[ANYWHE...  20.7 us
    pallas_call x1, Pallas kernels, act(): pl.pallas_call(act_kernel, grid=(held,), in_specs=[pl.BlockSpec(normed.sh...  11.2 us
  transfers between devices with their start and end apart: 69, of which 35 were waited for; matrix products, arithmetic and copies ran while one was open for 0% of the time, Pallas kernels for 15%

profile of v4, /device:TPU:0, one launch (start us, length us, event | category | flops | bytes accessed | tf_op | source)
XLA Modules:
  0.0 431.4 jit_solution(5578003127286836379)
XLA Ops:
  0.6 3.3 shard_map.121
  4.0 4.1 collective-permute-start.34
  9.7 2.2 collective-permute-start.49
  11.9 21.3 %collective-permute-done.34.refs_0_ = bf16[4,256,128]{2,1,0:T(8,128)(2,1)} collective-permute-done((bf16[4,256,128]{2,1,0:T(8,128)(2,1)}, bf16[4,256,128]{2,1,0:T(8,128)(2,1)}, u32[]{:S(2)}, u32[]{:S(2)}) %collective-permute-start.34) | collective-permute-done | bytes 262176 | tf_op jit(solution)/shard_map/ppermute | solution.py:366
  33.3 8.8 %collective-permute-done.39.refs_0_ = bf16[4,256,128]{2,1,0:T(8,128)(2,1)} collective-permute-done((bf16[4,256,128]{2,1,0:T(8,128)(2,1)}, bf16[4,256,128]{2,1,0:T(8,128)(2,1)}, u32[]{:S(2)}, u32[]{:S(2)}) %collective-permute-start.39) | collective-permute-done | bytes 262176 | tf_op jit(solution)/shard_map/ppermute | solution.py:366
  43.5 2.7 shard_map.112.refs_0_
  46.3 1.9 collective-permute-start.28
  48.2 5.5 %shard_map.111 = (bf16[2,4,256,128]{3,2,1,0:T(8,128)(2,1)}, bf16[2,4,256,128]{3,2,1,0:T(8,128)(2,1)}, bf16[2,4,256,128]{3,2,1,0:T(8,128)(2,1)}, bf16[2,4,256,128...) custom-call(f32[1,256]{1,0:T(1,128)} %bitcast.5, ...), custom_call_target="tpu_custom_call" | custom-call | tf_op jit(solution)/shard_map/pallas_call | solution.py:124
  55.3 2.7 collective-permute-start.20
  58.5 14.8 %collective-permute-done.32.refs_2_ = bf16[4,256,128]{2,1,0:T(8,128)(2,1)} collective-permute-done((bf16[4,256,128]{2,1,0:T(8,128)(2,1)}, bf16[4,256,128]{2,1,0:T(8,128)(2,1)}, u32[]{:S(2)}, u32[]{:S(2)}) %collective-permute-start.32) | collective-permute-done | bytes 262176 | tf_op jit(solution)/shard_map/ppermute | solution.py:370
  75.0 3.1 collective-permute-start.8
  78.1 2.2 collective-permute-start.4
  80.3 2.1 collective-permute-start
  82.4 7.4 %collective-permute-done.16.refs_0_ = bf16[2,4,256,128]{3,2,1,0:T(8,128)(2,1)S(1)} collective-permute-done((bf16[2,4,256,128]{3,2,1,0:T(8,128)(2,1)}, bf16[2,4,256,128]{3,2,1,0:T(8,128)(2,1)S(1)}, u32[]{:S(2)}, u32[]{:S(2)}) %collective-permute-start.16) | collective-permute-done | bytes 524320 | tf_op jit(solution)/shard_map/ppermute | solution.py:366
  90.3 8.8 %collective-permute-done.12.refs_0_ = bf16[2,4,256,128]{3,2,1,0:T(8,128)(2,1)S(1)} collective-permute-done((bf16[2,4,256,128]{3,2,1,0:T(8,128)(2,1)}, bf16[2,4,256,128]{3,2,1,0:T(8,128)(2,1)S(1)}, u32[]{:S(2)}, u32[]{:S(2)}) %collective-permute-start.12) | collective-permute-done | bytes 524320 | tf_op jit(solution)/shard_map/ppermute | solution.py:366
  100.7 7.8 %collective-permute-done.8.refs_0_ = bf16[2,4,256,128]{3,2,1,0:T(8,128)(2,1)S(1)} collective-permute-done((bf16[2,4,256,128]{3,2,1,0:T(8,128)(2,1)}, bf16[2,4,256,128]{3,2,1,0:T(8,128)(2,1)S(1)}, u32[]{:S(2)}, u32[]{:S(2)}) %collective-permute-start.8) | collective-permute-done | bytes 524320 | tf_op jit(solution)/shard_map/ppermute | solution.py:366
  110.0 36.9 %collective-permute-done.4.refs_0_ = bf16[2,4,256,128]{3,2,1,0:T(8,128)(2,1)S(1)} collective-permute-done((bf16[2,4,256,128]{3,2,1,0:T(8,128)(2,1)}, bf16[2,4,256,128]{3,2,1,0:T(8,128)(2,1)S(1)}, u32[]{:S(2)}, u32[]{:S(2)}) %collective-permute-start.4) | collective-permute-done | bytes 524320 | tf_op jit(solution)/shard_map/ppermute | solution.py:366
  147.4 6.9 %collective-permute-done.refs_0_ = bf16[2,4,256,128]{3,2,1,0:T(8,128)(2,1)S(1)} collective-permute-done((bf16[2,4,256,128]{3,2,1,0:T(8,128)(2,1)}, bf16[2,4,256,128]{3,2,1,0:T(8,128)(2,1)S(1)}, u32[]{:S(2)}, u32[]{:S(2)}) %collective-permute-start) | collective-permute-done | bytes 524320 | tf_op jit(solution)/shard_map/ppermute | solution.py:366
  158.9 4.0 collective-permute-done.45.refs_1_
  165.3 4.1 collective-permute-done.51.refs_2_
  171.4 2.8 collective-permute-done.55.refs_1_
  176.5 4.2 collective-permute-done.61.refs_2_
  182.8 2.7 collective-permute-done.65.refs_1_
  187.8 3.2 collective-permute-done.42.refs_3_
  192.6 21.8 %collective-permute-done.47.refs_3_ = bf16[4,256,128]{2,1,0:T(8,128)(2,1)S(1)} collective-permute-done((bf16[4,256,128]{2,1,0:T(8,128)(2,1)S(1)}, bf16[4,256,128]{2,1,0:T(8,128)(2,1)S(1)}, u32[]{:S(2)}, u32[]{:S(2)}) %collective-permute-start.47) | collective-permute-done | bytes 262176 | tf_op jit(solution)/shard_map/ppermute | solution.py:370
  216.4 3.5 collective-permute-done.57.refs_3_
  223.8 5.2 %collective-permute-done.25.refs_1_ = bf16[2,4,256,128]{3,2,1,0:T(8,128)(2,1)S(1)} collective-permute-done((bf16[2,4,256,128]{3,2,1,0:T(8,128)(2,1)S(1)}, bf16[2,4,256,128]{3,2,1,0:T(8,128)(2,1)S(1)}, u32[]{:S(2)}, u32[]{:S(2)}) %collective-permute-start.25) | collective-permute-done | bytes 524320 | tf_op jit(solution)/shard_map/ppermute | solution.py:370
  230.5 9.7 %collective-permute-done.21.refs_1_ = bf16[2,4,256,128]{3,2,1,0:T(8,128)(2,1)S(1)} collective-permute-done((bf16[2,4,256,128]{3,2,1,0:T(8,128)(2,1)S(1)}, bf16[2,4,256,128]{3,2,1,0:T(8,128)(2,1)S(1)}, u32[]{:S(2)}, u32[]{:S(2)}) %collective-permute-start.21) | collective-permute-done | bytes 524320 | tf_op jit(solution)/shard_map/ppermute | solution.py:370
  242.3 3.7 collective-permute-done.18.refs_2_
  247.5 4.0 collective-permute-done.17.refs_1_
  253.0 9.7 %collective-permute-done.13.refs_1_ = bf16[2,4,256,128]{3,2,1,0:T(8,128)(2,1)S(1)} collective-permute-done((bf16[2,4,256,128]{3,2,1,0:T(8,128)(2,1)S(1)}, bf16[2,4,256,128]{3,2,1,0:T(8,128)(2,1)S(1)}, u32[]{:S(2)}, u32[]{:S(2)}) %collective-permute-start.13) | collective-permute-done | bytes 524320 | tf_op jit(solution)/shard_map/ppermute | solution.py:370
  264.8 3.7 collective-permute-done.10.refs_2_
  269.9 4.0 collective-permute-done.9.refs_1_
  275.5 9.7 %collective-permute-done.5.refs_1_ = bf16[2,4,256,128]{3,2,1,0:T(8,128)(2,1)S(1)} collective-permute-done((bf16[2,4,256,128]{3,2,1,0:T(8,128)(2,1)S(1)}, bf16[2,4,256,128]{3,2,1,0:T(8,128)(2,1)S(1)}, u32[]{:S(2)}, u32[]{:S(2)}) %collective-permute-start.5) | collective-permute-done | bytes 524320 | tf_op jit(solution)/shard_map/ppermute | solution.py:370
  288.2 2.7 collective-permute-done.2.refs_2_
  292.4 4.0 collective-permute-done.1.refs_1_
  297.9 9.7 %collective-permute-done.27.refs_3_ = bf16[2,4,256,128]{3,2,1,0:T(8,128)(2,1)S(1)} collective-permute-done((bf16[2,4,256,128]{3,2,1,0:T(8,128)(2,1)S(1)}, bf16[2,4,256,128]{3,2,1,0:T(8,128)(2,1)S(1)}, u32[]{:S(2)}, u32[]{:S(2)}) %collective-permute-start.27) | collective-permute-done | bytes 524320 | tf_op jit(solution)/shard_map/ppermute | solution.py:370
  310.8 8.1 %collective-permute-done.19.refs_3_ = bf16[2,4,256,128]{3,2,1,0:T(8,128)(2,1)S(1)} collective-permute-done((bf16[2,4,256,128]{3,2,1,0:T(8,128)(2,1)S(1)}, bf16[2,4,256,128]{3,2,1,0:T(8,128)(2,1)S(1)}, u32[]{:S(2)}, u32[]{:S(2)}) %collective-permute-start.19) | collective-permute-done | bytes 524320 | tf_op jit(solution)/shard_map/ppermute | solution.py:370
  322.0 8.1 %collective-permute-done.11.refs_3_ = bf16[2,4,256,128]{3,2,1,0:T(8,128)(2,1)S(1)} collective-permute-done((bf16[2,4,256,128]{3,2,1,0:T(8,128)(2,1)S(1)}, bf16[2,4,256,128]{3,2,1,0:T(8,128)(2,1)S(1)}, u32[]{:S(2)}, u32[]{:S(2)}) %collective-permute-start.11) | collective-permute-done | bytes 524320 | tf_op jit(solution)/shard_map/ppermute | solution.py:370
  333.3 8.1 %collective-permute-done.3.refs_3_ = bf16[2,4,256,128]{3,2,1,0:T(8,128)(2,1)S(1)} collective-permute-done((bf16[2,4,256,128]{3,2,1,0:T(8,128)(2,1)S(1)}, bf16[2,4,256,128]{3,2,1,0:T(8,128)(2,1)S(1)}, u32[]{:S(2)}, u32[]{:S(2)}) %collective-permute-start.3) | collective-permute-done | bytes 524320 | tf_op jit(solution)/shard_map/ppermute | solution.py:370
  343.0 2.8 shard_map.122
  345.7 2.6 shard_map.113
  348.3 2.6 shard_map.114
  350.9 2.6 shard_map.115
  353.5 2.6 shard_map.116
  356.1 2.6 shard_map.117
  358.7 2.6 shard_map.118
  361.3 2.6 shard_map.119
  363.9 2.6 shard_map.120
  366.5 11.2 %shard_map.123.refs_4_ = bf16[256,2048]{1,0:T(8,128)(2,1)} custom-call(bf16[256,2048]{1,0:T(8,128)(2,1)} %get-tuple-element.77.normed_ref, bf16[2048,2048]{1,0:T(8,128)(2,1)} %get-tuple-element.49.gate_ref, bf16[2048,2048]{1,0:T(8,128)(2,1)} %get-tuple-element.50.up_ref, f32[4,256,128]{2,1,0:T(8,128)} %get-tuple-element.78.weight_ref), custom_call_target="tpu_custom_call" | custom-call | tf_op jit(solution)/shard_map/pallas_call | solution.py:345
  377.8 3.2 shard_map.124
  381.0 3.2 shard_map.125
  384.1 3.2 shard_map.126
  387.3 3.2 shard_map.127
  390.5 3.2 shard_map.128
  393.7 3.2 shard_map.129
  396.9 3.2 shard_map.130
  400.3 3.5 collective-permute-start.58
  403.8 3.8 collective-permute-start.48
  407.7 2.3 collective-permute-start.38
  410.0 4.4 %collective-permute-done.53.refs_8_ = bf16[256,256]{1,0:T(8,128)(2,1)} collective-permute-done((bf16[256,256]{1,0:T(8,128)(2,1)}, bf16[256,256]{1,0:T(8,128)(2,1)}, u32[]{:S(2)}, u32[]{:S(2)}) %collective-permute-start.53) | collective-permute-done | bytes 131104 | tf_op jit(solution)/shard_map/ppermute | solution.py:366
  415.2 9.8 %collective-permute-done.43.refs_6_ = bf16[256,256]{1,0:T(8,128)(2,1)} collective-permute-done((bf16[256,256]{1,0:T(8,128)(2,1)}, bf16[256,256]{1,0:T(8,128)(2,1)}, u32[]{:S(2)}, u32[]{:S(2)}) %collective-permute-start.43) | collective-permute-done | bytes 131104 | tf_op jit(solution)/shard_map/ppermute | solution.py:366
  425.0 2.8 collective-permute-done.38.refs_5_
  427.8 3.4 shard_map.131
  (181 shorter events, 63.6 us)
Async XLA Ops:
  4.0 29.3 %collective-permute-start.34 = (bf16[4,256,128]{2,1,0:T(8,128)(2,1)}, bf16[4,256,128]{2,1,0:T(8,128)(2,1)}, u32[]{:S(2)}, u32[]{:S(2)}) collective-permute-start(bf16[4,256,128]{2,1,0:T(8,128)(2,1)} %get-tuple-element.79), channel_id=1, source_target_pairs={{0,16},{4,20},{8,24},{12,28},{16,0},{20,4},{24,8},{28,12},{1,17},{... | collective-permute-start | bytes 786440 | tf_op jit(solution)/shard_map/ppermute | solution.py:366
  8.1 34.0 %collective-permute-start.39 = (bf16[4,256,128]{2,1,0:T(8,128)(2,1)}, bf16[4,256,128]{2,1,0:T(8,128)(2,1)}, u32[]{:S(2)}, u32[]{:S(2)}) collective-permute-start(bf16[4,256,128]{2,1,0:T(8,128)(2,1)} %get-tuple-element.81), channel_id=1, source_target_pairs={{0,20},{4,16},{8,28},{12,24},{16,4},{20,0},{24,12},{28,8},{1,21},{... | collective-permute-start | bytes 786440 | tf_op jit(solution)/shard_map/ppermute | solution.py:366
  8.1 38.2 %collective-permute-start.44 = (bf16[4,256,128]{2,1,0:T(8,128)(2,1)}, bf16[4,256,128]{2,1,0:T(8,128)(2,1)}, u32[]{:S(2)}, u32[]{:S(2)}) collective-permute-start(bf16[4,256,128]{2,1,0:T(8,128)(2,1)} %get-tuple-element.84), channel_id=1, source_target_pairs={{0,8},{4,12},{8,16},{12,20},{16,24},{20,28},{24,0},{28,4},{1,9},{5... | collective-permute-start | bytes 786440 | tf_op jit(solution)/shard_map/ppermute | solution.py:366
  9.7 44.0 %collective-permute-start.49 = (bf16[4,256,128]{2,1,0:T(8,128)(2,1)}, bf16[4,256,128]{2,1,0:T(8,128)(2,1)}, u32[]{:S(2)}, u32[]{:S(2)}) collective-permute-start(bf16[4,256,128]{2,1,0:T(8,128)(2,1)} %get-tuple-element.87), channel_id=1, source_target_pairs={{0,24},{4,28},{8,0},{12,4},{16,8},{20,12},{24,16},{28,20},{1,25},{... | collective-permute-start | bytes 786440 | tf_op jit(solution)/shard_map/ppermute | solution.py:366
  11.9 43.4 %collective-permute-start.54 = (bf16[4,256,128]{2,1,0:T(8,128)(2,1)}, bf16[4,256,128]{2,1,0:T(8,128)(2,1)}, u32[]{:S(2)}, u32[]{:S(2)}) collective-permute-start(bf16[4,256,128]{2,1,0:T(8,128)(2,1)} %get-tuple-element.90), channel_id=1, source_target_pairs={{0,12},{4,8},{8,20},{12,16},{16,28},{20,24},{24,4},{28,0},{1,13},{... | collective-permute-start | bytes 786440 | tf_op jit(solution)/shard_map/ppermute | solution.py:366
  33.3 22.0 %collective-permute-start.59 = (bf16[4,256,128]{2,1,0:T(8,128)(2,1)}, bf16[4,256,128]{2,1,0:T(8,128)(2,1)}, u32[]{:S(2)}, u32[]{:S(2)}) collective-permute-start(bf16[4,256,128]{2,1,0:T(8,128)(2,1)} %get-tuple-element.93), channel_id=1, source_target_pairs={{0,28},{4,24},{8,4},{12,0},{16,12},{20,8},{24,20},{28,16},{1,29},{... | collective-permute-start | bytes 786440 | tf_op jit(solution)/shard_map/ppermute | solution.py:366
  42.1 15.9 %collective-permute-start.64 = (bf16[4,256,128]{2,1,0:T(8,128)(2,1)}, bf16[4,256,128]{2,1,0:T(8,128)(2,1)}, u32[]{:S(2)}, u32[]{:S(2)}) collective-permute-start(bf16[4,256,128]{2,1,0:T(8,128)(2,1)} %get-tuple-element.96), channel_id=1, source_target_pairs={{0,4},{4,0},{8,12},{12,8},{16,20},{20,16},{24,28},{28,24},{1,5},{5... | collective-permute-start | bytes 786440 | tf_op jit(solution)/shard_map/ppermute | solution.py:366
  46.3 27.0 %collective-permute-start.28 = (bf16[2,4,256,128]{3,2,1,0:T(8,128)(2,1)}, bf16[2,4,256,128]{3,2,1,0:T(8,128)(2,1)}, u32[]{:S(2)}, u32[]{:S(2)}) collective-permute-start(bf16[2,4,256,128]{3,2,1,0:T(8,128)(2,1)} %shard_map.112.refs_0_), channel_id=1, source_target_pairs={{0,1},{1,0},{2,3},{3,2},{4,5},{5,4},{6,7},{7,6},{8,9},{9,8},{10,11... | collective-permute-start | bytes 1572872 | tf_op jit(solution)/shard_map/ppermute | solution.py:370
  53.7 20.5 %collective-permute-start.29 = (bf16[2,4,256,128]{3,2,1,0:T(8,128)(2,1)}, bf16[2,4,256,128]{3,2,1,0:T(8,128)(2,1)S(1)}, u32[]{:S(2)}, u32[]{:S(2)}) collective-permute-start(bf16[2,4,256,128]{3,2,1,0:T(8,128)(2,1)} %shard_map.112.refs_0_), channel_id=1, source_target_pairs={{0,2},{1,3},{2,0},{3,1},{4,6},{5,7},{6,4},{7,5},{8,10},{9,11},{10,... | collective-permute-start | bytes 1572872 | tf_op jit(solution)/shard_map/ppermute | solution.py:370
  55.3 22.8 %collective-permute-start.24 = (bf16[2,4,256,128]{3,2,1,0:T(8,128)(2,1)}, bf16[2,4,256,128]{3,2,1,0:T(8,128)(2,1)S(1)}, u32[]{:S(2)}, u32[]{:S(2)}) collective-permute-start(bf16[2,4,256,128]{3,2,1,0:T(8,128)(2,1)} %get-tuple-element.59), channel_id=1, source_target_pairs={{0,4},{4,0},{8,12},{12,8},{16,20},{20,16},{24,28},{28,24},{1,5},{5... | collective-permute-start | bytes 1572872 | tf_op jit(solution)/shard_map/ppermute | solution.py:366
  55.3 25.0 %collective-permute-start.20 = (bf16[2,4,256,128]{3,2,1,0:T(8,128)(2,1)}, bf16[2,4,256,128]{3,2,1,0:T(8,128)(2,1)S(1)}, u32[]{:S(2)}, u32[]{:S(2)}) collective-permute-start(bf16[2,4,256,128]{3,2,1,0:T(8,128)(2,1)} %get-tuple-element.58), channel_id=1, source_target_pairs={{0,8},{4,12},{8,16},{12,20},{16,24},{20,28},{24,0},{28,4},{1,9},{5... | collective-permute-start | bytes 1572872 | tf_op jit(solution)/shard_map/ppermute | solution.py:366
  58.0 15.3 %collective-permute-start.32 = (bf16[4,256,128]{2,1,0:T(8,128)(2,1)}, bf16[4,256,128]{2,1,0:T(8,128)(2,1)}, u32[]{:S(2)}, u32[]{:S(2)}) collective-permute-start(bf16[4,256,128]{2,1,0:T(8,128)(2,1)} %get-tuple-element.76.refs_0_), channel_id=1, source_target_pairs={{0,2},{1,3},{2,0},{3,1},{4,6},{5,7},{6,4},{7,5},{8,10},{9,11},{10,... | collective-permute-start | bytes 786440 | tf_op jit(solution)/shard_map/ppermute | solution.py:370
  73.2 16.5 %collective-permute-start.16 = (bf16[2,4,256,128]{3,2,1,0:T(8,128)(2,1)}, bf16[2,4,256,128]{3,2,1,0:T(8,128)(2,1)S(1)}, u32[]{:S(2)}, u32[]{:S(2)}) collective-permute-start(bf16[2,4,256,128]{3,2,1,0:T(8,128)(2,1)} %get-tuple-element.57), channel_id=1, source_target_pairs={{0,24},{4,28},{8,0},{12,4},{16,8},{20,12},{24,16},{28,20},{1,25},{... | collective-permute-start | bytes 1572872 | tf_op jit(solution)/shard_map/ppermute | solution.py:366
  73.3 25.9 %collective-permute-start.12 = (bf16[2,4,256,128]{3,2,1,0:T(8,128)(2,1)}, bf16[2,4,256,128]{3,2,1,0:T(8,128)(2,1)S(1)}, u32[]{:S(2)}, u32[]{:S(2)}) collective-permute-start(bf16[2,4,256,128]{3,2,1,0:T(8,128)(2,1)} %get-tuple-element.56), channel_id=1, source_target_pairs={{0,12},{4,8},{8,20},{12,16},{16,28},{20,24},{24,4},{28,0},{1,13},{... | collective-permute-start | bytes 1572872 | tf_op jit(solution)/shard_map/ppermute | solution.py:366
  75.0 33.4 %collective-permute-start.8 = (bf16[2,4,256,128]{3,2,1,0:T(8,128)(2,1)}, bf16[2,4,256,128]{3,2,1,0:T(8,128)(2,1)S(1)}, u32[]{:S(2)}, u32[]{:S(2)}) collective-permute-start(bf16[2,4,256,128]{3,2,1,0:T(8,128)(2,1)} %get-tuple-element.55), channel_id=1, source_target_pairs={{0,28},{4,24},{8,4},{12,0},{16,12},{20,8},{24,20},{28,16},{1,29},{... | collective-permute-start | bytes 1572872 | tf_op jit(solution)/shard_map/ppermute | solution.py:366
  78.1 68.8 %collective-permute-start.4 = (bf16[2,4,256,128]{3,2,1,0:T(8,128)(2,1)}, bf16[2,4,256,128]{3,2,1,0:T(8,128)(2,1)S(1)}, u32[]{:S(2)}, u32[]{:S(2)}) collective-permute-start(bf16[2,4,256,128]{3,2,1,0:T(8,128)(2,1)} %get-tuple-element.54), channel_id=1, source_target_pairs={{0,16},{4,20},{8,24},{12,28},{16,0},{20,4},{24,8},{28,12},{1,17},{... | collective-permute-start | bytes 1572872 | tf_op jit(solution)/shard_map/ppermute | solution.py:366
  80.3 74.0 %collective-permute-start = (bf16[2,4,256,128]{3,2,1,0:T(8,128)(2,1)}, bf16[2,4,256,128]{3,2,1,0:T(8,128)(2,1)S(1)}, u32[]{:S(2)}, u32[]{:S(2)}) collective-permute-start(bf16[2,4,256,128]{3,2,1,0:T(8,128)(2,1)} %get-tuple-element.53), channel_id=1, source_target_pairs={{0,20},{4,16},{8,28},{12,24},{16,4},{20,0},{24,12},{28,8},{1,21},{... | collective-permute-start | bytes 1572872 | tf_op jit(solution)/shard_map/ppermute | solution.py:366
  89.8 65.1 %collective-permute-start.35 = (bf16[4,256,128]{2,1,0:T(8,128)(2,1)}, bf16[4,256,128]{2,1,0:T(8,128)(2,1)S(1)}, u32[]{:S(2)}, u32[]{:S(2)}) collective-permute-start(bf16[4,256,128]{2,1,0:T(8,128)(2,1)} %collective-permute-done.34.refs_0_), channel_id=1, source_target_pairs={{0,1},{1,0},{2,3},{3,2},{4,5},{5,4},{6,7},{7,6},{8,9},{9,8},{10,11... | collective-permute-start | bytes 786440 | tf_op jit(solution)/shard_map/ppermute | solution.py:370
  99.1 57.2 %collective-permute-start.36 = (bf16[4,256,128]{2,1,0:T(8,128)(2,1)}, bf16[4,256,128]{2,1,0:T(8,128)(2,1)}, u32[]{:S(2)}, u32[]{:S(2)}) collective-permute-start(bf16[4,256,128]{2,1,0:T(8,128)(2,1)} %collective-permute-done.34.refs_0_), channel_id=1, source_target_pairs={{0,2},{1,3},{2,0},{3,1},{4,6},{5,7},{6,4},{7,5},{8,10},{9,11},{10,... | collective-permute-start | bytes 786440 | tf_op jit(solution)/shard_map/ppermute | solution.py:370
  108.4 48.4 %collective-permute-start.41 = (bf16[4,256,128]{2,1,0:T(8,128)(2,1)}, bf16[4,256,128]{2,1,0:T(8,128)(2,1)S(1)}, u32[]{:S(2)}, u32[]{:S(2)}) collective-permute-start(bf16[4,256,128]{2,1,0:T(8,128)(2,1)} %collective-permute-done.39.refs_0_), channel_id=1, source_target_pairs={{0,2},{1,3},{2,0},{3,1},{4,6},{5,7},{6,4},{7,5},{8,10},{9,11},{10,... | collective-permute-start | bytes 786440 | tf_op jit(solution)/shard_map/ppermute | solution.py:370
  146.9 11.5 %collective-permute-start.40 = (bf16[4,256,128]{2,1,0:T(8,128)(2,1)}, bf16[4,256,128]{2,1,0:T(8,128)(2,1)S(1)}, u32[]{:S(2)}, u32[]{:S(2)}) collective-permute-start(bf16[4,256,128]{2,1,0:T(8,128)(2,1)} %collective-permute-done.39.refs_0_), channel_id=1, source_target_pairs={{0,1},{1,0},{2,3},{3,2},{4,5},{5,4},{6,7},{7,6},{8,9},{9,8},{10,11... | collective-permute-start | bytes 786440 | tf_op jit(solution)/shard_map/ppermute | solution.py:370
  156.4 13.0 %collective-permute-start.51 = (bf16[4,256,128]{2,1,0:T(8,128)(2,1)}, bf16[4,256,128]{2,1,0:T(8,128)(2,1)S(1)}, u32[]{:S(2)}, u32[]{:S(2)}) collective-permute-start(bf16[4,256,128]{2,1,0:T(8,128)(2,1)} %collective-permute-done.49.refs_0_), channel_id=1, source_target_pairs={{0,2},{1,3},{2,0},{3,1},{4,6},{5,7},{6,4},{7,5},{8,10},{9,11},{10,... | collective-permute-start | bytes 786440 | tf_op jit(solution)/shard_map/ppermute | solution.py:370
  156.9 14.0 %collective-permute-start.50 = (bf16[4,256,128]{2,1,0:T(8,128)(2,1)}, bf16[4,256,128]{2,1,0:T(8,128)(2,1)S(1)}, u32[]{:S(2)}, u32[]{:S(2)}) collective-permute-start(bf16[4,256,128]{2,1,0:T(8,128)(2,1)} %collective-permute-done.49.refs_0_), channel_id=1, source_target_pairs={{0,1},{1,0},{2,3},{3,2},{4,5},{5,4},{6,7},{7,6},{8,9},{9,8},{10,11... | collective-permute-start | bytes 786440 | tf_op jit(solution)/shard_map/ppermute | solution.py:370
  158.4 15.8 %collective-permute-start.55 = (bf16[4,256,128]{2,1,0:T(8,128)(2,1)}, bf16[4,256,128]{2,1,0:T(8,128)(2,1)S(1)}, u32[]{:S(2)}, u32[]{:S(2)}) collective-permute-start(bf16[4,256,128]{2,1,0:T(8,128)(2,1)} %collective-permute-done.54.refs_0_), channel_id=1, source_target_pairs={{0,1},{1,0},{2,3},{3,2},{4,5},{5,4},{6,7},{7,6},{8,9},{9,8},{10,11... | collective-permute-start | bytes 786440 | tf_op jit(solution)/shard_map/ppermute | solution.py:370
  162.9 12.8 %collective-permute-start.56 = (bf16[4,256,128]{2,1,0:T(8,128)(2,1)}, bf16[4,256,128]{2,1,0:T(8,128)(2,1)S(1)}, u32[]{:S(2)}, u32[]{:S(2)}) collective-permute-start(bf16[4,256,128]{2,1,0:T(8,128)(2,1)} %collective-permute-done.54.refs_0_), channel_id=1, source_target_pairs={{0,2},{1,3},{2,0},{3,1},{4,6},{5,7},{6,4},{7,5},{8,10},{9,11},{10,... | collective-permute-start | bytes 786440 | tf_op jit(solution)/shard_map/ppermute | solution.py:370
  164.5 16.3 %collective-permute-start.61 = (bf16[4,256,128]{2,1,0:T(8,128)(2,1)}, bf16[4,256,128]{2,1,0:T(8,128)(2,1)}, u32[]{:S(2)}, u32[]{:S(2)}) collective-permute-start(bf16[4,256,128]{2,1,0:T(8,128)(2,1)} %collective-permute-done.59.refs_0_), channel_id=1, source_target_pairs={{0,2},{1,3},{2,0},{3,1},{4,6},{5,7},{6,4},{7,5},{8,10},{9,11},{10,... | collective-permute-start | bytes 786440 | tf_op jit(solution)/shard_map/ppermute | solution.py:370
  169.4 12.9 %collective-permute-start.60 = (bf16[4,256,128]{2,1,0:T(8,128)(2,1)}, bf16[4,256,128]{2,1,0:T(8,128)(2,1)S(1)}, u32[]{:S(2)}, u32[]{:S(2)}) collective-permute-start(bf16[4,256,128]{2,1,0:T(8,128)(2,1)} %collective-permute-done.59.refs_0_), channel_id=1, source_target_pairs={{0,1},{1,0},{2,3},{3,2},{4,5},{5,4},{6,7},{7,6},{8,9},{9,8},{10,11... | collective-permute-start | bytes 786440 | tf_op jit(solution)/shard_map/ppermute | solution.py:370
  170.9 14.6 %collective-permute-start.65 = (bf16[4,256,128]{2,1,0:T(8,128)(2,1)}, bf16[4,256,128]{2,1,0:T(8,128)(2,1)}, u32[]{:S(2)}, u32[]{:S(2)}) collective-permute-start(bf16[4,256,128]{2,1,0:T(8,128)(2,1)} %collective-permute-done.64.refs_0_), channel_id=1, source_target_pairs={{0,1},{1,0},{2,3},{3,2},{4,5},{5,4},{6,7},{7,6},{8,9},{9,8},{10,11... | collective-permute-start | bytes 786440 | tf_op jit(solution)/shard_map/ppermute | solution.py:370
  174.2 12.9 %collective-permute-start.37 = (bf16[4,256,128]{2,1,0:T(8,128)(2,1)S(1)}, bf16[4,256,128]{2,1,0:T(8,128)(2,1)}, u32[]{:S(2)}, u32[]{:S(2)}) collective-permute-start(bf16[4,256,128]{2,1,0:T(8,128)(2,1)S(1)} %collective-permute-done.35.refs_1_), channel_id=1, source_target_pairs={{0,2},{1,3},{2,0},{3,1},{4,6},{5,7},{6,4},{7,5},{8,10},{9,11},{10,... | collective-permute-start | bytes 786440 | tf_op jit(solution)/shard_map/ppermute | solution.py:370
  175.7 15.3 %collective-permute-start.42 = (bf16[4,256,128]{2,1,0:T(8,128)(2,1)S(1)}, bf16[4,256,128]{2,1,0:T(8,128)(2,1)S(1)}, u32[]{:S(2)}, u32[]{:S(2)}) collective-permute-start(bf16[4,256,128]{2,1,0:T(8,128)(2,1)S(1)} %collective-permute-done.41.refs_2_), channel_id=1, source_target_pairs={{0,1},{1,0},{2,3},{3,2},{4,5},{5,4},{6,7},{7,6},{8,9},{9,8},{10,11... | collective-permute-start | bytes 786440 | tf_op jit(solution)/shard_map/ppermute | solution.py:370
  180.7 40.7 %collective-permute-start.30 = (bf16[2,4,256,128]{3,2,1,0:T(8,128)(2,1)}, bf16[2,4,256,128]{3,2,1,0:T(8,128)(2,1)}, u32[]{:S(2)}, u32[]{:S(2)}) collective-permute-start(bf16[2,4,256,128]{3,2,1,0:T(8,128)(2,1)} %collective-permute-done.28.refs_1_), channel_id=1, source_target_pairs={{0,2},{1,3},{2,0},{3,1},{4,6},{5,7},{6,4},{7,5},{8,10},{9,11},{10,... | collective-permute-start | bytes 1572872 | tf_op jit(solution)/shard_map/ppermute | solution.py:370
  182.3 39.9 %collective-permute-start.26 = (bf16[2,4,256,128]{3,2,1,0:T(8,128)(2,1)S(1)}, bf16[2,4,256,128]{3,2,1,0:T(8,128)(2,1)S(1)}, u32[]{:S(2)}, u32[]{:S(2)}) collective-permute-start(bf16[2,4,256,128]{3,2,1,0:T(8,128)(2,1)S(1)} %collective-permute-done.24.refs_0_), channel_id=1, source_target_pairs={{0,2},{1,3},{2,0},{3,1},{4,6},{5,7},{6,4},{7,5},{8,10},{9,11},{10,... | collective-permute-start | bytes 1572872 | tf_op jit(solution)/shard_map/ppermute | solution.py:370
  185.5 28.8 %collective-permute-start.47 = (bf16[4,256,128]{2,1,0:T(8,128)(2,1)S(1)}, bf16[4,256,128]{2,1,0:T(8,128)(2,1)S(1)}, u32[]{:S(2)}, u32[]{:S(2)}) collective-permute-start(bf16[4,256,128]{2,1,0:T(8,128)(2,1)S(1)} %collective-permute-done.45.refs_1_), channel_id=1, source_target_pairs={{0,2},{1,3},{2,0},{3,1},{4,6},{5,7},{6,4},{7,5},{8,10},{9,11},{10,... | collective-permute-start | bytes 786440 | tf_op jit(solution)/shard_map/ppermute | solution.py:370
  187.0 28.8 %collective-permute-start.52 = (bf16[4,256,128]{2,1,0:T(8,128)(2,1)S(1)}, bf16[4,256,128]{2,1,0:T(8,128)(2,1)S(1)}, u32[]{:S(2)}, u32[]{:S(2)}) collective-permute-start(bf16[4,256,128]{2,1,0:T(8,128)(2,1)S(1)} %collective-permute-done.51.refs_2_), channel_id=1, source_target_pairs={{0,1},{1,0},{2,3},{3,2},{4,5},{5,4},{6,7},{7,6},{8,9},{9,8},{10,11... | collective-permute-start | bytes 786440 | tf_op jit(solution)/shard_map/ppermute | solution.py:370
  191.0 28.9 %collective-permute-start.57 = (bf16[4,256,128]{2,1,0:T(8,128)(2,1)S(1)}, bf16[4,256,128]{2,1,0:T(8,128)(2,1)S(1)}, u32[]{:S(2)}, u32[]{:S(2)}) collective-permute-start(bf16[4,256,128]{2,1,0:T(8,128)(2,1)S(1)} %collective-permute-done.55.refs_1_), channel_id=1, source_target_pairs={{0,2},{1,3},{2,0},{3,1},{4,6},{5,7},{6,4},{7,5},{8,10},{9,11},{10,... | collective-permute-start | bytes 786440 | tf_op jit(solution)/shard_map/ppermute | solution.py:370
  214.3 14.7 %collective-permute-start.25 = (bf16[2,4,256,128]{3,2,1,0:T(8,128)(2,1)S(1)}, bf16[2,4,256,128]{3,2,1,0:T(8,128)(2,1)S(1)}, u32[]{:S(2)}, u32[]{:S(2)}) collective-permute-start(bf16[2,4,256,128]{3,2,1,0:T(8,128)(2,1)S(1)} %collective-permute-done.24.refs_0_), channel_id=1, source_target_pairs={{0,1},{1,0},{2,3},{3,2},{4,5},{5,4},{6,7},{7,6},{8,9},{9,8},{10,11... | collective-permute-start | bytes 1572872 | tf_op jit(solution)/shard_map/ppermute | solution.py:370
  215.8 24.4 %collective-permute-start.21 = (bf16[2,4,256,128]{3,2,1,0:T(8,128)(2,1)S(1)}, bf16[2,4,256,128]{3,2,1,0:T(8,128)(2,1)S(1)}, u32[]{:S(2)}, u32[]{:S(2)}) collective-permute-start(bf16[2,4,256,128]{3,2,1,0:T(8,128)(2,1)S(1)} %collective-permute-done.20.refs_0_), channel_id=1, source_target_pairs={{0,1},{1,0},{2,3},{3,2},{4,5},{5,4},{6,7},{7,6},{8,9},{9,8},{10,11... | collective-permute-start | bytes 1572872 | tf_op jit(solution)/shard_map/ppermute | solution.py:370
  219.9 21.8 %collective-permute-start.22 = (bf16[2,4,256,128]{3,2,1,0:T(8,128)(2,1)S(1)}, bf16[2,4,256,128]{3,2,1,0:T(8,128)(2,1)S(1)}, u32[]{:S(2)}, u32[]{:S(2)}) collective-permute-start(bf16[2,4,256,128]{3,2,1,0:T(8,128)(2,1)S(1)} %collective-permute-done.20.refs_0_), channel_id=1, source_target_pairs={{0,2},{1,3},{2,0},{3,1},{4,6},{5,7},{6,4},{7,5},{8,10},{9,11},{10,... | collective-permute-start | bytes 1572872 | tf_op jit(solution)/shard_map/ppermute | solution.py:370
  221.5 24.5 %collective-permute-start.18 = (bf16[2,4,256,128]{3,2,1,0:T(8,128)(2,1)S(1)}, bf16[2,4,256,128]{3,2,1,0:T(8,128)(2,1)S(1)}, u32[]{:S(2)}, u32[]{:S(2)}) collective-permute-start(bf16[2,4,256,128]{3,2,1,0:T(8,128)(2,1)S(1)} %collective-permute-done.16.refs_0_), channel_id=1, source_target_pairs={{0,2},{1,3},{2,0},{3,1},{4,6},{5,7},{6,4},{7,5},{8,10},{9,11},{10,... | collective-permute-start | bytes 1572872 | tf_op jit(solution)/shard_map/ppermute | solution.py:370
  222.2 29.3 %collective-permute-start.17 = (bf16[2,4,256,128]{3,2,1,0:T(8,128)(2,1)S(1)}, bf16[2,4,256,128]{3,2,1,0:T(8,128)(2,1)S(1)}, u32[]{:S(2)}, u32[]{:S(2)}) collective-permute-start(bf16[2,4,256,128]{3,2,1,0:T(8,128)(2,1)S(1)} %collective-permute-done.16.refs_0_), channel_id=1, source_target_pairs={{0,1},{1,0},{2,3},{3,2},{4,5},{5,4},{6,7},{7,6},{8,9},{9,8},{10,11... | collective-permute-start | bytes 1572872 | tf_op jit(solution)/shard_map/ppermute | solution.py:370
  229.0 33.7 %collective-permute-start.13 = (bf16[2,4,256,128]{3,2,1,0:T(8,128)(2,1)S(1)}, bf16[2,4,256,128]{3,2,1,0:T(8,128)(2,1)S(1)}, u32[]{:S(2)}, u32[]{:S(2)}) collective-permute-start(bf16[2,4,256,128]{3,2,1,0:T(8,128)(2,1)S(1)} %collective-permute-done.12.refs_0_), channel_id=1, source_target_pairs={{0,1},{1,0},{2,3},{3,2},{4,5},{5,4},{6,7},{7,6},{8,9},{9,8},{10,11... | collective-permute-start | bytes 1572872 | tf_op jit(solution)/shard_map/ppermute | solution.py:370
  240.3 24.0 %collective-permute-start.14 = (bf16[2,4,256,128]{3,2,1,0:T(8,128)(2,1)S(1)}, bf16[2,4,256,128]{3,2,1,0:T(8,128)(2,1)S(1)}, u32[]{:S(2)}, u32[]{:S(2)}) collective-permute-start(bf16[2,4,256,128]{3,2,1,0:T(8,128)(2,1)S(1)} %collective-permute-done.12.refs_0_), channel_id=1, source_target_pairs={{0,2},{1,3},{2,0},{3,1},{4,6},{5,7},{6,4},{7,5},{8,10},{9,11},{10,... | collective-permute-start | bytes 1572872 | tf_op jit(solution)/shard_map/ppermute | solution.py:370
  241.8 26.7 %collective-permute-start.10 = (bf16[2,4,256,128]{3,2,1,0:T(8,128)(2,1)S(1)}, bf16[2,4,256,128]{3,2,1,0:T(8,128)(2,1)S(1)}, u32[]{:S(2)}, u32[]{:S(2)}) collective-permute-start(bf16[2,4,256,128]{3,2,1,0:T(8,128)(2,1)S(1)} %collective-permute-done.8.refs_0_), channel_id=1, source_target_pairs={{0,2},{1,3},{2,0},{3,1},{4,6},{5,7},{6,4},{7,5},{8,10},{9,11},{10,... | collective-permute-start | bytes 1572872 | tf_op jit(solution)/shard_map/ppermute | solution.py:370
  246.0 28.0 %collective-permute-start.9 = (bf16[2,4,256,128]{3,2,1,0:T(8,128)(2,1)S(1)}, bf16[2,4,256,128]{3,2,1,0:T(8,128)(2,1)S(1)}, u32[]{:S(2)}, u32[]{:S(2)}) collective-permute-start(bf16[2,4,256,128]{3,2,1,0:T(8,128)(2,1)S(1)} %collective-permute-done.8.refs_0_), channel_id=1, source_target_pairs={{0,1},{1,0},{2,3},{3,2},{4,5},{5,4},{6,7},{7,6},{8,9},{9,8},{10,11... | collective-permute-start | bytes 1572872 | tf_op jit(solution)/shard_map/ppermute | solution.py:370
  251.5 33.7 %collective-permute-start.5 = (bf16[2,4,256,128]{3,2,1,0:T(8,128)(2,1)S(1)}, bf16[2,4,256,128]{3,2,1,0:T(8,128)(2,1)S(1)}, u32[]{:S(2)}, u32[]{:S(2)}) collective-permute-start(bf16[2,4,256,128]{3,2,1,0:T(8,128)(2,1)S(1)} %collective-permute-done.4.refs_0_), channel_id=1, source_target_pairs={{0,1},{1,0},{2,3},{3,2},{4,5},{5,4},{6,7},{7,6},{8,9},{9,8},{10,11... | collective-permute-start | bytes 1572872 | tf_op jit(solution)/shard_map/ppermute | solution.py:370
  262.7 24.0 %collective-permute-start.6 = (bf16[2,4,256,128]{3,2,1,0:T(8,128)(2,1)S(1)}, bf16[2,4,256,128]{3,2,1,0:T(8,128)(2,1)S(1)}, u32[]{:S(2)}, u32[]{:S(2)}) collective-permute-start(bf16[2,4,256,128]{3,2,1,0:T(8,128)(2,1)S(1)} %collective-permute-done.4.refs_0_), channel_id=1, source_target_pairs={{0,2},{1,3},{2,0},{3,1},{4,6},{5,7},{6,4},{7,5},{8,10},{9,11},{10,... | collective-permute-start | bytes 1572872 | tf_op jit(solution)/shard_map/ppermute | solution.py:370
  264.3 26.7 %collective-permute-start.2 = (bf16[2,4,256,128]{3,2,1,0:T(8,128)(2,1)S(1)}, bf16[2,4,256,128]{3,2,1,0:T(8,128)(2,1)S(1)}, u32[]{:S(2)}, u32[]{:S(2)}) collective-permute-start(bf16[2,4,256,128]{3,2,1,0:T(8,128)(2,1)S(1)} %collective-permute-done.refs_0_), channel_id=1, source_target_pairs={{0,2},{1,3},{2,0},{3,1},{4,6},{5,7},{6,4},{7,5},{8,10},{9,11},{10,... | collective-permute-start | bytes 1572872 | tf_op jit(solution)/shard_map/ppermute | solution.py:370
  268.5 28.0 %collective-permute-start.1 = (bf16[2,4,256,128]{3,2,1,0:T(8,128)(2,1)S(1)}, bf16[2,4,256,128]{3,2,1,0:T(8,128)(2,1)S(1)}, u32[]{:S(2)}, u32[]{:S(2)}) collective-permute-start(bf16[2,4,256,128]{3,2,1,0:T(8,128)(2,1)S(1)} %collective-permute-done.refs_0_), channel_id=1, source_target_pairs={{0,1},{1,0},{2,3},{3,2},{4,5},{5,4},{6,7},{7,6},{8,9},{9,8},{10,11... | collective-permute-start | bytes 1572872 | tf_op jit(solution)/shard_map/ppermute | solution.py:370
  274.0 33.7 %collective-permute-start.27 = (bf16[2,4,256,128]{3,2,1,0:T(8,128)(2,1)S(1)}, bf16[2,4,256,128]{3,2,1,0:T(8,128)(2,1)S(1)}, u32[]{:S(2)}, u32[]{:S(2)}) collective-permute-start(bf16[2,4,256,128]{3,2,1,0:T(8,128)(2,1)S(1)} %collective-permute-done.26.refs_2_), channel_id=1, source_target_pairs={{0,1},{1,0},{2,3},{3,2},{4,5},{5,4},{6,7},{7,6},{8,9},{9,8},{10,11... | collective-permute-start | bytes 1572872 | tf_op jit(solution)/shard_map/ppermute | solution.py:370
  285.2 24.0 %collective-permute-start.23 = (bf16[2,4,256,128]{3,2,1,0:T(8,128)(2,1)S(1)}, bf16[2,4,256,128]{3,2,1,0:T(8,128)(2,1)S(1)}, u32[]{:S(2)}, u32[]{:S(2)}) collective-permute-start(bf16[2,4,256,128]{3,2,1,0:T(8,128)(2,1)S(1)} %collective-permute-done.21.refs_1_), channel_id=1, source_target_pairs={{0,2},{1,3},{2,0},{3,1},{4,6},{5,7},{6,4},{7,5},{8,10},{9,11},{10,... | collective-permute-start | bytes 1572872 | tf_op jit(solution)/shard_map/ppermute | solution.py:370
  286.7 32.2 %collective-permute-start.19 = (bf16[2,4,256,128]{3,2,1,0:T(8,128)(2,1)S(1)}, bf16[2,4,256,128]{3,2,1,0:T(8,128)(2,1)S(1)}, u32[]{:S(2)}, u32[]{:S(2)}) collective-permute-start(bf16[2,4,256,128]{3,2,1,0:T(8,128)(2,1)S(1)} %collective-permute-done.18.refs_2_), channel_id=1, source_target_pairs={{0,1},{1,0},{2,3},{3,2},{4,5},{5,4},{6,7},{7,6},{8,9},{9,8},{10,11... | collective-permute-start | bytes 1572872 | tf_op jit(solution)/shard_map/ppermute | solution.py:370
  290.9 29.5 %collective-permute-start.15 = (bf16[2,4,256,128]{3,2,1,0:T(8,128)(2,1)S(1)}, bf16[2,4,256,128]{3,2,1,0:T(8,128)(2,1)S(1)}, u32[]{:S(2)}, u32[]{:S(2)}) collective-permute-start(bf16[2,4,256,128]{3,2,1,0:T(8,128)(2,1)S(1)} %collective-permute-done.13.refs_1_), channel_id=1, source_target_pairs={{0,2},{1,3},{2,0},{3,1},{4,6},{5,7},{6,4},{7,5},{8,10},{9,11},{10,... | collective-permute-start | bytes 1572872 | tf_op jit(solution)/shard_map/ppermute | solution.py:370
  296.4 33.7 %collective-permute-start.11 = (bf16[2,4,256,128]{3,2,1,0:T(8,128)(2,1)S(1)}, bf16[2,4,256,128]{3,2,1,0:T(8,128)(2,1)S(1)}, u32[]{:S(2)}, u32[]{:S(2)}) collective-permute-start(bf16[2,4,256,128]{3,2,1,0:T(8,128)(2,1)S(1)} %collective-permute-done.10.refs_2_), channel_id=1, source_target_pairs={{0,1},{1,0},{2,3},{3,2},{4,5},{5,4},{6,7},{7,6},{8,9},{9,8},{10,11... | collective-permute-start | bytes 1572872 | tf_op jit(solution)/shard_map/ppermute | solution.py:370
  307.7 24.0 %collective-permute-start.7 = (bf16[2,4,256,128]{3,2,1,0:T(8,128)(2,1)S(1)}, bf16[2,4,256,128]{3,2,1,0:T(8,128)(2,1)S(1)}, u32[]{:S(2)}, u32[]{:S(2)}) collective-permute-start(bf16[2,4,256,128]{3,2,1,0:T(8,128)(2,1)S(1)} %collective-permute-done.5.refs_1_), channel_id=1, source_target_pairs={{0,2},{1,3},{2,0},{3,1},{4,6},{5,7},{6,4},{7,5},{8,10},{9,11},{10,... | collective-permute-start | bytes 1572872 | tf_op jit(solution)/shard_map/ppermute | solution.py:370
  309.2 32.2 %collective-permute-start.3 = (bf16[2,4,256,128]{3,2,1,0:T(8,128)(2,1)S(1)}, bf16[2,4,256,128]{3,2,1,0:T(8,128)(2,1)S(1)}, u32[]{:S(2)}, u32[]{:S(2)}) collective-permute-start(bf16[2,4,256,128]{3,2,1,0:T(8,128)(2,1)S(1)} %collective-permute-done.2.refs_2_), channel_id=1, source_target_pairs={{0,1},{1,0},{2,3},{3,2},{4,5},{5,4},{6,7},{7,6},{8,9},{9,8},{10,11... | collective-permute-start | bytes 1572872 | tf_op jit(solution)/shard_map/ppermute | solution.py:370
  318.9 74.8 %collective-permute-start.62 = (bf16[4,256,128]{2,1,0:T(8,128)(2,1)}, bf16[4,256,128]{2,1,0:T(8,128)(2,1)}, u32[]{:S(2)}, u32[]{:S(2)}) collective-permute-start(bf16[4,256,128]{2,1,0:T(8,128)(2,1)} %collective-permute-done.61.refs_2_), channel_id=1, source_target_pairs={{0,1},{1,0},{2,3},{3,2},{4,5},{5,4},{6,7},{7,6},{8,9},{9,8},{10,11... | collective-permute-start | bytes 786440 | tf_op jit(solution)/shard_map/ppermute | solution.py:370
  320.4 76.4 %collective-permute-start.66 = (bf16[4,256,128]{2,1,0:T(8,128)(2,1)}, bf16[4,256,128]{2,1,0:T(8,128)(2,1)}, u32[]{:S(2)}, u32[]{:S(2)}) collective-permute-start(bf16[4,256,128]{2,1,0:T(8,128)(2,1)} %collective-permute-done.64.refs_0_), channel_id=1, source_target_pairs={{0,2},{1,3},{2,0},{3,1},{4,6},{5,7},{6,4},{7,5},{8,10},{9,11},{10,... | collective-permute-start | bytes 786440 | tf_op jit(solution)/shard_map/ppermute | solution.py:370
  330.2 66.7 %collective-permute-start.67 = (bf16[4,256,128]{2,1,0:T(8,128)(2,1)}, bf16[4,256,128]{2,1,0:T(8,128)(2,1)}, u32[]{:S(2)}, u32[]{:S(2)}) collective-permute-start(bf16[4,256,128]{2,1,0:T(8,128)(2,1)} %collective-permute-done.65.refs_1_), channel_id=1, source_target_pairs={{0,2},{1,3},{2,0},{3,1},{4,6},{5,7},{6,4},{7,5},{8,10},{9,11},{10,... | collective-permute-start | bytes 786440 | tf_op jit(solution)/shard_map/ppermute | solution.py:370
  331.7 72.1 %collective-permute-start.31 = (bf16[4,256,128]{2,1,0:T(8,128)(2,1)}, bf16[4,256,128]{2,1,0:T(8,128)(2,1)}, u32[]{:S(2)}, u32[]{:S(2)}) collective-permute-start(bf16[4,256,128]{2,1,0:T(8,128)(2,1)} %get-tuple-element.76.refs_0_), channel_id=1, source_target_pairs={{0,1},{1,0},{2,3},{3,2},{4,5},{5,4},{6,7},{7,6},{8,9},{9,8},{10,11... | collective-permute-start | bytes 786440 | tf_op jit(solution)/shard_map/ppermute | solution.py:370
  341.4 62.4 %collective-permute-start.33 = (bf16[4,256,128]{2,1,0:T(8,128)(2,1)}, bf16[4,256,128]{2,1,0:T(8,128)(2,1)}, u32[]{:S(2)}, u32[]{:S(2)}) collective-permute-start(bf16[4,256,128]{2,1,0:T(8,128)(2,1)} %collective-permute-done.32.refs_2_), channel_id=1, source_target_pairs={{0,1},{1,0},{2,3},{3,2},{4,5},{5,4},{6,7},{7,6},{8,9},{9,8},{10,11... | collective-permute-start | bytes 786440 | tf_op jit(solution)/shard_map/ppermute | solution.py:370
  403.8 10.6 %collective-permute-start.53 = (bf16[256,256]{1,0:T(8,128)(2,1)}, bf16[256,256]{1,0:T(8,128)(2,1)}, u32[]{:S(2)}, u32[]{:S(2)}) collective-permute-start(bf16[256,256]{1,0:T(8,128)(2,1)} %get-tuple-element.89), channel_id=1, source_target_pairs={{0,8},{4,12},{8,16},{12,20},{16,24},{20,28},{24,0},{28,4},{1,9},{5... | collective-permute-start | bytes 393224 | tf_op jit(solution)/shard_map/ppermute | solution.py:366
  403.8 11.4 %collective-permute-start.48 = (bf16[256,256]{1,0:T(8,128)(2,1)}, bf16[256,256]{1,0:T(8,128)(2,1)}, u32[]{:S(2)}, u32[]{:S(2)}) collective-permute-start(bf16[256,256]{1,0:T(8,128)(2,1)} %get-tuple-element.86), channel_id=1, source_target_pairs={{0,24},{4,28},{8,0},{12,4},{16,8},{20,12},{24,16},{28,20},{1,25},{... | collective-permute-start | bytes 393224 | tf_op jit(solution)/shard_map/ppermute | solution.py:366
  407.6 17.4 %collective-permute-start.43 = (bf16[256,256]{1,0:T(8,128)(2,1)}, bf16[256,256]{1,0:T(8,128)(2,1)}, u32[]{:S(2)}, u32[]{:S(2)}) collective-permute-start(bf16[256,256]{1,0:T(8,128)(2,1)} %get-tuple-element.83), channel_id=1, source_target_pairs={{0,20},{4,16},{8,28},{12,24},{16,4},{20,0},{24,12},{28,8},{1,21},{... | collective-permute-start | bytes 393224 | tf_op jit(solution)/shard_map/ppermute | solution.py:366
  407.7 20.1 %collective-permute-start.38 = (bf16[256,256]{1,0:T(8,128)(2,1)}, bf16[256,256]{1,0:T(8,128)(2,1)}, u32[]{:S(2)}, u32[]{:S(2)}) collective-permute-start(bf16[256,256]{1,0:T(8,128)(2,1)} %get-tuple-element.80), channel_id=1, source_target_pairs={{0,16},{4,20},{8,24},{12,28},{16,0},{20,4},{24,8},{28,12},{1,17},{... | collective-permute-start | bytes 393224 | tf_op jit(solution)/shard_map/ppermute | solution.py:366
  (48 other events, 2941.3 us)
